TPU v7x, 128 devices: a whole 4x4x4 slice. The times are simulated.
128 devices in a mesh: sp: 32 (over z, y, core), tp: 4 (over x).
Axes of the slice: x: 4, y: 4, z: 4, core: 2. Of those that a mesh axis runs over, the one named last changes fastest.
Arguments:
- out_grad: bfloat16 [8192, 4096], P('sp'), may hold values from -6 to 6
- stream: bfloat16 [8192, 4096], P('sp'), may hold values from -6 to 6
- norm_gain: bfloat16 [4096], replicated, may hold values from 0.099609375 to 1.8984375
- routes: int32 [8192, 2], P('sp'), may hold values from 0 to 31, all different within a row; in each aligned block of 256 rows (0 to 255, 256 to 511, ...) at most 20 rows name the same one
- route_weight: float32 [8192, 2], P('sp'), may hold values from 0.3 to 1.5
- gate_weight: bfloat16 [32, 4096, 1024], P('sp', None, 'tp'), may hold values from -0.09375 to 0.09375
- up_weight: bfloat16 [32, 4096, 1024], P('sp', None, 'tp'), may hold values from -0.09375 to 0.09375
- down_weight: bfloat16 [32, 1024, 4096], P('sp', 'tp'), may hold values from -0.1875 to 0.1875
- out_proj: bfloat16 [4096, 1024], P(None, 'tp'), may hold values from -0.1875 to 0.1875
- conv_out: bfloat16 [8192, 1024], P('sp', 'tp'), as said below
- gate_branch: bfloat16 [8192, 1024], P('sp', 'tp'), may hold values from -6 to 6
- decay_map: bfloat16 [2, 4, 256, 256], P(None, 'tp'), as said below
- input_map: bfloat16 [2, 4, 256, 256], P(None, 'tp'), as said below
- decay_param: float32 [2, 1024], P(None, 'tp'), as said below
- decay_shift: float32 [2, 8192, 1024], P(None, 'sp', 'tp'), as said below
- states: float32 [2, 8192, 1024], P(None, 'sp', 'tp'), as said below
Outputs:
- conv_grad: float32 [8192, 1024], P('sp', 'tp')
- gate_branch_grad: float32 [8192, 1024], P('sp', 'tp')
- out_proj_grad: float32 [4096, 1024], P('sp', 'tp')
- gate_weight_grad: bfloat16 [32, 4096, 1024], P('sp', None, 'tp')
- up_weight_grad: bfloat16 [32, 4096, 1024], P('sp', None, 'tp')
- down_weight_grad: bfloat16 [32, 1024, 4096], P('sp', 'tp')
Inputs may be any that keep to these rules, and one draw needn't show every extreme that they name: `routes`: each token names 2 different experts. Among the 256 tokens of one index of sp no expert is named more than 20 times, a bound that some expert reaches in some of these blocks. `conv_out`: within -6 to 6. `decay_map`: entries within -4 to 4 times 256 to the power -0.5. `input_map`: entries within -4 to 4 times 256 to the power -0.5. `decay_param`: between 3.7 and 3.5 plus the logarithm of 8192. `decay_shift`: every entry lies between -0.7 and -0.00002. The forward pass's states: they follow the recurrences of the steps from conv_out, decay_map, input_map, decay_param and decay_shift.
All inputs are finite; a program needn't handle non-finite values.
Results may differ from a plain program's by a relative error of at most 0.018.
Values may be sent and summed in bfloat16 or wider, within the bound.
A program may use at most 128 MiB of HBM per device.

v0:
```python
import jax
import jax.numpy as jnp
from jax import lax
from jax.sharding import Mesh
from jax.sharding import PartitionSpec as P

TOP = 2
EXP_DEV = 1
TOK_DEV = 256
SP = ("sp_0", "sp_1", "sp_2")


rate_scale = 8.0
norm_eps = 1e-06


def sent_together(arrays, axis, split_dim, concat_dim, along):
    both = jnp.concatenate(arrays, axis=along)
    out, at, finished = (
        lax.all_to_all(both, axis, split_axis=split_dim, concat_axis=concat_dim, tiled=True),
        0,
        [],
    )
    for a in arrays:
        finished.append(lax.slice_in_dim(out, at, at + a.shape[along], axis=along))
        at += a.shape[along]
    return tuple(finished)


def in_one_piece(arrays, axis, dim, along):
    widths = [a.shape[along] for a in arrays]
    both = jnp.concatenate(arrays, axis=along)
    out = lax.all_gather(both, axis, axis=dim, tiled=True)
    return tuple(jnp.split(out, [sum(widths[:k]) for k in range(1, len(widths))], axis=along))


def in_blocks(x, dim, count):
    dims = x.shape
    tiles = x.reshape(*dims[:dim], count, dims[dim] // count, *dims[dim + 1 :])
    return jnp.moveaxis(tiles, dim, 0)


def in_order(tiles, dim):
    tiles = jnp.moveaxis(tiles, 0, dim)
    dims = tiles.shape
    return tiles.reshape(*dims[:dim], dims[dim] * dims[dim + 1], *dims[dim + 2 :])


def moved_by_axis(tiles, axes, order):
    dims = [lax.axis_size(a) for a in axes]
    tiles = tiles.reshape(*dims, *tiles.shape[1:])
    for k in order:
        tiles = lax.all_to_all(tiles, axes[k], split_axis=k, concat_axis=k, tiled=True)
    return tiles.reshape(-1, *tiles.shape[len(axes) :])


def exchange_by_chip(x, groups, order, split_dim, concat_dim):
    count = lax.axis_size(groups[0]) * lax.axis_size(groups[1])
    tiles = in_blocks(x, split_dim, count)
    return in_order(moved_by_axis(tiles, groups, order), concat_dim)


def summed_on_arrival(x, axis, dim):
    count = lax.axis_size(axis)
    tiles = lax.all_to_all(in_blocks(x, dim, count), axis, 0, 0, tiled=True)
    return jnp.sum(tiles.astype(jnp.float32), axis=0)


def contract(left, right, left_dim, right_dim):
    return lax.dot_general(
        left, right, (((left_dim,), (right_dim,)), ((), ())), preferred_element_type=jnp.float32
    )


def linear_scan(coeffs, values, reverse):

    def combine(earlier, later):
        return (earlier[0] * later[0], later[0] * earlier[1] + later[1])

    return lax.associative_scan(combine, (coeffs, values), axis=0, reverse=reverse)


def silu_grad(values):
    logistic = jax.nn.sigmoid(values)
    return logistic * (1.0 + values * (1.0 - logistic))


def expert_pass(slot_inputs, slot_cotan, gate_local, up_local, down_local):
    gate_pre = contract(slot_inputs, gate_local, 1, 0)
    up_pre = contract(slot_inputs, up_local, 1, 0)
    hidden = (jax.nn.silu(gate_pre) * up_pre).astype(jnp.bfloat16)
    down_wgrad = contract(hidden, slot_cotan, 0, 0)
    hidden_grad = contract(slot_cotan, down_local, 1, 1)
    up_grad = (hidden_grad * jax.nn.silu(gate_pre)).astype(jnp.bfloat16)
    gate_grad = (hidden_grad * up_pre * silu_grad(gate_pre)).astype(jnp.bfloat16)
    gate_wgrad = contract(slot_inputs, gate_grad, 0, 0)
    up_wgrad = contract(slot_inputs, up_grad, 0, 0)
    return (gate_wgrad, up_wgrad, down_wgrad, gate_grad, up_grad)


def block_forward(channels, block_maps):
    shaped = channels.reshape(channels.shape[0], block_maps.shape[0], block_maps.shape[1])
    mapped = jnp.einsum("tkc,kcd->tkd", shaped, block_maps, preferred_element_type=jnp.float32)
    return mapped.reshape(channels.shape)


def block_backward(pre_grad, block_maps):
    shaped = pre_grad.reshape(pre_grad.shape[0], block_maps.shape[0], block_maps.shape[2])
    mapped = jnp.einsum(
        "tkd,kcd->tkc", shaped, block_maps.astype(jnp.float32), precision=lax.Precision.HIGHEST
    )
    return mapped.reshape(pre_grad.shape)


def recurrence_back(adjoint, state_run, conv_float, gate_parts, decay_local, input_local):
    decay_gate, input_gate, decay_base, decay_rate, drive_scale, drive_term = gate_parts
    log_grad = (
        adjoint * (state_run - drive_term)
        - adjoint * input_gate * conv_float * decay_rate * decay_rate / drive_scale
    )
    decay_pre_grad = log_grad * (-rate_scale * decay_base) * decay_gate * (1.0 - decay_gate)
    input_pre_grad = adjoint * drive_scale * conv_float * input_gate * (1.0 - input_gate)
    return (
        adjoint * drive_scale * input_gate
        + block_backward(decay_pre_grad, decay_local)
        + block_backward(input_pre_grad, input_local)
    )


def body(
    out_grad,
    stream,
    norm_gain,
    routes,
    route_weight,
    gate_weight,
    up_weight,
    down_weight,
    out_proj,
    conv_out,
    gate_branch,
    decay_map,
    input_map,
    decay_param,
    decay_shift,
    states,
):
    sources = lax.axis_size(SP)
    quarters = lax.axis_size("tp")
    experts = EXP_DEV * sources
    capacity = (5 * TOP * TOK_DEV + 4 * experts - 1) // (4 * experts)
    token_count, model_width = stream.shape
    stream_f = stream.astype(jnp.float32)
    row_scale = lax.rsqrt(jnp.mean(stream_f * stream_f, axis=1, keepdims=True) + norm_eps)
    unit_rows = stream_f * row_scale
    gain_row = norm_gain.astype(jnp.float32)[None, :]
    normed = (unit_rows * gain_row).astype(jnp.bfloat16)
    pair_expert = routes.reshape(-1)
    pair_count = pair_expert.shape[0]
    onehot = (pair_expert[:, None] == jnp.arange(experts, dtype=jnp.int32)[None, :]).astype(
        jnp.int32
    )
    slot_rank = jnp.sum((jnp.cumsum(onehot, axis=0) - onehot) * onehot, axis=1)
    slot_index = pair_expert * capacity + slot_rank
    slot_pair = (
        jnp.full((experts * capacity,), pair_count, jnp.int32)
        .at[slot_index]
        .set(jnp.arange(pair_count, dtype=jnp.int32))
    )
    slot_token = slot_pair // TOP
    weight_pad = jnp.concatenate([route_weight.reshape(-1), jnp.zeros((1,), jnp.float32)])
    slot_weight = weight_pad[slot_pair][:, None]
    column_width = model_width // quarters
    column_start = lax.axis_index("tp") * column_width
    normed_cols = lax.dynamic_slice_in_dim(normed, column_start, column_width, 1)
    zero_row = jnp.zeros((1, normed_cols.shape[1]), jnp.bfloat16)
    slot_inputs = jnp.concatenate([normed_cols, zero_row])[slot_token]
    slot_cotan = (
        slot_weight
        * jnp.concatenate(
            [lax.dynamic_slice_in_dim(out_grad, column_start, column_width, 1), zero_row]
        )[slot_token].astype(jnp.float32)
    ).astype(jnp.bfloat16)
    part_inputs, part_cotan = sent_together((slot_inputs, slot_cotan), SP, 0, 0, 1)
    got_inputs, got_cotan = in_one_piece((part_inputs, part_cotan), "tp", 1, 0)

    def by_expert(slot_block):
        shaped = slot_block.reshape(sources, EXP_DEV, capacity, model_width)
        return jnp.swapaxes(shaped, 0, 1).reshape(EXP_DEV, sources * capacity, model_width)

    expert_inputs = by_expert(got_inputs)
    expert_cotan = by_expert(got_cotan)
    gate_grads, up_grads, down_grads, partials = ([], [], [], [])
    gate_wgrad, up_wgrad, down_wgrad, gate_grad, up_grad = expert_pass(
        expert_inputs[0], expert_cotan[0], gate_weight[0], up_weight[0], down_weight[0]
    )
    gate_grads.append(gate_wgrad.astype(jnp.bfloat16))
    up_grads.append(up_wgrad.astype(jnp.bfloat16))
    down_grads.append(down_wgrad.astype(jnp.bfloat16))
    partials.append(
        (contract(gate_grad, gate_weight[0], 1, 1) + contract(up_grad, up_weight[0], 1, 1)).astype(
            jnp.bfloat16
        )
    )
    partial_slots = jnp.swapaxes(
        jnp.stack(partials).reshape(EXP_DEV, sources, capacity, model_width), 0, 1
    )
    partial_slots = partial_slots.reshape(sources * EXP_DEV * capacity, model_width)
    summed = (
        lax.psum_scatter(partial_slots, "tp", scatter_dimension=1, tiled=True)
        .astype(jnp.float32)
        .astype(jnp.bfloat16)
    )
    part_back = exchange_by_chip(summed, (("sp_0", "sp_1"), "sp_2"), (1, 0), 0, 0)
    returned = lax.all_gather(part_back, "tp", axis=1, tiled=True)
    normed_grad = jnp.sum(
        returned[slot_index].reshape(token_count, TOP, model_width).astype(jnp.float32), axis=1
    )
    scaled_grad = gain_row * normed_grad
    stream_grad = out_grad.astype(jnp.float32) + row_scale * (
        scaled_grad - unit_rows * jnp.mean(unit_rows * scaled_grad, axis=1, keepdims=True)
    )
    stream_grad_b = stream_grad.astype(jnp.bfloat16)
    total_state = states[0] + states[1]
    gate_float = gate_branch.astype(jnp.float32)
    gelu_gate, gelu_back = jax.vjp(jax.nn.gelu, gate_float)
    lru_out = (total_state * gelu_gate).astype(jnp.bfloat16)
    out_proj_grad = summed_on_arrival(
        contract(stream_grad_b, lru_out, 0, 0).astype(jnp.bfloat16), SP, 0
    )
    lru_out_grad = contract(stream_grad_b, out_proj, 1, 0)
    gate_branch_grad = gelu_back(lru_out_grad * total_state)[0]
    state_grad = lru_out_grad * gelu_gate
    conv_float = conv_out.astype(jnp.float32)
    ones_row = jnp.ones((1, conv_float.shape[1]), jnp.float32)
    saved, summaries = ([], [])
    for direction in range(2):
        decay_gate = jax.nn.sigmoid(block_forward(conv_out, decay_map[direction]))
        input_gate = jax.nn.sigmoid(block_forward(conv_out, input_map[direction]))
        decay_base = jax.nn.softplus(-decay_param[direction])[None, :]
        log_decay = -rate_scale * decay_gate * decay_base + decay_shift[direction]
        decay_rate = jnp.exp(log_decay)
        drive_scale = jnp.sqrt(-jnp.expm1(2.0 * log_decay))
        drive_term = drive_scale * input_gate * conv_float
        if direction == 0:
            reach_coeff, inner_sum = linear_scan(
                jnp.concatenate([decay_rate[1:], ones_row]), state_grad, True
            )
            summaries.append(decay_rate[:1] * reach_coeff[:1])
            summaries.append(decay_rate[:1] * inner_sum[:1])
        else:
            reach_coeff, inner_sum = linear_scan(
                jnp.concatenate([ones_row, decay_rate[:-1]]), state_grad, False
            )
            summaries.append(decay_rate[-1:] * reach_coeff[-1:])
            summaries.append(decay_rate[-1:] * inner_sum[-1:])
        saved.append(
            (
                (decay_gate, input_gate, decay_base, decay_rate, drive_scale, drive_term),
                reach_coeff,
                inner_sum,
            )
        )
    gathered = in_one_piece((summaries[0], summaries[1], summaries[2], summaries[3]), SP, 0, 1)
    device_index = lax.axis_index(SP)
    zero_row = jnp.zeros_like(ones_row)
    from_right = linear_scan(gathered[0], gathered[1], True)[1]
    from_left = linear_scan(gathered[2], gathered[3], False)[1]
    incoming = (
        lax.dynamic_slice_in_dim(jnp.concatenate([from_right[1:], zero_row]), device_index, 1, 0),
        lax.dynamic_slice_in_dim(jnp.concatenate([zero_row, from_left[:-1]]), device_index, 1, 0),
    )
    conv_grad = jnp.zeros_like(conv_float)
    for direction in range(2):
        gate_parts, reach_coeff, inner_sum = saved[direction]
        adjoint = inner_sum + reach_coeff * incoming[direction]
        conv_grad = conv_grad + recurrence_back(
            adjoint,
            states[direction],
            conv_float,
            gate_parts,
            decay_map[direction],
            input_map[direction],
        )
    return (
        conv_grad,
        gate_branch_grad,
        out_proj_grad,
        jnp.stack(gate_grads),
        jnp.stack(up_grads),
        jnp.stack(down_grads),
    )


def solution(mesh):
    torus = Mesh(mesh.devices.reshape(4, 4, 2, mesh.shape["tp"]), ("sp_0", "sp_1", "sp_2", "tp"))
    in_specs = (
        P(SP, None),
        P(SP, None),
        P(),
        P(SP, None),
        P(SP, None),
        P(SP, None, "tp"),
        P(SP, None, "tp"),
        P(SP, "tp", None),
        P(None, "tp"),
        P(SP, "tp"),
        P(SP, "tp"),
        P(None, "tp", None, None),
        P(None, "tp", None, None),
        P(None, "tp"),
        P(None, SP, "tp"),
        P(None, SP, "tp"),
    )
    out_specs = (
        P(SP, "tp"),
        P(SP, "tp"),
        P(SP, "tp"),
        P(SP, None, "tp"),
        P(SP, None, "tp"),
        P(SP, "tp", None),
    )
    return jax.shard_map(body, mesh=torus, in_specs=in_specs, out_specs=out_specs, check_vma=False)
```

profile of v0, /device:TPU:1, one launch (start us, length us, event | category | flops | bytes accessed | tf_op | source)
XLA Modules:
  0.0 490.1 jit_solution(9868422574608995593)
XLA Ops:
  16.5 2.8 gather_fusion.1
  20.6 3.5 gather_fusion.2
  24.1 3.3 reshape.202
  29.6 3.5 gather_fusion
  33.1 3.2 concatenate.142
  39.2 49.0 %all_to_all.24 = bf16[32,20,2048]{2,1,0:T(8,128)(2,1)} all-to-all(bf16[32,20,2048]{2,1,0:T(8,128)(2,1)S(1)} %pad_maximum_fusion), channel_id=1, replica_groups=mesh['sp_0'=4,'sp_1'=4,'sp_2'=2,'tp'=4] {'sp_0','sp_1','sp_2'}, dimensions={0} | all-to-all | bytes 5242880 | tf_op jit(solution)/shard_map/all_to_all | solution.py:20
  88.2 5.2 %all_to_all.16 = bf16[640,2048]{1,0:T(8,128)(2,1)} reshape(bf16[32,20,2048]{2,1,0:T(8,128)(2,1)} %all_to_all.24) | data formatting | bytes 5242880 | tf_op jit(solution)/shard_map/all_to_all | solution.py:20
  97.4 98.0 %all-gather.4.cloned.1.call-done = bf16[1280,4096]{1,0:T(8,128)(2,1)} async-done(((bf16[1280,1024]{1,0:T(8,128)(2,1)}), bf16[1280,4096]{1,0:T(8,128)(2,1)}) %all-gather.4.cloned.1.call-update) | async-done | bytes 10485776 | tf_op jit(solution)/shard_map/all_gather | solution.py:33
  195.5 4.2 fusion.9
  206.8 3.9 add_convert_fusion
  210.7 56.6 %reduce-scatter.2.cloned.1.call-done = bf16[640,1024]{1,0:T(8,128)(2,1)} async-done(((bf16[640,4096]{1,0:T(8,128)(2,1)}), bf16[640,1024]{1,0:T(8,128)(2,1)}) %reduce-scatter.2.cloned.1.call-update) | async-done | bytes 1310736 | tf_op jit(solution)/shard_map/reduce_scatter | solution.py:210
  270.2 5.1 %all_to_all.25 = bf16[16,2,20,1024]{3,0,2,1:T(8,128)(2,1)S(1)} all-to-all(bf16[16,2,20,1024]{3,0,2,1:T(8,128)(2,1)S(1)} %copy.48), channel_id=1, replica_groups=mesh['sp_0'=4,'sp_1'=4,'sp_2'=2,'tp'=4] {'sp_2'}, dimensions={1} | all-to-all | bytes 2621440 | tf_op jit(solution)/shard_map/all_to_all | solution.py:53
  276.7 26.2 %all_to_all.26 = bf16[16,2,20,1024]{3,1,2,0:T(2,128)(2,1)S(1)} all-to-all(bf16[16,2,20,1024]{3,1,2,0:T(2,128)(2,1)S(1)} %copy.49), channel_id=1, replica_groups=mesh['sp_0'=4,'sp_1'=4,'sp_2'=2,'tp'=4] {'sp_0','sp_1'}, dimensions={0} | all-to-all | bytes 2621440 | tf_op jit(solution)/shard_map/all_to_all | solution.py:53
  309.0 6.4 %fusion.1 = bf16[1,4096,256]{2,1,0:T(8,128)(2,1)} fusion(bf16[640,256]{1,0:T(8,128)(2,1)S(1)} %copy-done.14, bf16[1280,4096]{1,0:T(8,128)(2,1)} %all-gather.4.cloned.1.call-done), kind=kOutput, calls=%fused_computation.13 | convolution fusion | flops 1343225856 | bytes 7667712 | tf_op jit(solution)/shard_map/dot_general | solution.py:70
  315.4 3.2 fusion
  318.5 3.3 fusion.2
  321.8 36.2 %all-gather.6.cloned.1.call-done = bf16[640,4096]{1,0:T(8,128)(2,1)} async-done(((bf16[640,1024]{1,0:T(8,128)(2,1)}), bf16[640,4096]{1,0:T(8,128)(2,1)}) %all-gather.6.cloned.1.call-update) | async-done | bytes 5242896 | tf_op jit(solution)/shard_map/all_gather | solution.py:215
  358.1 11.7 %gather_fusion.3 = bf16[512,4096]{1,0:T(8,128)(2,1)} fusion(bf16[640,4096]{1,0:T(8,128)(2,1)} %all-gather.6.cloned.1.call-done, s32[1024]{0:T(1024)S(1)} %pad_clamp_fusion), kind=kCustom, calls=%fused_computation.3 | custom fusion | bytes 8390656 | tf_op jit(solution)/shard_map/gather | solution.py:217
  369.8 10.1 %reshape.203 = f32[256,2,4096]{2,1,0:T(2,128)} reshape(bf16[512,4096]{1,0:T(8,128)(2,1)} %gather_fusion.3) | data formatting | bytes 12582912 | tf_op jit(solution)/shard_map/convert_element_type | solution.py:217
  379.9 13.8 %reduce_sum.50 = f32[256,4096]{1,0:T(8,128)} reduce(f32[256,2,4096]{2,1,0:T(2,128)} %reshape.203, f32[]{:T(128)} %constant.30.clone.1), dimensions={1}, to_apply=%region_6.7 | reduce | flops 1048576 | bytes 12582916 | tf_op jit(solution)/shard_map/reduce_sum | solution.py:216
  393.7 3.2 multiply_reduce_fusion
  408.6 25.6 %all-gather = f32[32,1,1024]{2,1,0:T(1,128)S(1)} all-gather(f32[1,1,1024]{2,1,0:T(1,128)S(1)} %maximum_bitcast_fusion), channel_id=1, replica_groups=mesh['sp_0'=4,'sp_1'=4,'sp_2'=2,'tp'=4] {'sp_0','sp_1','sp_2'}, dimensions={0}, use_global_device_ids=true | all-gather | bytes 135168 | tf_op jit(solution)/shard_map/all_gather | solution.py:33
  447.0 5.1 %all-to-all-start.3 = ((bf16[32,128,256]{2,1,0:T(8,128)(2,1)}), bf16[32,128,256]{2,1,0:T(8,128)(2,1)}, u32[]{:S(2)}, u32[]{:S(2)}) async-start(bf16[32,128,256]{2,1,0:T(8,128)(2,1)} %bitcast.39), calls=%async_computation.4 | async-start | bytes 4194304 | tf_op jit(solution)/shard_map/all_to_all | solution.py:65
  470.4 10.5 %all-to-all-done.3 = bf16[32,128,256]{2,1,0:T(8,128)(2,1)} async-done(((bf16[32,128,256]{2,1,0:T(8,128)(2,1)}), bf16[32,128,256]{2,1,0:T(8,128)(2,1)}, u32[]{:S(2)}, u32[]{:S(2)}) %all-to-all-start.3) | async-done | bytes 2097184 | tf_op jit(solution)/shard_map/all_to_all | solution.py:65
  (532 shorter events, 80.5 us)
Async XLA Ops:
  7.2 188.3 %copy-start = (bf16[1,4096,256]{2,1,0:T(8,128)(2,1)S(1)}, bf16[1,4096,256]{2,1,0:T(8,128)(2,1)}, u32[]{:S(2)}) copy-start(bf16[1,4096,256]{2,1,0:T(8,128)(2,1)} %param.21) | copy-start | bytes 6291460
  7.2 9.1 %copy-start.33 = (f32[256,2]{0,1:T(2,128)S(1)}, f32[256,2]{0,1:T(2,128)}, u32[]{:S(2)}) copy-start(f32[256,2]{0,1:T(2,128)} %param.20) | copy-start | bytes 6148
  7.2 188.3 %all-gather.4.cloned.1.call-start = ((), (), s32[]{:S(2)}) async-start(), calls=%async_computation.5 | async-start | bytes 13107200 | tf_op jit(solution)/shard_map/all_gather | solution.py:33
  9.2 10.3 %copy-start.24 = (bf16[4096]{0:T(1024)(128)(2,1)S(1)}, bf16[4096]{0:T(1024)(128)(2,1)}, u32[]{:S(2)}) copy-start(bf16[4096]{0:T(1024)(128)(2,1)} %param.18) | copy-start | bytes 24580
  11.3 16.1 %copy-start.25 = (f32[256]{0:T(256)}, f32[256]{0:T(256)S(1)}, u32[]{:S(2)}) copy-start(f32[256]{0:T(256)S(1)} %add_rsqrt_fusion) | copy-start | bytes 3076
  97.2 170.1 %reduce-scatter.2.cloned.1.call-start = ((), (), s32[]{:S(2)}) async-start(), calls=%async_computation.6 | async-start | bytes 6553600 | tf_op jit(solution)/shard_map/reduce_scatter | solution.py:210
  195.5 4.2 copy-start.6
  195.5 6.2 %copy-start.35 = (bf16[1280,4096]{1,0:T(8,128)(2,1)S(1)}, bf16[1280,4096]{1,0:T(8,128)(2,1)}, u32[]{:S(2)}) copy-start(bf16[1280,4096]{1,0:T(8,128)(2,1)} %all-gather.4.cloned.1.call-done) | copy-start | bytes 31457284
  210.7 147.4 %all-gather.6.cloned.1.call-start = ((), (), s32[]{:S(2)}) async-start(), calls=%async_computation.7 | async-start | bytes 6553600 | tf_op jit(solution)/shard_map/all_gather | solution.py:215
  307.0 8.3 %slice-start = ((s8[10485760]{0:T(1024)(128)(4,1)}), s8[4194304]{0:T(1024)(128)(4,1)S(1)}, s32[]{:S(2)}) async-start(s8[10485760]{0:T(1024)(128)(4,1)} %bitcast.182), calls=%async_computation.8 | async-start | bytes 8388608
  309.0 6.4 %copy-start.12 = (bf16[640,256]{1,0:T(8,128)(2,1)S(1)}, bf16[640,256]{1,0:T(8,128)(2,1)}, u32[]{:S(2)}) copy-start(bf16[640,256]{1,0:T(8,128)(2,1)} %copy-done.11) | copy-start | bytes 983044
  309.0 6.4 %slice-start.1 = ((s8[10485760]{0:T(1024)(128)(4,1)}), s8[4194304]{0:T(1024)(128)(4,1)S(1)}, s32[]{:S(2)}) async-start(s8[10485760]{0:T(1024)(128)(4,1)} %bitcast.182), calls=%async_computation.9 | async-start | bytes 8388608
  309.0 6.4 %slice-start.2 = ((s8[10485760]{0:T(1024)(128)(4,1)}), s8[2097152]{0:T(1024)(128)(4,1)S(1)}, s32[]{:S(2)}) async-start(s8[10485760]{0:T(1024)(128)(4,1)} %bitcast.182), calls=%async_computation.10 | async-start | bytes 4194304
  379.9 13.8 %copy-start.3 = (bf16[256,4096]{1,0:T(8,128)(2,1)S(1)}, bf16[256,4096]{1,0:T(8,128)(2,1)}, u32[]{:S(2)}) copy-start(bf16[256,4096]{1,0:T(8,128)(2,1)} %param.17) | copy-start | bytes 6291460
  393.7 4.1 copy-start.5
  393.7 4.1 copy-start.26
  447.0 17.6 %copy-start.8 = (f32[2,256,256]{2,1,0:T(8,128)S(1)}, f32[2,256,256]{2,1,0:T(8,128)}, u32[]{:S(2)}) copy-start(f32[2,256,256]{2,1,0:T(8,128)} %param.30) | copy-start | bytes 1572868
  447.0 17.6 %copy-start.20 = (f32[256,256]{1,0:T(8,128)S(1)}, f32[256,256]{1,0:T(8,128)}, u32[]{:S(2)}) copy-start(f32[256,256]{1,0:T(8,128)} %get-tuple-element.118) | copy-start | bytes 786436
  447.0 17.6 %copy-start.22 = (f32[256,256]{1,0:T(8,128)S(1)}, f32[256,256]{1,0:T(8,128)}, u32[]{:S(2)}) copy-start(f32[256,256]{1,0:T(8,128)} %fusion.23) | copy-start | bytes 786436
  447.0 33.8 %all-to-all-start.3 = ((bf16[32,128,256]{2,1,0:T(8,128)(2,1)}), bf16[32,128,256]{2,1,0:T(8,128)(2,1)}, u32[]{:S(2)}, u32[]{:S(2)}) async-start(bf16[32,128,256]{2,1,0:T(8,128)(2,1)} %bitcast.39), calls=%async_computation.4 | async-start | bytes 4194304 | tf_op jit(solution)/shard_map/all_to_all | solution.py:65
  452.3 14.2 %copy-start.16 = (f32[256,256]{1,0:T(8,128)S(1)}, f32[256,256]{1,0:T(8,128)}, u32[]{:S(2)}) copy-start(f32[256,256]{1,0:T(8,128)} %copy-done.15) | copy-start | bytes 786436
  464.7 3.9 copy-start.9
  464.7 3.9 copy-start.17
  466.5 16.9 %copy-start.1 = (bf16[1,4096,256]{2,1,0:T(8,128)(2,1)S(1)}, bf16[1,4096,256]{2,1,0:T(8,128)(2,1)}, u32[]{:S(2)}) copy-start(bf16[1,4096,256]{2,1,0:T(8,128)(2,1)} %param.21) | copy-start | bytes 6291460
  (29 other events, 63.6 us)
Sparse Core Ops, SparseCore 0:
  97.3 98.0 all-gather.3
  210.8 56.4 reduce-scatter.1
  304.7 53.3 all-gather.5
where the time goes:
time: 498 us; the launch traced here: 490 us
  waiting for transfers between devices  201 us (40%)
  blocking collectives  106 us (21%)
  local copies, waits for them, and re-layouts  78.6 us (16%)
  other arithmetic  44.7 us (9%)
  matrix products  37.9 us (8%)
  between operations  16.3 us (3%)
  starting transfers between devices  5.38 us (1%)
    all_gather x1, waiting for transfers between devices, in_one_piece(): out = lax.all_gather(both, axis, axis=dim, tiled=True)  98 us
    reduce_scatter x1, waiting for transfers between devices, body(): lax.psum_scatter(partial_slots, 'tp', scatter_dimension=1, tiled=True)  56.6 us
    all_to_all x1, blocking collectives, sent_together(): lax.all_to_all(both, axis, split_axis=split_dim, concat_axis=concat_dim,...  49 us
    all_gather x1, waiting for transfers between devices, body(): returned = lax.all_gather(part_back, 'tp', axis=1, tiled=True)  36.2 us
    all_to_all x2, blocking collectives, moved_by_axis(): lax.all_to_all(tiles, axes[k], split_axis=k, concat_axis=k, tiled=True)  31.3 us
    dot_general x10, matrix products, contract(): lax.dot_general(left, right, (((left_dim,), (right_dim,)), ((), ())), pre...  29.2 us
    all_gather x1, blocking collectives, in_one_piece(): out = lax.all_gather(both, axis, axis=dim, tiled=True)  25.6 us
    slice x160, local copies, waits for them, and re-layouts, linear_scan(): lax.associative_scan(combine, (coeffs, values), axis=0, reverse=reverse)  14.9 us
  transfers between devices with their start and end apart: 4, of which 4 were waited for; matrix products, arithmetic and copies ran while one was open for 7% of the time, Pallas kernels for 0%

commit v1 on v0

v1 whole, which is shorter than its diff:
```python
import functools

import jax
import jax.numpy as jnp
from jax import lax
from jax.experimental import pallas as pl
from jax.experimental.pallas import tpu as pltpu
from jax.sharding import PartitionSpec as P

BF = jnp.bfloat16
F32 = jnp.float32
I32 = jnp.int32
MESH = pl.DeviceIdType.MESH
ANY = pl.BlockSpec(memory_space=pl.ANY)
VM = pl.BlockSpec(memory_space=pltpu.VMEM)

SPN = 32
TPN = 4
TOK = 256
QW = 1024
FFQ = 256
CHUNKS = 4
SP = "sp"
CW = QW // CHUNKS
HALF = 320
rate_scale = 8.0
norm_eps = 1e-06


def contract(left, right, left_dim, right_dim, precision=None):
    return lax.dot_general(
        left,
        right,
        (((left_dim,), (right_dim,)), ((), ())),
        preferred_element_type=F32,
        precision=precision,
    )


def prep_kernel(stream, out_grad, gain, routes, weight, send, combine, qi, qc0, qc1, scale):
    h = pl.program_id(0)
    low = lax.axis_index("tp") % 2

    @pl.when(h == 0)
    def _():
        wide = stream[...].astype(F32)
        mean = jnp.sum(wide * wide, axis=1, keepdims=True) * (1.0 / (TPN * QW))
        scale[...] = jnp.broadcast_to(lax.rsqrt(mean + norm_eps), (TOK, 128))
        lanes = lax.broadcasted_iota(I32, (TOK, 128), 1)
        r0, r1 = routes[:, 0:1], routes[:, 1:2]
        hot0 = (r0 == lanes).astype(F32)
        hot1 = (r1 == lanes).astype(F32)
        before = (
            lax.broadcasted_iota(I32, (TOK, TOK), 1) < lax.broadcasted_iota(I32, (TOK, TOK), 0)
        ).astype(F32)
        counts = contract(before.astype(BF), (hot0 + hot1).astype(BF), 1, 0)
        upper = lax.axis_index("sp") // 16
        slots = lax.broadcasted_iota(I32, (TOK, 768), 1)

        def places(route, hot):
            rank = jnp.sum(counts * hot, axis=1, keepdims=True).astype(I32)
            pure = (rank // 8) * 256 + route * 8 + rank % 8
            mixed = 512 + route * 8 + (rank - 16)
            of_input = jnp.where(rank < 16, pure, mixed + 4 * upper)
            of_cotan = jnp.where(rank < 16, pure, mixed + 4 * (1 - upper))
            return (slots == of_input).astype(F32), (slots == of_cotan).astype(F32)

        in0, cot0 = places(r0, hot0)
        in1, cot1 = places(r1, hot1)
        both = (in0 + in1).astype(BF)
        qi[...] = both
        combine[...] = both
        qc0[...] = cot0.astype(BF)
        qc1[...] = cot1.astype(BF)

    cols = pl.ds(pl.multiple_of((2 * h + low) * QW, QW), QW)
    normed = (stream[:, cols].astype(F32) * scale[:, 0:1] * gain[:, cols].astype(F32)).astype(BF)
    grad = out_grad[:, cols].astype(F32)
    scaled0 = (weight[:, 0:1] * grad).astype(BF)
    scaled1 = (weight[:, 1:2] * grad).astype(BF)
    for plane in range(3):
        span = slice(plane * 256, plane * 256 + 256)
        rows_in = contract(qi[:, span], normed, 0, 0)
        rows_cot = contract(qc0[:, span], scaled0, 0, 0) + contract(qc1[:, span], scaled1, 0, 0)
        if plane < 2:
            send[0, plane] = rows_in.astype(BF)
            send[0, plane + 2] = rows_cot.astype(BF)
        else:
            send[0, 4] = (rows_in + rows_cot).astype(BF)


def prep(stream, out_grad, gain, routes, weight):
    whole = lambda shape: pl.BlockSpec(shape, lambda h: (0,) * len(shape))
    return pl.pallas_call(
        prep_kernel,
        grid=(2,),
        in_specs=[
            whole((TOK, 4 * QW)),
            whole((TOK, 4 * QW)),
            whole((1, 4 * QW)),
            whole((TOK, 2)),
            whole((TOK, 2)),
        ],
        out_specs=[
            pl.BlockSpec((1, 5, 256, QW), lambda h: (h, 0, 0, 0)),
            whole((TOK, 768)),
        ],
        out_shape=[
            jax.ShapeDtypeStruct((2, 5, 256, QW), BF),
            jax.ShapeDtypeStruct((TOK, 768), BF),
        ],
        scratch_shapes=[
            pltpu.VMEM((TOK, 768), BF),
            pltpu.VMEM((TOK, 768), BF),
            pltpu.VMEM((TOK, 768), BF),
            pltpu.VMEM((TOK, 128), F32),
        ],
        compiler_params=pltpu.CompilerParams(vmem_limit_bytes=48 * 1024 * 1024),
        name="prep",
    )(stream, out_grad, gain, routes, weight)


def greet(s, x):
    barrier = pltpu.get_barrier_semaphore()

    def hello(d, carry):
        pl.semaphore_signal(barrier, inc=1, device_id=(s ^ d, x), device_id_type=MESH)
        return carry

    lax.fori_loop(1, SPN, hello, 0)
    for step in (1, TPN - 1):
        pl.semaphore_signal(
            barrier, inc=1, device_id=(s, lax.rem(x + step, TPN)), device_id_type=MESH
        )
    pl.semaphore_wait(barrier, SPN + 1)


def remote(src, dst, send_sem, recv_sem, target):
    return pltpu.make_async_remote_copy(
        src_ref=src,
        dst_ref=dst,
        send_sem=send_sem,
        recv_sem=recv_sem,
        device_id=target,
        device_id_type=MESH,
    )


def loop(lower, upper, step):
    def run(d, carry):
        step(d)
        return carry

    lax.fori_loop(lower, upper, run, 0)


def dispatch_kernel(send, got, own_sem, send_sem, recv_sem, fwd_send, fwd_recv):
    s = lax.axis_index("sp")
    x = lax.axis_index("tp")
    high, low = x // 2, x % 2
    right, left = lax.rem(x + 1, TPN), lax.rem(x + TPN - 1, TPN)
    greet(s, x)

    def rows(i):
        return pl.ds(pl.multiple_of(i * 8, 8), 8)

    def across(d):
        return remote(
            send.at[:, :, rows(s ^ d), :],
            got.at[:, low, :, rows(s), :],
            send_sem.at[d],
            recv_sem.at[d],
            (s ^ d, x),
        )

    def onward(d, side):
        src = got.at[high, low, :, rows(s ^ d), :]
        return remote(
            src,
            src,
            fwd_send.at[side, d],
            fwd_recv.at[side, d],
            (s, right if side == 0 else left),
        )

    def onward_own(side):
        return remote(
            send.at[high, :, rows(s), :],
            got.at[high, low, :, rows(s), :],
            fwd_send.at[side, 0],
            fwd_recv.at[side, 0],
            (s, right if side == 0 else left),
        )

    def arriving(d, side):
        quarter = left if side == 0 else right
        src = got.at[quarter // 2, quarter % 2, :, rows(s ^ d), :]
        return remote(src, src, fwd_send.at[side, d], fwd_recv.at[side, d], (s, quarter))

    own = pltpu.make_async_copy(
        send.at[:, :, rows(s), :], got.at[:, low, :, rows(s), :], own_sem
    )
    own.start()
    onward_own(0).start()
    onward_own(1).start()
    loop(1, SPN, lambda d: across(d).start())

    def pass_on(d):
        across(d).wait_recv()
        onward(d, 0).start()
        onward(d, 1).start()

    loop(1, SPN, pass_on)
    own.wait()
    onward_own(0).wait_send()
    onward_own(1).wait_send()

    def finish(d):
        across(d).wait_send()
        onward(d, 0).wait_send()
        onward(d, 1).wait_send()

    loop(1, SPN, finish)

    def landed(d):
        arriving(d, 0).wait_recv()
        arriving(d, 1).wait_recv()

    loop(0, SPN, landed)


def dispatch(send):
    return pl.pallas_call(
        dispatch_kernel,
        in_specs=[ANY],
        out_specs=ANY,
        out_shape=jax.ShapeDtypeStruct((2, 2, 5, 256, QW), BF),
        scratch_shapes=[
            pltpu.SemaphoreType.DMA,
            pltpu.SemaphoreType.DMA((SPN,)),
            pltpu.SemaphoreType.DMA((SPN,)),
            pltpu.SemaphoreType.DMA((2, SPN)),
            pltpu.SemaphoreType.DMA((2, SPN)),
        ],
        compiler_params=pltpu.CompilerParams(collective_id=0, has_side_effects=True),
        name="dispatch",
    )(send)


def swap_halves(v):
    tiles = v.reshape(16, 8, v.shape[1])
    return pltpu.roll(tiles, 4, 1).reshape(v.shape)


def expert_kernel(
    got, gate, up, down, part, gate_wg, up_wg, down_wg,
    vin, vcot, vmix, vg, vu, vd, vpart, ogu, od, gp, upre, hg, gu, hid,
    in_sem, w_sem, part_sem, o_sem,
):
    def loads(q):
        hi, lo = q // 2, q % 2
        out = []
        for plane in range(5):
            if plane < 2:
                dst = vin.at[q, pl.ds(plane * 256, 256), :]
            elif plane < 4:
                dst = vcot.at[q, pl.ds((plane - 2) * 256, 256), :]
            else:
                dst = vmix.at[q]
            out.append(pltpu.make_async_copy(got.at[hi, lo, plane], dst, in_sem.at[q, plane]))
        rows = pl.ds(pl.multiple_of(q * QW, QW), QW)
        out.append(pltpu.make_async_copy(gate.at[rows, :], vg.at[q], w_sem.at[0, q]))
        out.append(pltpu.make_async_copy(up.at[rows, :], vu.at[q], w_sem.at[1, q]))
        out.append(pltpu.make_async_copy(down.at[:, rows], vd.at[q], w_sem.at[2, q]))
        return out

    loop(0, TPN, lambda q: [c.start() for c in loads(q)])
    gp[...] = jnp.zeros_like(gp)
    upre[...] = jnp.zeros_like(upre)
    hg[...] = jnp.zeros_like(hg)

    def forward(q):
        for c in loads(q):
            c.wait()
        first = lax.broadcasted_iota(I32, (128, QW), 0) % 8 < 4
        a = vmix[q, 0:128, :].astype(F32)
        b = vmix[q, 128:256, :].astype(F32)
        vin[q, 512:640, :] = jnp.where(first, a, b).astype(BF)
        vcot[q, 512:640, :] = jnp.where(first, b, a).astype(BF)
        rows = vin[q]
        gp[...] += contract(rows, vg[q], 1, 0)
        upre[...] += contract(rows, vu[q], 1, 0)
        hg[...] += contract(vcot[q], vd[q], 1, 1)

    loop(0, TPN, forward)
    hg[512:640, :] = swap_halves(hg[512:640, :])
    gate_pre, up_pre, hidden_grad = gp[...], upre[...], hg[...]
    logistic = jax.nn.sigmoid(gate_pre)
    silu = gate_pre * logistic
    hidden = silu * up_pre
    hid[0:512, :] = hidden[0:512, :].astype(BF)
    hid[512:640, :] = swap_halves(hidden[512:640, :]).astype(BF)
    gu[:, 0:FFQ] = (
        hidden_grad * up_pre * (logistic * (1.0 + gate_pre * (1.0 - logistic)))
    ).astype(BF)
    gu[:, FFQ : 2 * FFQ] = (hidden_grad * silu).astype(BF)

    def part_out(q):
        return pltpu.make_async_copy(vpart.at[q], part.at[q], part_sem.at[q])

    def back(q):
        vpart[q] = (
            contract(gu[:, 0:FFQ], vg[q], 1, 1) + contract(gu[:, FFQ : 2 * FFQ], vu[q], 1, 1)
        ).astype(BF)
        part_out(q).start()

    loop(0, TPN, back)

    def grads_out(q):
        rows = pl.ds(pl.multiple_of(q * QW, QW), QW)
        return (
            pltpu.make_async_copy(ogu.at[0, q], gate_wg.at[rows, :], o_sem.at[0, q]),
            pltpu.make_async_copy(ogu.at[1, q], up_wg.at[rows, :], o_sem.at[1, q]),
            pltpu.make_async_copy(od.at[q], down_wg.at[:, rows], o_sem.at[2, q]),
        )

    def weights(q):
        both = contract(vin[q], gu[...], 0, 0)
        ogu[0, q] = both[:, 0:FFQ].astype(BF)
        ogu[1, q] = both[:, FFQ : 2 * FFQ].astype(BF)
        od[q] = contract(hid[...], vcot[q], 0, 0).astype(BF)
        for c in grads_out(q):
            c.start()

    loop(0, TPN, weights)
    loop(0, TPN, lambda q: part_out(q).wait())
    loop(0, TPN, lambda q: [c.wait() for c in grads_out(q)])


def expert(got, gate, up, down):
    full = TPN * QW
    return pl.pallas_call(
        expert_kernel,
        in_specs=[ANY] * 4,
        out_specs=[ANY] * 4,
        out_shape=[
            jax.ShapeDtypeStruct((TPN, 640, QW), BF),
            jax.ShapeDtypeStruct((full, FFQ), BF),
            jax.ShapeDtypeStruct((full, FFQ), BF),
            jax.ShapeDtypeStruct((FFQ, full), BF),
        ],
        scratch_shapes=[
            pltpu.VMEM((TPN, 640, QW), BF),
            pltpu.VMEM((TPN, 640, QW), BF),
            pltpu.VMEM((TPN, 256, QW), BF),
            pltpu.VMEM((TPN, QW, FFQ), BF),
            pltpu.VMEM((TPN, QW, FFQ), BF),
            pltpu.VMEM((TPN, FFQ, QW), BF),
            pltpu.VMEM((TPN, 640, QW), BF),
            pltpu.VMEM((2, TPN, QW, FFQ), BF),
            pltpu.VMEM((TPN, FFQ, QW), BF),
            pltpu.VMEM((640, FFQ), F32),
            pltpu.VMEM((640, FFQ), F32),
            pltpu.VMEM((640, FFQ), F32),
            pltpu.VMEM((640, 2 * FFQ), BF),
            pltpu.VMEM((640, FFQ), BF),
            pltpu.SemaphoreType.DMA((TPN, 5)),
            pltpu.SemaphoreType.DMA((3, TPN)),
            pltpu.SemaphoreType.DMA((TPN,)),
            pltpu.SemaphoreType.DMA((3, TPN)),
        ],
        compiler_params=pltpu.CompilerParams(vmem_limit_bytes=60 * 1024 * 1024),
        name="expert",
    )(got, gate, up, down)


def back_kernel(
    part, combine, grad, far, near, relay, final, back,
    far_send, far_recv, near_send, near_recv, own_sem, ret_send, ret_recv, all_send, all_recv,
):
    s = lax.axis_index("sp")
    x = lax.axis_index("tp")
    right, left, across = (lax.rem(x + k, TPN) for k in (1, 3, 2))
    greet(s, x)

    def rows(i):
        return pl.ds(pl.multiple_of(i * 8, 8), 8)

    def cols(c):
        return pl.ds(pl.multiple_of(c * CW, CW), CW)

    def half(side):
        return pl.ds(side * HALF, HALF)

    def to_far(c, side):
        return remote(
            part.at[across, half(side), cols(c)],
            far.at[side, c],
            far_send.at[side, c],
            far_recv.at[side, c],
            (s, (right, left)[side]),
        )

    def to_near_plain(c, side):
        return remote(
            part.at[(right, left)[side], half(1 - side), cols(c)],
            near.at[side, c, half(1 - side), :],
            near_send.at[side, 0, c],
            near_recv.at[side, 0, c],
            (s, (right, left)[side]),
        )

    def to_near_sum(c, side):
        return remote(
            relay.at[side, c],
            near.at[side, c, half(side), :],
            near_send.at[side, 1, c],
            near_recv.at[side, 1, c],
            (s, (right, left)[side]),
        )

    def own_back(c):
        return pltpu.make_async_copy(
            final.at[c, :, rows(s), :], back.at[c, :, rows(s), :], own_sem.at[c]
        )

    def home(c, d):
        return remote(
            final.at[c, :, rows(s ^ d), :],
            back.at[c, :, rows(s), :],
            ret_send.at[c, d],
            ret_recv.at[c, d],
            (s ^ d, x),
        )

    def spread(c, side):
        src = grad.at[x, :, cols(c)]
        return remote(
            src, src, all_send.at[side, 0, c], all_recv.at[side, 0, c], (s, (right, left)[side])
        )

    def spread_on(c, side):
        src = grad.at[(left, right)[side], pl.ds(side * 128, 128), cols(c)]
        return remote(
            src, src, all_send.at[side, 1, c], all_recv.at[side, 1, c], (s, (right, left)[side])
        )

    def stage(t):
        @pl.when(t < CHUNKS)
        def _():
            for side in range(2):
                to_far(t, side).start()
                to_near_plain(t, side).start()

        c1 = t - 1

        @pl.when((c1 >= 0) & (c1 < CHUNKS))
        def _():
            for side in range(2):
                to_far(c1, side).wait_recv()
                mine = part[(right, left)[side], pl.ds(side * HALF, HALF), cols(c1)]
                relay[side, c1] = (far[side, c1].astype(F32) + mine.astype(F32)).astype(BF)
                to_near_sum(c1, side).start()

        c2 = t - 2

        @pl.when((c2 >= 0) & (c2 < CHUNKS))
        def _():
            for side in range(2):
                to_near_plain(c2, side).wait_recv()
                to_near_sum(c2, side).wait_recv()
            total = (
                part[x, :, cols(c2)].astype(F32)
                + near[0, c2].astype(F32)
                + near[1, c2].astype(F32)
            ).astype(BF)
            final[c2, 0] = total[0:256]
            final[c2, 1] = total[256:512]
            final[c2, 2, 0:128, :] = total[512:640]
            final[c2, 2, 128:256, :] = total[512:640]
            own_back(c2).start()
            loop(1, SPN, lambda d: home(c2, d).start())

        c3 = t - 3

        @pl.when((c3 >= 0) & (c3 < CHUNKS))
        def _():
            own_back(c3).wait()
            loop(1, SPN, lambda d: home(c3, d).wait_recv())
            summed = contract(combine[...], back[c3].reshape(768, CW), 1, 0)
            grad[x, :, cols(c3)] = summed.astype(BF)
            for side in range(2):
                spread(c3, side).start()

        c4 = t - 4

        @pl.when((c4 >= 0) & (c4 < CHUNKS))
        def _():
            for side in range(2):
                spread(c4, side).wait_recv()
                spread_on(c4, side).start()

    loop(0, CHUNKS + 4, stage)

    def finish(c):
        for side in range(2):
            to_far(c, side).wait_send()
            to_near_plain(c, side).wait_send()
            to_near_sum(c, side).wait_send()
            spread(c, side).wait_send()
            spread_on(c, side).wait_send()
            spread_on(c, side).wait_recv()
        loop(1, SPN, lambda d: home(c, d).wait_send())

    loop(0, CHUNKS, finish)


def send_back(part, combine):
    return pl.pallas_call(
        back_kernel,
        in_specs=[VM, VM],
        out_specs=VM,
        out_shape=jax.ShapeDtypeStruct((TPN, TOK, QW), BF),
        scratch_shapes=[
            pltpu.VMEM((2, CHUNKS, HALF, CW), BF),
            pltpu.VMEM((2, CHUNKS, 2 * HALF, CW), BF),
            pltpu.VMEM((2, CHUNKS, HALF, CW), BF),
            pltpu.VMEM((CHUNKS, 3, 256, CW), BF),
            pltpu.VMEM((CHUNKS, 3, 256, CW), BF),
            pltpu.SemaphoreType.DMA((2, CHUNKS)),
            pltpu.SemaphoreType.DMA((2, CHUNKS)),
            pltpu.SemaphoreType.DMA((2, 2, CHUNKS)),
            pltpu.SemaphoreType.DMA((2, 2, CHUNKS)),
            pltpu.SemaphoreType.DMA((CHUNKS,)),
            pltpu.SemaphoreType.DMA((CHUNKS, SPN)),
            pltpu.SemaphoreType.DMA((CHUNKS, SPN)),
            pltpu.SemaphoreType.DMA((2, 2, CHUNKS)),
            pltpu.SemaphoreType.DMA((2, 2, CHUNKS)),
        ],
        compiler_params=pltpu.CompilerParams(
            collective_id=1, has_side_effects=True, vmem_limit_bytes=48 * 1024 * 1024
        ),
        name="send_back",
    )(part, combine)


def expm1_negative(v):
    series = 1.0 + v * (1.0 / 9.0)
    for k in (8, 7, 6, 5, 4, 3, 2):
        series = 1.0 + v * (1.0 / k) * series
    return jnp.where(v > -0.5, v * series, jnp.exp(v) - 1.0)


def scan_rows(coeff, value, reverse):
    rows = lax.broadcasted_iota(I32, coeff.shape, 0)
    for k in (1, 2, 4, 8, 16, 32, 64, 128):
        if reverse:
            inside = rows < TOK - k
            shift = TOK - k
        else:
            inside = rows >= k
            shift = k
        coeff_far = jnp.where(inside, pltpu.roll(coeff, shift, 0), 1.0)
        value_far = jnp.where(inside, pltpu.roll(value, shift, 0), 0.0)
        value = value + coeff * value_far
        coeff = coeff * coeff_far
    return coeff, value


def mixer_kernel(
    stream, out_grad, gain, grad, states, branch, out_proj, conv, decay_map, input_map, base, shift,
    branch_grad, proj_part, ends, linear, sgb, dot, scale, lru,
):
    def squares(q, carry):
        v = stream[:, pl.ds(pl.multiple_of(q * QW, QW), QW)].astype(F32)
        g = gain[:, pl.ds(pl.multiple_of(q * QW, QW), QW)].astype(F32)
        w = v * (g * grad[q].astype(F32))
        return (
            carry[0] + jnp.sum(v * v, axis=1, keepdims=True),
            carry[1] + jnp.sum(w, axis=1, keepdims=True),
        )

    zero = jnp.zeros((TOK, 1), F32)
    square, along = lax.fori_loop(0, TPN, squares, (zero, zero))
    inverse = 1.0 / (TPN * QW)
    row_scale = lax.rsqrt(square * inverse + norm_eps)
    scale[...] = jnp.broadcast_to(row_scale, (TOK, 128))
    dot[...] = jnp.broadcast_to(along * row_scale * inverse, (TOK, 128))

    def rows_grad(q, carry):
        cols = pl.ds(pl.multiple_of(q * QW, QW), QW)
        r = scale[:, 0:1]
        unit = stream[:, cols].astype(F32) * r
        scaled = gain[:, cols].astype(F32) * grad[q].astype(F32)
        v = (out_grad[:, cols].astype(F32) + r * (scaled - unit * dot[:, 0:1])).astype(BF)
        sgb[:, cols] = v
        return carry + contract(v, out_proj[cols, :], 1, 0)

    lru_grad = lax.fori_loop(0, TPN, rows_grad, jnp.zeros((TOK, FFQ), F32))
    total = states[0] + states[1]
    b = branch[...].astype(F32)
    root = 0.7978845608028654
    tanh = jnp.tanh(root * (b + 0.044715 * b * b * b))
    gelu = 0.5 * b * (1.0 + tanh)
    slope = 0.5 * (1.0 + tanh) + 0.5 * b * (1.0 - tanh * tanh) * root * (
        1.0 + 3.0 * 0.044715 * b * b
    )
    lru[...] = (total * gelu).astype(BF)
    branch_grad[...] = lru_grad * total * slope
    state_grad = lru_grad * gelu

    def proj(q):
        cols = pl.ds(pl.multiple_of(q * QW, QW), QW)
        proj_part[pl.ds(q * 8, 8)] = contract(sgb[:, cols], lru[...], 0, 0).astype(BF).reshape(
            8, 128, FFQ
        )

    loop(0, TPN, proj)
    c = conv[...].astype(F32)
    rows = lax.broadcasted_iota(I32, (TOK, FFQ), 0)
    for d in range(2):
        r = jax.nn.sigmoid(contract(conv[...], decay_map[d], 1, 0))
        i = jax.nn.sigmoid(contract(conv[...], input_map[d], 1, 0))
        rate = (-rate_scale) * base[d : d + 1, :]
        log_decay = r * rate + shift[d]
        decay = jnp.exp(log_decay)
        width = jnp.sqrt(-expm1_negative(2.0 * log_decay))
        drive = width * i * c
        if d == 0:
            coeff = jnp.where(rows == TOK - 1, 1.0, pltpu.roll(decay, TOK - 1, 0))
            edge = slice(0, 1)
        else:
            coeff = jnp.where(rows == 0, 1.0, pltpu.roll(decay, 1, 0))
            edge = slice(TOK - 1, TOK)
        reach, inner = scan_rows(coeff, state_grad, d == 0)
        ends[2 * d : 2 * d + 1, :] = decay[edge] * reach[edge]
        ends[2 * d + 1 : 2 * d + 2, :] = decay[edge] * inner[edge]
        linear[d, 0] = reach
        linear[d, 1] = inner
        linear[d, 2] = width * i
        linear[d, 3] = ((states[d] - drive) - i * c * decay * decay / width) * rate * r * (1.0 - r)
        linear[d, 4] = width * c * i * (1.0 - i)
    ends[4:8, :] = jnp.zeros((4, FFQ), F32)


def mixer(*operands):
    return pl.pallas_call(
        mixer_kernel,
        in_specs=[VM] * 12,
        out_specs=[VM] * 4,
        out_shape=[
            jax.ShapeDtypeStruct((TOK, FFQ), F32),
            jax.ShapeDtypeStruct((SPN, 128, FFQ), BF),
            jax.ShapeDtypeStruct((8, FFQ), F32),
            jax.ShapeDtypeStruct((2, 5, TOK, FFQ), F32),
        ],
        scratch_shapes=[
            pltpu.VMEM((TOK, TPN * QW), BF),
            pltpu.VMEM((TOK, 128), F32),
            pltpu.VMEM((TOK, 128), F32),
            pltpu.VMEM((TOK, FFQ), BF),
        ],
        compiler_params=pltpu.CompilerParams(vmem_limit_bytes=56 * 1024 * 1024),
        name="mixer",
    )(*operands)


def across_kernel(
    ends, proj_part, linear, decay_map, input_map, conv_grad, proj_grad, edges, pieces,
    end_send, end_recv, piece_send, piece_recv, own_sem,
):
    s = lax.axis_index("sp")
    x = lax.axis_index("tp")
    greet(s, x)

    def ends_to(d):
        return remote(ends, edges.at[s], end_send.at[d], end_recv.at[d], (s ^ d, x))

    def piece_to(d):
        return remote(
            proj_part.at[s ^ d], pieces.at[s], piece_send.at[d], piece_recv.at[d], (s ^ d, x)
        )

    loop(1, SPN, lambda d: ends_to(d).start())
    loop(1, SPN, lambda d: piece_to(d).start())
    own = pltpu.make_async_copy(proj_part.at[s], pieces.at[s], own_sem)
    own.start()
    edges[s] = ends[...]
    loop(1, SPN, lambda d: ends_to(d).wait_recv())

    def carry_in(j, carry):
        later = SPN - 1 - j
        e0, e1 = edges[later], edges[j]
        from_right = jnp.where(later > s, e0[1:2] + e0[0:1] * carry[0], carry[0])
        from_left = jnp.where(j < s, e1[3:4] + e1[2:3] * carry[1], carry[1])
        return from_right, from_left

    zero = jnp.zeros((1, FFQ), F32)
    incoming = lax.fori_loop(0, SPN, carry_in, (zero, zero))
    highest = lax.Precision.HIGHEST
    total = jnp.zeros((TOK, FFQ), F32)
    for d in range(2):
        adjoint = linear[d, 1] + linear[d, 0] * incoming[d]
        total = total + (
            adjoint * linear[d, 2]
            + contract(adjoint * linear[d, 3], decay_map[d].astype(F32), 1, 1, highest)
            + contract(adjoint * linear[d, 4], input_map[d].astype(F32), 1, 1, highest)
        )
    conv_grad[...] = total
    own.wait()

    def add(d, acc):
        piece_to(d).wait_recv()
        return acc + pieces[s ^ d].astype(F32)

    proj_grad[...] = lax.fori_loop(1, SPN, add, pieces[s].astype(F32))

    def finish(d):
        ends_to(d).wait_send()
        piece_to(d).wait_send()

    loop(1, SPN, finish)


def across(ends, proj_part, linear, decay_map, input_map):
    return pl.pallas_call(
        across_kernel,
        in_specs=[VM] * 5,
        out_specs=[VM] * 2,
        out_shape=[
            jax.ShapeDtypeStruct((TOK, FFQ), F32),
            jax.ShapeDtypeStruct((128, FFQ), F32),
        ],
        scratch_shapes=[
            pltpu.VMEM((SPN, 8, FFQ), F32),
            pltpu.VMEM((SPN, 128, FFQ), BF),
            pltpu.SemaphoreType.DMA((SPN,)),
            pltpu.SemaphoreType.DMA((SPN,)),
            pltpu.SemaphoreType.DMA((SPN,)),
            pltpu.SemaphoreType.DMA((SPN,)),
            pltpu.SemaphoreType.DMA,
        ],
        compiler_params=pltpu.CompilerParams(
            collective_id=2, has_side_effects=True, vmem_limit_bytes=40 * 1024 * 1024
        ),
        name="across",
    )(ends, proj_part, linear, decay_map, input_map)


def body(
    out_grad,
    stream,
    norm_gain,
    routes,
    route_weight,
    gate_weight,
    up_weight,
    down_weight,
    out_proj,
    conv_out,
    gate_branch,
    decay_map,
    input_map,
    decay_param,
    decay_shift,
    states,
):
    send, combine = prep(stream, out_grad, norm_gain[None, :], routes, route_weight)
    got = dispatch(send)
    part, gate_wgrad, up_wgrad, down_wgrad = expert(
        got, gate_weight[0], up_weight[0], down_weight[0]
    )
    grad = send_back(part, combine)
    base = jax.nn.softplus(-decay_param)
    decay_maps, input_maps = decay_map[:, 0], input_map[:, 0]
    branch_grad, proj_part, ends, linear = mixer(
        stream, out_grad, norm_gain[None, :], grad, states, gate_branch, out_proj, conv_out,
        decay_maps, input_maps, base, decay_shift,
    )
    conv_grad, proj_grad = across(ends, proj_part, linear, decay_maps, input_maps)
    return (
        conv_grad, branch_grad, proj_grad, gate_wgrad[None], up_wgrad[None], down_wgrad[None]
    )


def solution(mesh):
    in_specs = (
        P(SP, None),
        P(SP, None),
        P(),
        P(SP, None),
        P(SP, None),
        P(SP, None, "tp"),
        P(SP, None, "tp"),
        P(SP, "tp", None),
        P(None, "tp"),
        P(SP, "tp"),
        P(SP, "tp"),
        P(None, "tp", None, None),
        P(None, "tp", None, None),
        P(None, "tp"),
        P(None, SP, "tp"),
        P(None, SP, "tp"),
    )
    out_specs = (
        P(SP, "tp"),
        P(SP, "tp"),
        P(SP, "tp"),
        P(SP, None, "tp"),
        P(SP, None, "tp"),
        P(SP, "tp", None),
    )
    return jax.shard_map(body, mesh=mesh, in_specs=in_specs, out_specs=out_specs, check_vma=False)
```

time: 498 us -> 272 us (0.55); the launches traced: 490 us -> 271 us
  Pallas kernels: 0 us -> 258 us
  waiting for transfers between devices: 201 us -> 0 us
  blocking collectives: 106 us -> 0 us
  local copies, waits for them, and re-layouts: 78.6 us -> 12.2 us
  other arithmetic: 44.7 us -> 0.6 us
  matrix products: 37.9 us -> 0 us
  between operations: 16.3 us -> 0.73 us
  starting transfers between devices: 5.38 us -> 0 us
    pallas_call x0 -> x6, Pallas kernels: none -> 258 us  [the longest x1 105 us: dispatch(): pl.pallas_call(dispatch_kernel, in_specs=[ANY], out_specs=ANY, out_shape=...]
    all_gather x2 -> x0, waiting for transfers between devices: 134 us -> none  [the longest x1 98 us: in_one_piece(): out = lax.all_gather(both, axis, axis=dim, tiled=True)]
    all_to_all x3 -> x0, blocking collectives: 80.3 us -> none  [the longest x1 49 us: sent_together(): lax.all_to_all(both, axis, split_axis=split_dim, concat_axis=concat_dim,...]
    reduce_scatter x1 -> x0, waiting for transfers between devices: 56.6 us -> none  [body(): lax.psum_scatter(partial_slots, 'tp', scatter_dimension=1, tiled=True)]
    dot_general x18 -> x0, matrix products: 37.9 us -> none  [the longest x10 29.2 us: contract(): lax.dot_general(left, right, (((left_dim,), (right_dim,)), ((), ())), pre...]
    all_gather x1 -> x0, blocking collectives: 25.6 us -> none  [in_one_piece(): out = lax.all_gather(both, axis, axis=dim, tiled=True)]
    reduce_sum x5 -> x0, other arithmetic: 21.7 us -> none  [the longest x1 13.8 us: body(): jnp.sum(returned[slot_index].reshape(token_count, TOP, model_width).astyp...]
    gather x4 -> x0, local copies, waits for them, and re-layouts: 21.5 us -> none  [the longest x1 11.7 us: body(): returned[slot_index].reshape(token_count, TOP, model_width)]
  transfers between devices with their start and end apart: 4 -> 0, of which waited for: 4 -> 0; matrix products, arithmetic and copies ran while one was open for 7% -> 0% of each run, Pallas kernels for 0% -> 0%
where the time goes in v1:
time: 272 us; the launch traced here: 271 us
  Pallas kernels  258 us (95%)
  local copies, waits for them, and re-layouts  12.2 us (4%)
    pallas_call x1, Pallas kernels, dispatch(): pl.pallas_call(dispatch_kernel, in_specs=[ANY], out_specs=ANY, out_shape=...  105 us
    pallas_call x1, Pallas kernels, send_back(): pl.pallas_call(back_kernel, in_specs=[VM, VM], out_specs=VM, out_shape=ja...  72.5 us
    pallas_call x1, Pallas kernels, across(): pl.pallas_call(across_kernel, in_specs=[VM] * 5, out_specs=[VM] * 2, out_...  42.4 us
    pallas_call x1, Pallas kernels, expert(): pl.pallas_call(expert_kernel, in_specs=[ANY] * 4, out_specs=[ANY] * 4, ou...  18.1 us
    pallas_call x1, Pallas kernels, mixer(): pl.pallas_call(mixer_kernel, in_specs=[VM] * 12, out_specs=[VM] * 4, out_...  13.3 us
    unnamed x24, local copies, waits for them, and re-layouts  11.5 us
    pallas_call x1, Pallas kernels, prep(): pl.pallas_call(prep_kernel, grid=(2,), in_specs=[whole((TOK, 4 * QW)), wh...  6 us

profile of v1, /device:TPU:1, one launch (start us, length us, event | category | flops | bytes accessed | tf_op | source)
XLA Modules:
  0.0 271.3 jit_solution(16249799520142381564)
XLA Ops:
  0.6 0.7 broadcast_in_dim.13.gain
  1.3 0.0 copy-start.7
  1.4 0.8 copy.22.routes
  2.2 0.8 copy.23.weight
  3.0 0.0 copy-start
  3.0 1.6 copy-done
  4.6 1.6 copy-done.1
  6.2 6.0 %prep.1 = (bf16[2,5,256,1024]{3,2,1,0:T(8,128)(2,1)}, bf16[256,768]{1,0:T(8,128)(2,1)S(1)}) custom-call(bf16[256,4096]{1,0:T(8,128)(2,1)S(1)} %copy-done, bf16[256,4096]{1,0:T(8,128)(2,1)S(1)} %copy-done.1, bf16[1,4096]{1,0:T(2,128)(2,1)S(1)} %broadcast_in_dim.13.gain, s32[256,2]{1,0:T(8,128)S(1)} %copy.22.routes, f32[256,2]{1,0:T(8,128)S(1)} %copy.23.weight), custom_call_target="tpu_custom_call" | custom-call | tf_op jit(solution)/shard_map/prep/pallas_call | solution.py:94
  12.2 0.0 copy-done.7
  12.2 105.5 %dispatch.1.got = bf16[2,2,5,256,1024]{4,3,2,1,0:T(8,128)(2,1)} custom-call(bf16[2,5,256,1024]{3,2,1,0:T(8,128)(2,1)} %get-tuple-element.18.send), custom_call_target="tpu_custom_call" | custom-call | tf_op jit(solution)/shard_map/dispatch/pallas_call | solution.py:233
  117.6 18.1 %expert.1 = (bf16[4,640,1024]{2,1,0:T(8,128)(2,1)}, bf16[4096,256]{1,0:T(8,128)(2,1)}, bf16[4096,256]{1,0:T(8,128)(2,1)}, bf16[256,4096]{1,0:T(8,128)(2,1)}) custom-call(bf16[2,2,5,256,1024]{4,3,2,1,0:T(8,128)(2,1)} %dispatch.1.got, bf16[4096,256]{1,0:T(8,128)(2,1)} %bitcast.12, bf16[4096,256]{1,0:T(8,128)(2,1)} %bitcast.13, bf16[256,4096]{1,0:T(8,128)(2,1)} %bitcast.14), custom_call_target="tpu_custom_call" | custom-call | tf_op jit(solution)/shard_map/expert/pallas_call | solution.py:342
  135.7 0.0 copy-start.9
  135.7 72.5 %send_back.1.grad = bf16[4,256,1024]{2,1,0:T(8,128)(2,1)S(1)} custom-call(bf16[4,640,1024]{2,1,0:T(8,128)(2,1)} %get-tuple-element.19.part, bf16[256,768]{1,0:T(8,128)(2,1)S(1)} %get-tuple-element.20.combine), custom_call_target="tpu_custom_call" | custom-call | tf_op jit(solution)/shard_map/send_back/pallas_call | solution.py:519
  208.3 1.3 copy-done.2
  209.6 0.0 copy-done.9
  209.6 0.6 compare_select_fusion.base
  210.2 13.3 %mixer.1 = (f32[256,256]{1,0:T(8,128)}, bf16[32,128,256]{2,1,0:T(8,128)(2,1)}, f32[8,256]{1,0:T(8,128)}, f32[2,5,256,256]{3,2,1,0:T(8,128)}) custom-call(bf16[256,4096]{1,0:T(8,128)(2,1)} %stream.3, bf16[256,4096]{1,0:T(8,128)(2,1)} %out_grad.3, bf16[1,4096]{1,0:T(2,128)(2,1)} %copy-done.7, bf16[4,256,1024]{2,1,0:T(8,128)(2,1)} %copy-done.2, ...), custom_call_target="tpu_custom_call" | custom-call | tf_op jit(solution)/shard_map/mixer/pallas_call | solution.py:647
  223.5 0.0 copy-done.6
  223.5 1.7 copy-done.3
  225.3 1.6 copy-done.4
  226.9 0.7 copy-done.8
  227.6 42.4 %across.1 = (f32[256,256]{1,0:T(8,128)S(1)}, f32[128,256]{1,0:T(8,128)S(1)}) custom-call(f32[8,256]{1,0:T(8,128)S(1)} %copy-done.8, bf16[32,128,256]{2,1,0:T(8,128)(2,1)S(1)} %copy-done.4, f32[2,5,256,256]{3,2,1,0:T(8,128)S(1)} %copy-done.3, bf16[2,256,256]{2,1,0:T(8,128)(2,1)S(1)} %bitcast.9, bf16[2,256,256]{2,1,0:T(8,128)(2,1)S(1)} %bitcast.11), custom_call_target="tpu_custom_call" | custom-call | tf_op jit(solution)/shard_map/across/pallas_call | solution.py:726
  269.9 0.7 copy.26
  270.6 0.7 copy.27
  (8 shorter events, 0.0 us)
Async XLA Ops:
  1.3 10.8 %copy-start.7 = (bf16[1,4096]{1,0:T(2,128)(2,1)}, bf16[1,4096]{1,0:T(2,128)(2,1)S(1)}, u32[]{:S(2)}) copy-start(bf16[1,4096]{1,0:T(2,128)(2,1)S(1)} %broadcast_in_dim.13.gain) | copy-start | bytes 24580
  3.0 1.6 copy-start
  4.6 1.6 copy-start.1
  135.7 73.9 %copy-start.9 = (f32[2,256]{1,0:T(2,128)S(1)}, f32[2,256]{1,0:T(2,128)}, u32[]{:S(2)}) copy-start(f32[2,256]{1,0:T(2,128)} %param.29) | copy-start | bytes 6148
  208.3 1.3 copy-start.2
  210.2 13.3 %copy-start.5 = (bf16[2,1,256,256]{3,2,1,0:T(8,128)(2,1)S(1)}, bf16[2,1,256,256]{3,2,1,0:T(8,128)(2,1)}, u32[]{:S(2)}) copy-start(bf16[2,1,256,256]{3,2,1,0:T(8,128)(2,1)} %param.27) | copy-start | bytes 786436
  210.2 13.3 %copy-start.6 = (bf16[2,1,256,256]{3,2,1,0:T(8,128)(2,1)S(1)}, bf16[2,1,256,256]{3,2,1,0:T(8,128)(2,1)}, u32[]{:S(2)}) copy-start(bf16[2,1,256,256]{3,2,1,0:T(8,128)(2,1)} %param.28) | copy-start | bytes 786436
  223.5 1.7 copy-start.3
  225.3 1.6 copy-start.4
  226.9 0.7 copy-start.8

commit v2 on v1

--- a/solution.py
+++ b/solution.py
@@ -120,6 +120,22 @@
     )(stream, out_grad, gain, routes, weight)
 
 
+NEAR = (
+    (0, 1), (1, 0), (0, 3), (3, 0), (1, 1), (3, 3), (1, 3), (3, 1),
+    (0, 2), (2, 0), (1, 2), (2, 1), (3, 2), (2, 3), (2, 2),
+)
+STEPS = ((0, 0, 1),) + tuple((z, y, c) for c in (0, 1) for z, y in NEAR)
+
+
+def peer(s, k, sign=1):
+    z, y, c = STEPS[k - 1]
+    return (
+        lax.rem(s // 8 + (z if sign > 0 else 4 - z), 4) * 8
+        + lax.rem((s // 2) % 4 + (y if sign > 0 else 4 - y), 4) * 2
+        + lax.rem(s % 2 + c, 2)
+    )
+
+
 def greet(s, x):
     barrier = pltpu.get_barrier_semaphore()
 
@@ -164,69 +180,53 @@
     def rows(i):
         return pl.ds(pl.multiple_of(i * 8, 8), 8)
 
-    def across(d):
+    def over(turn, k, target):
+        hi = high if turn == 0 else 1 - high
         return remote(
-            send.at[:, :, rows(s ^ d), :],
-            got.at[:, low, :, rows(s), :],
-            send_sem.at[d],
-            recv_sem.at[d],
-            (s ^ d, x),
-        )
-
-    def onward(d, side):
-        src = got.at[high, low, :, rows(s ^ d), :]
+            send.at[hi, :, rows(target), :],
+            got.at[hi, low, :, rows(s), :],
+            send_sem.at[turn, k],
+            recv_sem.at[turn, k],
+            (target, x),
+        )
+
+    def onward(src, dst, k, side):
         return remote(
-            src,
-            src,
-            fwd_send.at[side, d],
-            fwd_recv.at[side, d],
-            (s, right if side == 0 else left),
-        )
-
-    def onward_own(side):
-        return remote(
-            send.at[high, :, rows(s), :],
-            got.at[high, low, :, rows(s), :],
-            fwd_send.at[side, 0],
-            fwd_recv.at[side, 0],
-            (s, right if side == 0 else left),
-        )
-
-    def arriving(d, side):
-        quarter = left if side == 0 else right
-        src = got.at[quarter // 2, quarter % 2, :, rows(s ^ d), :]
-        return remote(src, src, fwd_send.at[side, d], fwd_recv.at[side, d], (s, quarter))
+            src, dst, fwd_send.at[side, k], fwd_recv.at[side, k], (s, (right, left)[side])
+        )
+
+    def block(i):
+        return got.at[high, low, :, rows(i), :]
 
     own = pltpu.make_async_copy(
         send.at[:, :, rows(s), :], got.at[:, low, :, rows(s), :], own_sem
     )
     own.start()
-    onward_own(0).start()
-    onward_own(1).start()
-    loop(1, SPN, lambda d: across(d).start())
-
-    def pass_on(d):
-        across(d).wait_recv()
-        onward(d, 0).start()
-        onward(d, 1).start()
-
-    loop(1, SPN, pass_on)
+    for side in range(2):
+        onward(send.at[high, :, rows(s), :], block(s), 0, side).start()
+    for turn in range(2):
+        for k in range(1, SPN):
+            over(turn, k, peer(s, k)).start()
+    for k in range(1, SPN):
+        source = peer(s, k, -1)
+        over(0, k, source).wait_recv()
+        for side in range(2):
+            onward(block(source), block(source), k, side).start()
     own.wait()
-    onward_own(0).wait_send()
-    onward_own(1).wait_send()
-
-    def finish(d):
-        across(d).wait_send()
-        onward(d, 0).wait_send()
-        onward(d, 1).wait_send()
+
+    def finish(k):
+        for turn in range(2):
+            over(turn, k, s ^ 1).wait_send()
+        over(1, k, s ^ 1).wait_recv()
+
+    def finish_onward(k):
+        for side in range(2):
+            copy = onward(block(s), block(s), k, side)
+            copy.wait_send()
+            copy.wait_recv()
 
     loop(1, SPN, finish)
-
-    def landed(d):
-        arriving(d, 0).wait_recv()
-        arriving(d, 1).wait_recv()
-
-    loop(0, SPN, landed)
+    loop(0, SPN, finish_onward)
 
 
 def dispatch(send):
@@ -237,8 +237,8 @@
         out_shape=jax.ShapeDtypeStruct((2, 2, 5, 256, QW), BF),
         scratch_shapes=[
             pltpu.SemaphoreType.DMA,
-            pltpu.SemaphoreType.DMA((SPN,)),
-            pltpu.SemaphoreType.DMA((SPN,)),
+            pltpu.SemaphoreType.DMA((2, SPN)),
+            pltpu.SemaphoreType.DMA((2, SPN)),
             pltpu.SemaphoreType.DMA((2, SPN)),
             pltpu.SemaphoreType.DMA((2, SPN)),
         ],
@@ -424,13 +424,13 @@
             final.at[c, :, rows(s), :], back.at[c, :, rows(s), :], own_sem.at[c]
         )
 
-    def home(c, d):
+    def home(c, k, target):
         return remote(
-            final.at[c, :, rows(s ^ d), :],
+            final.at[c, :, rows(target), :],
             back.at[c, :, rows(s), :],
-            ret_send.at[c, d],
-            ret_recv.at[c, d],
-            (s ^ d, x),
+            ret_send.at[c, k],
+            ret_recv.at[c, k],
+            (target, x),
         )
 
     def spread(c, side):
@@ -479,14 +479,15 @@
             final[c2, 2, 0:128, :] = total[512:640]
             final[c2, 2, 128:256, :] = total[512:640]
             own_back(c2).start()
-            loop(1, SPN, lambda d: home(c2, d).start())
+            for k in range(1, SPN):
+                home(c2, k, peer(s, k)).start()
 
         c3 = t - 3
 
         @pl.when((c3 >= 0) & (c3 < CHUNKS))
         def _():
             own_back(c3).wait()
-            loop(1, SPN, lambda d: home(c3, d).wait_recv())
+            loop(1, SPN, lambda k: home(c3, k, s ^ 1).wait_recv())
             summed = contract(combine[...], back[c3].reshape(768, CW), 1, 0)
             grad[x, :, cols(c3)] = summed.astype(BF)
             for side in range(2):
@@ -510,7 +511,7 @@
             spread(c, side).wait_send()
             spread_on(c, side).wait_send()
             spread_on(c, side).wait_recv()
-        loop(1, SPN, lambda d: home(c, d).wait_send())
+        loop(1, SPN, lambda k: home(c, k, s ^ 1).wait_send())
 
     loop(0, CHUNKS, finish)
 
@@ -676,13 +677,20 @@
     def ends_to(d):
         return remote(ends, edges.at[s], end_send.at[d], end_recv.at[d], (s ^ d, x))
 
-    def piece_to(d):
+    def piece_to(turn, k, target):
+        half = pl.ds(turn * 64, 64)
         return remote(
-            proj_part.at[s ^ d], pieces.at[s], piece_send.at[d], piece_recv.at[d], (s ^ d, x)
+            proj_part.at[target, half, :],
+            pieces.at[s, half, :],
+            piece_send.at[turn, k],
+            piece_recv.at[turn, k],
+            (target, x),
         )
 
     loop(1, SPN, lambda d: ends_to(d).start())
-    loop(1, SPN, lambda d: piece_to(d).start())
+    for turn in range(2):
+        for k in range(1, SPN):
+            piece_to(turn, k, peer(s, k)).start()
     own = pltpu.make_async_copy(proj_part.at[s], pieces.at[s], own_sem)
     own.start()
     edges[s] = ends[...]
@@ -709,15 +717,19 @@
     conv_grad[...] = total
     own.wait()
 
-    def add(d, acc):
-        piece_to(d).wait_recv()
-        return acc + pieces[s ^ d].astype(F32)
-
-    proj_grad[...] = lax.fori_loop(1, SPN, add, pieces[s].astype(F32))
-
-    def finish(d):
-        ends_to(d).wait_send()
-        piece_to(d).wait_send()
+    def landed(k):
+        for turn in range(2):
+            piece_to(turn, k, s ^ 1).wait_recv()
+
+    loop(1, SPN, landed)
+    proj_grad[...] = lax.fori_loop(
+        1, SPN, lambda i, acc: acc + pieces[i].astype(F32), pieces[0].astype(F32)
+    )
+
+    def finish(k):
+        ends_to(k).wait_send()
+        for turn in range(2):
+            piece_to(turn, k, s ^ 1).wait_send()
 
     loop(1, SPN, finish)
 
@@ -736,8 +748,8 @@
             pltpu.VMEM((SPN, 128, FFQ), BF),
             pltpu.SemaphoreType.DMA((SPN,)),
             pltpu.SemaphoreType.DMA((SPN,)),
-            pltpu.SemaphoreType.DMA((SPN,)),
-            pltpu.SemaphoreType.DMA((SPN,)),
+            pltpu.SemaphoreType.DMA((2, SPN)),
+            pltpu.SemaphoreType.DMA((2, SPN)),
             pltpu.SemaphoreType.DMA,
         ],
         compiler_params=pltpu.CompilerParams(

time: 272 us -> 234 us (0.86)
  Pallas kernels: 258 us -> 220 us
    pallas_call x1, Pallas kernels: 105 us -> 73.6 us  [dispatch(): pl.pallas_call(dispatch_kernel, in_specs=[ANY], out_specs=ANY, out_shape=...]
    pallas_call x1, Pallas kernels: 42.4 us -> 34.9 us  [across(): pl.pallas_call(across_kernel, in_specs=[VM] * 5, out_specs=[VM] * 2, out_...]
where the time goes in v2:
time: 234 us
  Pallas kernels  220 us (94%)
  local copies, waits for them, and re-layouts  12.2 us (5%)
    pallas_call x1, Pallas kernels, send_back(): pl.pallas_call(back_kernel, in_specs=[VM, VM], out_specs=VM, out_shape=ja...  74.5 us
    pallas_call x1, Pallas kernels, dispatch(): pl.pallas_call(dispatch_kernel, in_specs=[ANY], out_specs=ANY, out_shape=...  73.6 us
    pallas_call x1, Pallas kernels, across(): pl.pallas_call(across_kernel, in_specs=[VM] * 5, out_specs=[VM] * 2, out_...  34.9 us
    pallas_call x1, Pallas kernels, expert(): pl.pallas_call(expert_kernel, in_specs=[ANY] * 4, out_specs=[ANY] * 4, ou...  18.1 us
    pallas_call x1, Pallas kernels, mixer(): pl.pallas_call(mixer_kernel, in_specs=[VM] * 12, out_specs=[VM] * 4, out_...  13.3 us
    unnamed x24, local copies, waits for them, and re-layouts  11.5 us
    pallas_call x1, Pallas kernels, prep(): pl.pallas_call(prep_kernel, grid=(2,), in_specs=[whole((TOK, 4 * QW)), wh...  6 us

profile of v2, /device:TPU:1, one launch (start us, length us, event | category | flops | bytes accessed | tf_op | source)
XLA Modules:
  0.0 233.9 jit_solution(3890404223878437070)
XLA Ops:
  0.6 0.7 broadcast_in_dim.13.gain
  1.3 0.0 copy-start.7
  1.4 0.8 copy.22.routes
  2.2 0.8 copy.23.weight
  3.0 0.0 copy-start
  3.0 1.6 copy-done
  4.6 1.6 copy-done.1
  6.2 6.0 %prep.1 = (bf16[2,5,256,1024]{3,2,1,0:T(8,128)(2,1)}, bf16[256,768]{1,0:T(8,128)(2,1)S(1)}) custom-call(bf16[256,4096]{1,0:T(8,128)(2,1)S(1)} %copy-done, bf16[256,4096]{1,0:T(8,128)(2,1)S(1)} %copy-done.1, bf16[1,4096]{1,0:T(2,128)(2,1)S(1)} %broadcast_in_dim.13.gain, s32[256,2]{1,0:T(8,128)S(1)} %copy.22.routes, f32[256,2]{1,0:T(8,128)S(1)} %copy.23.weight), custom_call_target="tpu_custom_call" | custom-call | tf_op jit(solution)/shard_map/prep/pallas_call | solution.py:94
  12.2 0.0 copy-done.7
  12.2 73.6 %dispatch.1.got = bf16[2,2,5,256,1024]{4,3,2,1,0:T(8,128)(2,1)} custom-call(bf16[2,5,256,1024]{3,2,1,0:T(8,128)(2,1)} %get-tuple-element.18.send), custom_call_target="tpu_custom_call" | custom-call | tf_op jit(solution)/shard_map/dispatch/pallas_call | solution.py:233
  85.8 18.1 %expert.1 = (bf16[4,640,1024]{2,1,0:T(8,128)(2,1)}, bf16[4096,256]{1,0:T(8,128)(2,1)}, bf16[4096,256]{1,0:T(8,128)(2,1)}, bf16[256,4096]{1,0:T(8,128)(2,1)}) custom-call(bf16[2,2,5,256,1024]{4,3,2,1,0:T(8,128)(2,1)} %dispatch.1.got, bf16[4096,256]{1,0:T(8,128)(2,1)} %bitcast.12, bf16[4096,256]{1,0:T(8,128)(2,1)} %bitcast.13, bf16[256,4096]{1,0:T(8,128)(2,1)} %bitcast.14), custom_call_target="tpu_custom_call" | custom-call | tf_op jit(solution)/shard_map/expert/pallas_call | solution.py:342
  103.8 0.0 copy-start.9
  103.9 74.5 %send_back.1.grad = bf16[4,256,1024]{2,1,0:T(8,128)(2,1)S(1)} custom-call(bf16[4,640,1024]{2,1,0:T(8,128)(2,1)} %get-tuple-element.19.part, bf16[256,768]{1,0:T(8,128)(2,1)S(1)} %get-tuple-element.20.combine), custom_call_target="tpu_custom_call" | custom-call | tf_op jit(solution)/shard_map/send_back/pallas_call | solution.py:520
  178.4 0.0 copy-start.2
  178.4 1.3 copy-done.2
  179.7 0.0 copy-done.9
  179.7 0.6 compare_select_fusion.base
  180.3 13.3 %mixer.1 = (f32[256,256]{1,0:T(8,128)}, bf16[32,128,256]{2,1,0:T(8,128)(2,1)}, f32[8,256]{1,0:T(8,128)}, f32[2,5,256,256]{3,2,1,0:T(8,128)}) custom-call(bf16[256,4096]{1,0:T(8,128)(2,1)} %stream.3, bf16[256,4096]{1,0:T(8,128)(2,1)} %out_grad.3, bf16[1,4096]{1,0:T(2,128)(2,1)} %copy-done.7, bf16[4,256,1024]{2,1,0:T(8,128)(2,1)} %copy-done.2, ...), custom_call_target="tpu_custom_call" | custom-call | tf_op jit(solution)/shard_map/mixer/pallas_call | solution.py:648
  193.6 1.7 copy-done.3
  195.4 1.6 copy-done.4
  197.0 0.7 copy-done.8
  197.7 34.9 %across.1 = (f32[256,256]{1,0:T(8,128)S(1)}, f32[128,256]{1,0:T(8,128)S(1)}) custom-call(f32[8,256]{1,0:T(8,128)S(1)} %copy-done.8, bf16[32,128,256]{2,1,0:T(8,128)(2,1)S(1)} %copy-done.4, f32[2,5,256,256]{3,2,1,0:T(8,128)S(1)} %copy-done.3, bf16[2,256,256]{2,1,0:T(8,128)(2,1)S(1)} %bitcast.9, bf16[2,256,256]{2,1,0:T(8,128)(2,1)S(1)} %bitcast.11), custom_call_target="tpu_custom_call" | custom-call | tf_op jit(solution)/shard_map/across/pallas_call | solution.py:738
  232.6 0.7 copy.26
  233.3 0.7 copy.27
  (8 shorter events, 0.0 us)
Async XLA Ops:
  1.3 10.8 %copy-start.7 = (bf16[1,4096]{1,0:T(2,128)(2,1)}, bf16[1,4096]{1,0:T(2,128)(2,1)S(1)}, u32[]{:S(2)}) copy-start(bf16[1,4096]{1,0:T(2,128)(2,1)S(1)} %broadcast_in_dim.13.gain) | copy-start | bytes 24580
  3.0 1.6 copy-start
  4.6 1.6 copy-start.1
  103.8 75.9 %copy-start.9 = (f32[2,256]{1,0:T(2,128)S(1)}, f32[2,256]{1,0:T(2,128)}, u32[]{:S(2)}) copy-start(f32[2,256]{1,0:T(2,128)} %param.29) | copy-start | bytes 6148
  178.4 1.3 copy-start.2
  180.3 13.3 %copy-start.5 = (bf16[2,1,256,256]{3,2,1,0:T(8,128)(2,1)S(1)}, bf16[2,1,256,256]{3,2,1,0:T(8,128)(2,1)}, u32[]{:S(2)}) copy-start(bf16[2,1,256,256]{3,2,1,0:T(8,128)(2,1)} %param.27) | copy-start | bytes 786436
  180.3 13.3 %copy-start.6 = (bf16[2,1,256,256]{3,2,1,0:T(8,128)(2,1)S(1)}, bf16[2,1,256,256]{3,2,1,0:T(8,128)(2,1)}, u32[]{:S(2)}) copy-start(bf16[2,1,256,256]{3,2,1,0:T(8,128)(2,1)} %param.28) | copy-start | bytes 786436
  193.6 1.7 copy-start.3
  195.4 1.6 copy-start.4
  197.0 0.7 copy-start.8

commit v3 on v2

--- a/solution.py
+++ b/solution.py
@@ -137,6 +137,15 @@
 
 
 def greet(s, x):
+    hello_all(s, x)
+    met()
+
+
+def met():
+    pl.semaphore_wait(pltpu.get_barrier_semaphore(), SPN + 1)
+
+
+def hello_all(s, x):
     barrier = pltpu.get_barrier_semaphore()
 
     def hello(d, carry):
@@ -148,7 +157,6 @@
         pl.semaphore_signal(
             barrier, inc=1, device_id=(s, lax.rem(x + step, TPN)), device_id_type=MESH
         )
-    pl.semaphore_wait(barrier, SPN + 1)
 
 
 def remote(src, dst, send_sem, recv_sem, target):
@@ -570,12 +578,80 @@
 
 def mixer_kernel(
     stream, out_grad, gain, grad, states, branch, out_proj, conv, decay_map, input_map, base, shift,
-    branch_grad, proj_part, ends, linear, sgb, dot, scale, lru,
+    branch_grad, conv_grad, proj_grad,
+    v_stream, v_out, v_grad, v_proj, v_states, v_shift, v_branch, v_conv, v_decay, v_input,
+    sgb, dot, scale, lru, pulled, linear, coeffs,
+    ends, edges, pieces, pair, paired, far_y, far_z, sum_y, sum_z, last_y, last_z,
+    big_sem, small_sem, end_send, end_recv, pair_send, pair_recv, one_send, one_recv,
+    two_send, two_recv,
 ):
+    s = lax.axis_index("sp")
+    x = lax.axis_index("tp")
+    z, y, core = s // 8, (s // 2) % 4, s % 2
+    hello_all(s, x)
+
+    def big(which, q):
+        cols = pl.ds(pl.multiple_of(q * QW, QW), QW)
+        src, dst = (
+            (stream.at[:, cols], v_stream.at[q]),
+            (grad.at[q], v_grad.at[q]),
+            (out_grad.at[:, cols], v_out.at[q]),
+            (out_proj.at[cols, :], v_proj.at[q]),
+        )[which]
+        return pltpu.make_async_copy(src, dst, big_sem.at[which, q])
+
+    small = [
+        pltpu.make_async_copy(src, dst, small_sem.at[k])
+        for k, (src, dst) in enumerate(
+            (
+                (conv, v_conv),
+                (decay_map, v_decay),
+                (input_map, v_input),
+                (shift, v_shift),
+                (states, v_states),
+                (branch, v_branch),
+            )
+        )
+    ]
+    for copy in small:
+        copy.start()
+
+    def begin(q):
+        for which in range(4):
+            big(which, q).start()
+
+    loop(0, TPN, begin)
+    for copy in small:
+        copy.wait()
+
+    c = v_conv[...].astype(F32)
+    rows = lax.broadcasted_iota(I32, (TOK, FFQ), 0)
+    for d in range(2):
+        r = jax.nn.sigmoid(contract(v_conv[...], v_decay[d], 1, 0))
+        i = jax.nn.sigmoid(contract(v_conv[...], v_input[d], 1, 0))
+        rate = (-rate_scale) * base[d : d + 1, :]
+        log_decay = r * rate + v_shift[d]
+        decay = jnp.exp(log_decay)
+        width = jnp.sqrt(-expm1_negative(2.0 * log_decay))
+        drive = width * i * c
+        if d == 0:
+            coeffs[d] = jnp.where(rows == TOK - 1, 1.0, pltpu.roll(decay, TOK - 1, 0))
+            ends[0:1, :] = decay[0:1]
+        else:
+            coeffs[d] = jnp.where(rows == 0, 1.0, pltpu.roll(decay, 1, 0))
+            ends[2:3, :] = decay[TOK - 1 : TOK]
+        linear[d, 0] = width * i
+        linear[d, 1] = (
+            ((v_states[d] - drive) - i * c * decay * decay / width) * rate * r * (1.0 - r)
+        )
+        linear[d, 2] = width * c * i * (1.0 - i)
+
     def squares(q, carry):
-        v = stream[:, pl.ds(pl.multiple_of(q * QW, QW), QW)].astype(F32)
+        big(0, q).wait()
+        big(1, q).wait()
+        v = v_stream[q].astype(F32)
         g = gain[:, pl.ds(pl.multiple_of(q * QW, QW), QW)].astype(F32)
-        w = v * (g * grad[q].astype(F32))
+        w = v * (g * v_grad[q].astype(F32))
         return (
             carry[0] + jnp.sum(v * v, axis=1, keepdims=True),
             carry[1] + jnp.sum(w, axis=1, keepdims=True),
@@ -587,19 +663,22 @@
     row_scale = lax.rsqrt(square * inverse + norm_eps)
     scale[...] = jnp.broadcast_to(row_scale, (TOK, 128))
     dot[...] = jnp.broadcast_to(along * row_scale * inverse, (TOK, 128))
-
-    def rows_grad(q, carry):
-        cols = pl.ds(pl.multiple_of(q * QW, QW), QW)
+    pulled[...] = jnp.zeros_like(pulled)
+
+    def rows_grad(q):
+        big(2, q).wait()
+        big(3, q).wait()
         r = scale[:, 0:1]
-        unit = stream[:, cols].astype(F32) * r
-        scaled = gain[:, cols].astype(F32) * grad[q].astype(F32)
-        v = (out_grad[:, cols].astype(F32) + r * (scaled - unit * dot[:, 0:1])).astype(BF)
-        sgb[:, cols] = v
-        return carry + contract(v, out_proj[cols, :], 1, 0)
-
-    lru_grad = lax.fori_loop(0, TPN, rows_grad, jnp.zeros((TOK, FFQ), F32))
-    total = states[0] + states[1]
-    b = branch[...].astype(F32)
+        unit = v_stream[q].astype(F32) * r
+        scaled = gain[:, pl.ds(pl.multiple_of(q * QW, QW), QW)].astype(F32) * v_grad[q].astype(F32)
+        v = (v_out[q].astype(F32) + r * (scaled - unit * dot[:, 0:1])).astype(BF)
+        sgb[q] = v
+        pulled[...] += contract(v, v_proj[q], 1, 0)
+
+    loop(0, TPN, rows_grad)
+    lru_grad = pulled[...]
+    total = v_states[0] + v_states[1]
+    b = v_branch[...].astype(F32)
     root = 0.7978845608028654
     tanh = jnp.tanh(root * (b + 0.044715 * b * b * b))
     gelu = 0.5 * b * (1.0 + tanh)
@@ -609,92 +688,75 @@
     lru[...] = (total * gelu).astype(BF)
     branch_grad[...] = lru_grad * total * slope
     state_grad = lru_grad * gelu
+    for d in range(2):
+        reach, inner = scan_rows(coeffs[d], state_grad, d == 0)
+        edge = slice(0, 1) if d == 0 else slice(TOK - 1, TOK)
+        decay = ends[2 * d : 2 * d + 1, :]
+        ends[2 * d : 2 * d + 1, :] = decay * reach[edge]
+        ends[2 * d + 1 : 2 * d + 2, :] = decay * inner[edge]
+        linear[d, 3] = reach
+        linear[d, 4] = inner
+
+    def ends_to(k, target):
+        return remote(ends, edges.at[s], end_send.at[k], end_recv.at[k], (target, x))
+
+    met()
+    for k in range(1, SPN):
+        ends_to(k, peer(s, k)).start()
+    edges[s] = ends[...]
+
+    def pair_to(q):
+        return remote(
+            pieces.at[q, :, 1 - core],
+            pair.at[q],
+            pair_send.at[q],
+            pair_recv.at[q],
+            (s + 1 - 2 * core, x),
+        )
 
     def proj(q):
-        cols = pl.ds(pl.multiple_of(q * QW, QW), QW)
-        proj_part[pl.ds(q * 8, 8)] = contract(sgb[:, cols], lru[...], 0, 0).astype(BF).reshape(
-            8, 128, FFQ
-        )
+        pieces[q] = (
+            contract(sgb[q], lru[...], 0, 0).astype(BF).reshape(TPN, 2, 128, FFQ)
+        )
+        pair_to(q).start()
 
     loop(0, TPN, proj)
-    c = conv[...].astype(F32)
-    rows = lax.broadcasted_iota(I32, (TOK, FFQ), 0)
-    for d in range(2):
-        r = jax.nn.sigmoid(contract(conv[...], decay_map[d], 1, 0))
-        i = jax.nn.sigmoid(contract(conv[...], input_map[d], 1, 0))
-        rate = (-rate_scale) * base[d : d + 1, :]
-        log_decay = r * rate + shift[d]
-        decay = jnp.exp(log_decay)
-        width = jnp.sqrt(-expm1_negative(2.0 * log_decay))
-        drive = width * i * c
-        if d == 0:
-            coeff = jnp.where(rows == TOK - 1, 1.0, pltpu.roll(decay, TOK - 1, 0))
-            edge = slice(0, 1)
+
+    def meet(q):
+        pair_to(q).wait_recv()
+        paired[q] = (pieces[q, :, core].astype(F32) + pair[q].astype(F32)).astype(BF)
+
+    loop(0, TPN, meet)
+    first, second = pl.ds(0, 64), pl.ds(64, 64)
+
+    def along_y(k):
+        return lax.rem(y + k, 4), (z * 8 + lax.rem(y + k, 4) * 2 + core, x)
+
+    def along_z(k):
+        return lax.rem(z + k, 4), (lax.rem(z + k, 4) * 8 + y * 2 + core, x)
+
+    def one(side, k):
+        place, target = (along_y, along_z)[side](k)
+        if side == 0:
+            src, dst = paired.at[:, place, first, :], far_y.at[k - 1]
         else:
-            coeff = jnp.where(rows == 0, 1.0, pltpu.roll(decay, 1, 0))
-            edge = slice(TOK - 1, TOK)
-        reach, inner = scan_rows(coeff, state_grad, d == 0)
-        ends[2 * d : 2 * d + 1, :] = decay[edge] * reach[edge]
-        ends[2 * d + 1 : 2 * d + 2, :] = decay[edge] * inner[edge]
-        linear[d, 0] = reach
-        linear[d, 1] = inner
-        linear[d, 2] = width * i
-        linear[d, 3] = ((states[d] - drive) - i * c * decay * decay / width) * rate * r * (1.0 - r)
-        linear[d, 4] = width * c * i * (1.0 - i)
-    ends[4:8, :] = jnp.zeros((4, FFQ), F32)
-
-
-def mixer(*operands):
-    return pl.pallas_call(
-        mixer_kernel,
-        in_specs=[VM] * 12,
-        out_specs=[VM] * 4,
-        out_shape=[
-            jax.ShapeDtypeStruct((TOK, FFQ), F32),
-            jax.ShapeDtypeStruct((SPN, 128, FFQ), BF),
-            jax.ShapeDtypeStruct((8, FFQ), F32),
-            jax.ShapeDtypeStruct((2, 5, TOK, FFQ), F32),
-        ],
-        scratch_shapes=[
-            pltpu.VMEM((TOK, TPN * QW), BF),
-            pltpu.VMEM((TOK, 128), F32),
-            pltpu.VMEM((TOK, 128), F32),
-            pltpu.VMEM((TOK, FFQ), BF),
-        ],
-        compiler_params=pltpu.CompilerParams(vmem_limit_bytes=56 * 1024 * 1024),
-        name="mixer",
-    )(*operands)
-
-
-def across_kernel(
-    ends, proj_part, linear, decay_map, input_map, conv_grad, proj_grad, edges, pieces,
-    end_send, end_recv, piece_send, piece_recv, own_sem,
-):
-    s = lax.axis_index("sp")
-    x = lax.axis_index("tp")
-    greet(s, x)
-
-    def ends_to(d):
-        return remote(ends, edges.at[s], end_send.at[d], end_recv.at[d], (s ^ d, x))
-
-    def piece_to(turn, k, target):
-        half = pl.ds(turn * 64, 64)
-        return remote(
-            proj_part.at[target, half, :],
-            pieces.at[s, half, :],
-            piece_send.at[turn, k],
-            piece_recv.at[turn, k],
-            (target, x),
-        )
-
-    loop(1, SPN, lambda d: ends_to(d).start())
-    for turn in range(2):
-        for k in range(1, SPN):
-            piece_to(turn, k, peer(s, k)).start()
-    own = pltpu.make_async_copy(proj_part.at[s], pieces.at[s], own_sem)
-    own.start()
-    edges[s] = ends[...]
-    loop(1, SPN, lambda d: ends_to(d).wait_recv())
+            src, dst = paired.at[place, :, second, :], far_z.at[k - 1]
+        return remote(src, dst, one_send.at[side, k], one_recv.at[side, k], target)
+
+    def two(side, k):
+        place, target = (along_z, along_y)[side](k)
+        if side == 0:
+            src, dst = sum_y.at[place], last_y.at[k - 1]
+        else:
+            src, dst = sum_z.at[place], last_z.at[k - 1]
+        return remote(src, dst, two_send.at[side, k], two_recv.at[side, k], target)
+
+    for k in (1, 3, 2):
+        for side in range(2):
+            one(side, k).start()
+
+    for k in range(1, SPN):
+        ends_to(k, s ^ 1).wait_recv()
 
     def carry_in(j, carry):
         later = SPN - 1 - j
@@ -703,60 +765,107 @@
         from_left = jnp.where(j < s, e1[3:4] + e1[2:3] * carry[1], carry[1])
         return from_right, from_left
 
-    zero = jnp.zeros((1, FFQ), F32)
-    incoming = lax.fori_loop(0, SPN, carry_in, (zero, zero))
-    highest = lax.Precision.HIGHEST
-    total = jnp.zeros((TOK, FFQ), F32)
-    for d in range(2):
-        adjoint = linear[d, 1] + linear[d, 0] * incoming[d]
-        total = total + (
-            adjoint * linear[d, 2]
-            + contract(adjoint * linear[d, 3], decay_map[d].astype(F32), 1, 1, highest)
-            + contract(adjoint * linear[d, 4], input_map[d].astype(F32), 1, 1, highest)
-        )
-    conv_grad[...] = total
-    own.wait()
-
-    def landed(k):
-        for turn in range(2):
-            piece_to(turn, k, s ^ 1).wait_recv()
-
-    loop(1, SPN, landed)
-    proj_grad[...] = lax.fori_loop(
-        1, SPN, lambda i, acc: acc + pieces[i].astype(F32), pieces[0].astype(F32)
-    )
-
-    def finish(k):
-        ends_to(k).wait_send()
-        for turn in range(2):
-            piece_to(turn, k, s ^ 1).wait_send()
-
-    loop(1, SPN, finish)
-
-
-def across(ends, proj_part, linear, decay_map, input_map):
+    none = jnp.zeros((1, FFQ), F32)
+    incoming = lax.fori_loop(0, SPN, carry_in, (none, none))
+
+    def back_maps(d):
+        adjoint = linear[d, 4] + linear[d, 3] * incoming[d]
+        highest = lax.Precision.HIGHEST
+        return (
+            adjoint * linear[d, 0]
+            + contract(adjoint * linear[d, 1], v_decay[d].astype(F32), 1, 1, highest)
+            + contract(adjoint * linear[d, 2], v_input[d].astype(F32), 1, 1, highest)
+        )
+
+    conv_grad[...] = back_maps(0) + back_maps(1)
+
+    for side in range(2):
+        for k in (1, 3, 2):
+            one(side, k).wait_recv()
+        if side == 0:
+            acc = paired[:, y, first, :].astype(F32)
+        else:
+            acc = paired[z, :, second, :].astype(F32)
+        came = (far_y, far_z)[side]
+        acc = acc + came[0].astype(F32) + came[1].astype(F32) + came[2].astype(F32)
+        (sum_y, sum_z)[side][...] = acc.astype(BF)
+        for k in (1, 3, 2):
+            two(side, k).start()
+
+    for side in range(2):
+        for k in (1, 3, 2):
+            two(side, k).wait_recv()
+        came = (last_y, last_z)[side]
+        acc = (sum_y[z] if side == 0 else sum_z[y]).astype(F32)
+        acc = acc + came[0].astype(F32) + came[1].astype(F32) + came[2].astype(F32)
+        proj_grad[pl.ds(side * 64, 64), :] = acc
+
+    for side in range(2):
+        for k in (1, 3, 2):
+            one(side, k).wait_send()
+            two(side, k).wait_send()
+    loop(1, SPN, lambda k: ends_to(k, s ^ 1).wait_send())
+    loop(0, TPN, lambda q: pair_to(q).wait_send())
+
+
+def mixer(*operands):
+    whole = (TPN, TOK, QW)
+    square = (TOK, FFQ)
+    dma = pltpu.SemaphoreType.DMA
     return pl.pallas_call(
-        across_kernel,
-        in_specs=[VM] * 5,
-        out_specs=[VM] * 2,
+        mixer_kernel,
+        in_specs=[ANY, ANY, VM, ANY, ANY, ANY, ANY, ANY, ANY, ANY, VM, ANY],
+        out_specs=[VM] * 3,
         out_shape=[
-            jax.ShapeDtypeStruct((TOK, FFQ), F32),
+            jax.ShapeDtypeStruct(square, F32),
+            jax.ShapeDtypeStruct(square, F32),
             jax.ShapeDtypeStruct((128, FFQ), F32),
         ],
         scratch_shapes=[
-            pltpu.VMEM((SPN, 8, FFQ), F32),
-            pltpu.VMEM((SPN, 128, FFQ), BF),
-            pltpu.SemaphoreType.DMA((SPN,)),
-            pltpu.SemaphoreType.DMA((SPN,)),
-            pltpu.SemaphoreType.DMA((2, SPN)),
-            pltpu.SemaphoreType.DMA((2, SPN)),
-            pltpu.SemaphoreType.DMA,
+            pltpu.VMEM(whole, BF),
+            pltpu.VMEM(whole, BF),
+            pltpu.VMEM(whole, BF),
+            pltpu.VMEM((TPN, QW, FFQ), BF),
+            pltpu.VMEM((2,) + square, F32),
+            pltpu.VMEM((2,) + square, F32),
+            pltpu.VMEM(square, BF),
+            pltpu.VMEM(square, BF),
+            pltpu.VMEM((2, FFQ, FFQ), BF),
+            pltpu.VMEM((2, FFQ, FFQ), BF),
+            pltpu.VMEM(whole, BF),
+            pltpu.VMEM((TOK, 128), F32),
+            pltpu.VMEM((TOK, 128), F32),
+            pltpu.VMEM(square, BF),
+            pltpu.VMEM(square, F32),
+            pltpu.VMEM((2, 5) + square, F32),
+            pltpu.VMEM((2,) + square, F32),
+            pltpu.VMEM((4, FFQ), F32),
+            pltpu.VMEM((SPN, 4, FFQ), F32),
+            pltpu.VMEM((4, 4, 2, 128, FFQ), BF),
+            pltpu.VMEM((4, 4, 128, FFQ), BF),
+            pltpu.VMEM((4, 4, 128, FFQ), BF),
+            pltpu.VMEM((3, 4, 64, FFQ), BF),
+            pltpu.VMEM((3, 4, 64, FFQ), BF),
+            pltpu.VMEM((4, 64, FFQ), BF),
+            pltpu.VMEM((4, 64, FFQ), BF),
+            pltpu.VMEM((3, 64, FFQ), BF),
+            pltpu.VMEM((3, 64, FFQ), BF),
+            dma((4, TPN)),
+            dma((6,)),
+            dma((SPN,)),
+            dma((SPN,)),
+            dma((TPN,)),
+            dma((TPN,)),
+            dma((2, 4)),
+            dma((2, 4)),
+            dma((2, 4)),
+            dma((2, 4)),
         ],
         compiler_params=pltpu.CompilerParams(
-            collective_id=2, has_side_effects=True, vmem_limit_bytes=40 * 1024 * 1024
+            collective_id=2, has_side_effects=True, vmem_limit_bytes=48 * 1024 * 1024
         ),
-        name="across",
-    )(ends, proj_part, linear, decay_map, input_map)
+        name="mixer",
+    )(*operands)
 
 
 def body(
@@ -784,12 +893,10 @@
     )
     grad = send_back(part, combine)
     base = jax.nn.softplus(-decay_param)
-    decay_maps, input_maps = decay_map[:, 0], input_map[:, 0]
-    branch_grad, proj_part, ends, linear = mixer(
+    branch_grad, conv_grad, proj_grad = mixer(
         stream, out_grad, norm_gain[None, :], grad, states, gate_branch, out_proj, conv_out,
-        decay_maps, input_maps, base, decay_shift,
+        decay_map[:, 0], input_map[:, 0], base, decay_shift,
     )
-    conv_grad, proj_grad = across(ends, proj_part, linear, decay_maps, input_maps)
     return (
         conv_grad, branch_grad, proj_grad, gate_wgrad[None], up_wgrad[None], down_wgrad[None]
     )

time: 234 us -> 207 us (0.88)
  Pallas kernels: 220 us -> 197 us
  local copies, waits for them, and re-layouts: 12.2 us -> 8.94 us
    pallas_call x2 -> x1, Pallas kernels: 48.2 us -> 24.3 us  [mixer(): pl.pallas_call(mixer_kernel, in_specs=[ANY, ANY, VM, ANY, ANY, ANY, ANY,...]
    unnamed x24 -> x27, local copies, waits for them, and re-layouts: 11.5 us -> 8.23 us
where the time goes in v3:
time: 207 us; the launch traced here: 206 us
  Pallas kernels  197 us (95%)
  local copies, waits for them, and re-layouts  8.94 us (4%)
    pallas_call x1, Pallas kernels, send_back(): pl.pallas_call(back_kernel, in_specs=[VM, VM], out_specs=VM, out_shape=ja...  74.7 us
    pallas_call x1, Pallas kernels, dispatch(): pl.pallas_call(dispatch_kernel, in_specs=[ANY], out_specs=ANY, out_shape=...  73.5 us
    pallas_call x1, Pallas kernels, mixer(): pl.pallas_call(mixer_kernel, in_specs=[ANY, ANY, VM, ANY, ANY, ANY, ANY,...  24.3 us
    pallas_call x1, Pallas kernels, expert(): pl.pallas_call(expert_kernel, in_specs=[ANY] * 4, out_specs=[ANY] * 4, ou...  18.1 us
    unnamed x27, local copies, waits for them, and re-layouts  8.23 us
    pallas_call x1, Pallas kernels, prep(): pl.pallas_call(prep_kernel, grid=(2,), in_specs=[whole((TOK, 4 * QW)), wh...  6 us

profile of v3, /device:TPU:1, one launch (start us, length us, event | category | flops | bytes accessed | tf_op | source)
XLA Modules:
  0.0 206.3 jit_solution(5155098207680704031)
XLA Ops:
  0.6 0.7 broadcast_in_dim.13.gain
  1.3 0.8 copy.22.routes
  2.2 0.8 copy.23.weight
  3.0 0.0 copy-start
  3.0 1.6 copy-done
  4.6 1.6 copy-done.2
  6.2 6.0 %prep.1 = (bf16[2,5,256,1024]{3,2,1,0:T(8,128)(2,1)}, bf16[256,768]{1,0:T(8,128)(2,1)S(1)}) custom-call(bf16[256,4096]{1,0:T(8,128)(2,1)S(1)} %copy-done, bf16[256,4096]{1,0:T(8,128)(2,1)S(1)} %copy-done.2, bf16[1,4096]{1,0:T(2,128)(2,1)S(1)} %broadcast_in_dim.13.gain, s32[256,2]{1,0:T(8,128)S(1)} %copy.22.routes, f32[256,2]{1,0:T(8,128)S(1)} %copy.23.weight), custom_call_target="tpu_custom_call" | custom-call | tf_op jit(solution)/shard_map/prep/pallas_call | solution.py:94
  12.2 73.5 %dispatch.1.got = bf16[2,2,5,256,1024]{4,3,2,1,0:T(8,128)(2,1)} custom-call(bf16[2,5,256,1024]{3,2,1,0:T(8,128)(2,1)} %get-tuple-element.15.send), custom_call_target="tpu_custom_call" | custom-call | tf_op jit(solution)/shard_map/dispatch/pallas_call | solution.py:241
  85.7 18.1 %expert.1 = (bf16[4,640,1024]{2,1,0:T(8,128)(2,1)}, bf16[4096,256]{1,0:T(8,128)(2,1)}, bf16[4096,256]{1,0:T(8,128)(2,1)}, bf16[256,4096]{1,0:T(8,128)(2,1)}) custom-call(bf16[2,2,5,256,1024]{4,3,2,1,0:T(8,128)(2,1)} %dispatch.1.got, bf16[4096,256]{1,0:T(8,128)(2,1)} %bitcast.10, bf16[4096,256]{1,0:T(8,128)(2,1)} %bitcast.11, bf16[256,4096]{1,0:T(8,128)(2,1)} %bitcast.12), custom_call_target="tpu_custom_call" | custom-call | tf_op jit(solution)/shard_map/expert/pallas_call | solution.py:350
  103.8 0.0 copy-start.10
  103.8 0.0 copy-start.1
  103.8 0.0 copy-start.4
  103.8 0.0 copy-start.5
  103.8 0.0 copy-start.6
  103.8 0.0 copy-start.7
  103.8 0.0 copy-start.8
  103.9 0.0 copy-start.9
  103.9 74.7 %send_back.1.grad = bf16[4,256,1024]{2,1,0:T(8,128)(2,1)S(1)} custom-call(bf16[4,640,1024]{2,1,0:T(8,128)(2,1)} %get-tuple-element.16.part, bf16[256,768]{1,0:T(8,128)(2,1)S(1)} %get-tuple-element.17.combine), custom_call_target="tpu_custom_call" | custom-call | tf_op jit(solution)/shard_map/send_back/pallas_call | solution.py:528
  178.5 0.0 copy-start.3
  178.5 1.3 copy-done.3
  180.0 24.3 %mixer.1 = (f32[256,256]{1,0:T(8,128)S(1)}, f32[256,256]{1,0:T(8,128)S(1)}, f32[128,256]{1,0:T(8,128)S(1)}) custom-call(bf16[256,4096]{1,0:T(8,128)(2,1)S(1)} %copy-done.1, bf16[256,4096]{1,0:T(8,128)(2,1)} %out_grad.3, bf16[1,4096]{1,0:T(2,128)(2,1)S(1)} %broadcast_in_dim.13.gain, bf16[4,256,1024]{2,1,0:T(8,128)(2,1)} %copy-done.3, ...), custom_call_target="tpu_custom_call" | custom-call | tf_op jit(solution)/shard_map/mixer/pallas_call | solution.py:815
  204.3 0.7 copy.27
  205.0 0.7 copy.28
  205.7 0.7 copy.29
  (10 shorter events, 0.0 us)
Async XLA Ops:
  3.0 1.6 copy-start
  4.6 1.6 copy-start.2
  103.8 76.1 %copy-start.10 = (f32[2,256]{1,0:T(2,128)S(1)}, f32[2,256]{1,0:T(2,128)}, u32[]{:S(2)}) copy-start(f32[2,256]{1,0:T(2,128)} %param.29) | copy-start | bytes 6148
  103.8 76.1 %copy-start.1 = (bf16[256,4096]{1,0:T(8,128)(2,1)S(1)}, bf16[256,4096]{1,0:T(8,128)(2,1)}, u32[]{:S(2)}) copy-start(bf16[256,4096]{1,0:T(8,128)(2,1)} %stream.3) | copy-start | bytes 6291460
  103.8 76.1 %copy-start.4 = (f32[2,256,256]{2,1,0:T(8,128)S(1)}, f32[2,256,256]{2,1,0:T(8,128)}, u32[]{:S(2)}) copy-start(f32[2,256,256]{2,1,0:T(8,128)} %states.1) | copy-start | bytes 1572868
  103.8 76.1 %copy-start.5 = (f32[2,256,256]{2,1,0:T(8,128)S(1)}, f32[2,256,256]{2,1,0:T(8,128)}, u32[]{:S(2)}) copy-start(f32[2,256,256]{2,1,0:T(8,128)} %shift.1) | copy-start | bytes 1572868
  103.8 76.1 %copy-start.6 = (bf16[2,1,256,256]{3,2,1,0:T(8,128)(2,1)S(1)}, bf16[2,1,256,256]{3,2,1,0:T(8,128)(2,1)}, u32[]{:S(2)}) copy-start(bf16[2,1,256,256]{3,2,1,0:T(8,128)(2,1)} %param.27) | copy-start | bytes 786436
  103.8 76.1 %copy-start.7 = (bf16[2,1,256,256]{3,2,1,0:T(8,128)(2,1)S(1)}, bf16[2,1,256,256]{3,2,1,0:T(8,128)(2,1)}, u32[]{:S(2)}) copy-start(bf16[2,1,256,256]{3,2,1,0:T(8,128)(2,1)} %param.28) | copy-start | bytes 786436
  103.8 76.1 %copy-start.8 = (bf16[256,256]{1,0:T(8,128)(2,1)S(1)}, bf16[256,256]{1,0:T(8,128)(2,1)}, u32[]{:S(2)}) copy-start(bf16[256,256]{1,0:T(8,128)(2,1)} %branch.1) | copy-start | bytes 393220
  103.9 76.1 %copy-start.9 = (bf16[256,256]{1,0:T(8,128)(2,1)S(1)}, bf16[256,256]{1,0:T(8,128)(2,1)}, u32[]{:S(2)}) copy-start(bf16[256,256]{1,0:T(8,128)(2,1)} %conv.1) | copy-start | bytes 393220
  178.5 1.3 copy-start.3

commit v4 on v3

--- a/solution.py
+++ b/solution.py
@@ -19,10 +19,9 @@
 TOK = 256
 QW = 1024
 FFQ = 256
-CHUNKS = 4
+CHUNKS = 8
 SP = "sp"
 CW = QW // CHUNKS
-HALF = 320
 rate_scale = 8.0
 norm_eps = 1e-06
 
@@ -37,17 +36,36 @@
     )
 
 
-def prep_kernel(stream, out_grad, gain, routes, weight, send, combine, qi, qc0, qc1, scale):
+def prep_kernel(
+    stream, out_grad, gain, routes, weight, send, combine,
+    v_stream, v_out, qi, qc0, qc1, scale, load_sem,
+):
     h = pl.program_id(0)
     low = lax.axis_index("tp") % 2
+    cols = pl.ds(pl.multiple_of((2 * h + low) * QW, QW), QW)
+
+    def load_stream():
+        return pltpu.make_async_copy(stream, v_stream, load_sem.at[0])
+
+    def load_out(half):
+        part = pl.ds(pl.multiple_of((2 * half + low) * QW, QW), QW)
+        return pltpu.make_async_copy(out_grad.at[:, part], v_out.at[half], load_sem.at[1 + half])
+
+    diagonal = lax.broadcasted_iota(I32, (TOK, TOK), 0) == lax.broadcasted_iota(
+        I32, (TOK, TOK), 1
+    )
+
+    def column(row):
+        return jnp.sum(jnp.where(diagonal, row.astype(F32), 0.0), axis=1, keepdims=True)
 
     @pl.when(h == 0)
     def _():
-        wide = stream[...].astype(F32)
-        mean = jnp.sum(wide * wide, axis=1, keepdims=True) * (1.0 / (TPN * QW))
-        scale[...] = jnp.broadcast_to(lax.rsqrt(mean + norm_eps), (TOK, 128))
+        load_stream().start()
+        load_out(0).start()
+        load_out(1).start()
         lanes = lax.broadcasted_iota(I32, (TOK, 128), 1)
-        r0, r1 = routes[:, 0:1], routes[:, 1:2]
+        r0 = column(routes[0:1, :]).astype(I32)
+        r1 = column(routes[1:2, :]).astype(I32)
         hot0 = (r0 == lanes).astype(F32)
         hot1 = (r1 == lanes).astype(F32)
         before = (
@@ -63,21 +81,29 @@
             mixed = 512 + route * 8 + (rank - 16)
             of_input = jnp.where(rank < 16, pure, mixed + 4 * upper)
             of_cotan = jnp.where(rank < 16, pure, mixed + 4 * (1 - upper))
-            return (slots == of_input).astype(F32), (slots == of_cotan).astype(F32)
-
-        in0, cot0 = places(r0, hot0)
-        in1, cot1 = places(r1, hot1)
-        both = (in0 + in1).astype(BF)
-        qi[...] = both
-        combine[...] = both
+            of_return = route * 24 + rank + jnp.where(rank < 16, 0, 4 * upper)
+            return tuple(
+                (slots == place).astype(F32) for place in (of_input, of_cotan, of_return)
+            )
+
+        in0, cot0, ret0 = places(r0, hot0)
+        in1, cot1, ret1 = places(r1, hot1)
+        qi[...] = (in0 + in1).astype(BF)
+        combine[...] = (ret0 + ret1).astype(BF)
         qc0[...] = cot0.astype(BF)
         qc1[...] = cot1.astype(BF)
-
-    cols = pl.ds(pl.multiple_of((2 * h + low) * QW, QW), QW)
-    normed = (stream[:, cols].astype(F32) * scale[:, 0:1] * gain[:, cols].astype(F32)).astype(BF)
-    grad = out_grad[:, cols].astype(F32)
-    scaled0 = (weight[:, 0:1] * grad).astype(BF)
-    scaled1 = (weight[:, 1:2] * grad).astype(BF)
+        load_stream().wait()
+        wide = v_stream[...].astype(F32)
+        mean = jnp.sum(wide * wide, axis=1, keepdims=True) * (1.0 / (TPN * QW))
+        scale[...] = jnp.broadcast_to(lax.rsqrt(mean + norm_eps), (TOK, 128))
+
+    load_out(h).wait()
+    normed = (
+        v_stream[:, cols].astype(F32) * scale[:, 0:1] * gain[:, cols].astype(F32)
+    ).astype(BF)
+    grad = v_out[h].astype(F32)
+    scaled0 = (column(weight[0:1, :]) * grad).astype(BF)
+    scaled1 = (column(weight[1:2, :]) * grad).astype(BF)
     for plane in range(3):
         span = slice(plane * 256, plane * 256 + 256)
         rows_in = contract(qi[:, span], normed, 0, 0)
@@ -94,13 +120,7 @@
     return pl.pallas_call(
         prep_kernel,
         grid=(2,),
-        in_specs=[
-            whole((TOK, 4 * QW)),
-            whole((TOK, 4 * QW)),
-            whole((1, 4 * QW)),
-            whole((TOK, 2)),
-            whole((TOK, 2)),
-        ],
+        in_specs=[ANY, ANY, whole((1, 4 * QW)), whole((2, TOK)), whole((2, TOK))],
         out_specs=[
             pl.BlockSpec((1, 5, 256, QW), lambda h: (h, 0, 0, 0)),
             whole((TOK, 768)),
@@ -110,10 +130,13 @@
             jax.ShapeDtypeStruct((TOK, 768), BF),
         ],
         scratch_shapes=[
+            pltpu.VMEM((TOK, 4 * QW), BF),
+            pltpu.VMEM((2, TOK, QW), BF),
             pltpu.VMEM((TOK, 768), BF),
             pltpu.VMEM((TOK, 768), BF),
             pltpu.VMEM((TOK, 768), BF),
             pltpu.VMEM((TOK, 128), F32),
+            pltpu.SemaphoreType.DMA((3,)),
         ],
         compiler_params=pltpu.CompilerParams(vmem_limit_bytes=48 * 1024 * 1024),
         name="prep",
@@ -317,9 +340,11 @@
         return pltpu.make_async_copy(vpart.at[q], part.at[q], part_sem.at[q])
 
     def back(q):
-        vpart[q] = (
+        rows = (
             contract(gu[:, 0:FFQ], vg[q], 1, 1) + contract(gu[:, FFQ : 2 * FFQ], vu[q], 1, 1)
         ).astype(BF)
+        for c in range(CHUNKS):
+            vpart[q, c] = rows[:, c * CW : (c + 1) * CW]
         part_out(q).start()
 
     loop(0, TPN, back)
@@ -352,7 +377,7 @@
         in_specs=[ANY] * 4,
         out_specs=[ANY] * 4,
         out_shape=[
-            jax.ShapeDtypeStruct((TPN, 640, QW), BF),
+            jax.ShapeDtypeStruct((TPN, CHUNKS, 640, CW), BF),
             jax.ShapeDtypeStruct((full, FFQ), BF),
             jax.ShapeDtypeStruct((full, FFQ), BF),
             jax.ShapeDtypeStruct((FFQ, full), BF),
@@ -364,7 +389,7 @@
             pltpu.VMEM((TPN, QW, FFQ), BF),
             pltpu.VMEM((TPN, QW, FFQ), BF),
             pltpu.VMEM((TPN, FFQ, QW), BF),
-            pltpu.VMEM((TPN, 640, QW), BF),
+            pltpu.VMEM((TPN, CHUNKS, 640, CW), BF),
             pltpu.VMEM((2, TPN, QW, FFQ), BF),
             pltpu.VMEM((TPN, FFQ, QW), BF),
             pltpu.VMEM((640, FFQ), F32),
@@ -383,121 +408,96 @@
 
 
 def back_kernel(
-    part, combine, grad, far, near, relay, final, back,
-    far_send, far_recv, near_send, near_recv, own_sem, ret_send, ret_recv, all_send, all_recv,
+    part, combine, grad, near, final, back, held, give, second,
+    near_send, near_recv, own_sem, ret_send, ret_recv, two_send, two_recv, all_send, all_recv,
 ):
     s = lax.axis_index("sp")
     x = lax.axis_index("tp")
-    right, left, across = (lax.rem(x + k, TPN) for k in (1, 3, 2))
+    right, left = lax.rem(x + 1, TPN), lax.rem(x + 3, TPN)
     greet(s, x)
 
-    def rows(i):
-        return pl.ds(pl.multiple_of(i * 8, 8), 8)
-
-    def cols(c):
-        return pl.ds(pl.multiple_of(c * CW, CW), CW)
-
-    def half(side):
-        return pl.ds(side * HALF, HALF)
-
-    def to_far(c, side):
+    def partners(c):
+        odd = lax.rem(c, 2)
+        one = x + 1 - 2 * lax.rem(x, 2)
+        other = TPN - 1 - x
+        return one + odd * (other - one), other + odd * (one - other)
+
+    def to_pair(c, j):
+        pair, _ = partners(c)
+        quarter = pair if j == 0 else lax.rem(x + 2, TPN)
         return remote(
-            part.at[across, half(side), cols(c)],
-            far.at[side, c],
-            far_send.at[side, c],
-            far_recv.at[side, c],
-            (s, (right, left)[side]),
-        )
-
-    def to_near_plain(c, side):
-        return remote(
-            part.at[(right, left)[side], half(1 - side), cols(c)],
-            near.at[side, c, half(1 - side), :],
-            near_send.at[side, 0, c],
-            near_recv.at[side, 0, c],
-            (s, (right, left)[side]),
-        )
-
-    def to_near_sum(c, side):
-        return remote(
-            relay.at[side, c],
-            near.at[side, c, half(side), :],
-            near_send.at[side, 1, c],
-            near_recv.at[side, 1, c],
-            (s, (right, left)[side]),
+            part.at[quarter, c],
+            near.at[c, j],
+            near_send.at[c, j],
+            near_recv.at[c, j],
+            (s, pair),
         )
 
     def own_back(c):
-        return pltpu.make_async_copy(
-            final.at[c, :, rows(s), :], back.at[c, :, rows(s), :], own_sem.at[c]
-        )
+        return pltpu.make_async_copy(final.at[c, s], back.at[c, s], own_sem.at[c])
 
     def home(c, k, target):
         return remote(
-            final.at[c, :, rows(target), :],
-            back.at[c, :, rows(s), :],
-            ret_send.at[c, k],
-            ret_recv.at[c, k],
-            (target, x),
-        )
+            final.at[c, target], back.at[c, s], ret_send.at[c, k], ret_recv.at[c, k], (target, x)
+        )
+
+    def to_other(c):
+        _, other = partners(c)
+        return remote(give.at[c], second.at[c], two_send.at[c], two_recv.at[c], (s, other))
 
     def spread(c, side):
-        src = grad.at[x, :, cols(c)]
+        src = grad.at[x, c]
         return remote(
             src, src, all_send.at[side, 0, c], all_recv.at[side, 0, c], (s, (right, left)[side])
         )
 
     def spread_on(c, side):
-        src = grad.at[(left, right)[side], pl.ds(side * 128, 128), cols(c)]
+        src = grad.at[(left, right)[side], c, pl.ds(side * 128, 128), :]
         return remote(
             src, src, all_send.at[side, 1, c], all_recv.at[side, 1, c], (s, (right, left)[side])
         )
+
+    def begin(c):
+        for j in range(2):
+            to_pair(c, j).start()
+
+    loop(0, CHUNKS, begin)
 
     def stage(t):
         @pl.when(t < CHUNKS)
         def _():
-            for side in range(2):
-                to_far(t, side).start()
-                to_near_plain(t, side).start()
-
-        c1 = t - 1
-
-        @pl.when((c1 >= 0) & (c1 < CHUNKS))
-        def _():
-            for side in range(2):
-                to_far(c1, side).wait_recv()
-                mine = part[(right, left)[side], pl.ds(side * HALF, HALF), cols(c1)]
-                relay[side, c1] = (far[side, c1].astype(F32) + mine.astype(F32)).astype(BF)
-                to_near_sum(c1, side).start()
+            _, other = partners(t)
+            for j in range(2):
+                to_pair(t, j).wait_recv()
+                mine = part[x if j == 0 else other, t]
+                total = (mine.astype(F32) + near[t, j].astype(F32)).astype(BF)
+                lanes = slice(j * CW, (j + 1) * CW)
+                final[t, :, 0:8, lanes] = total[0:256].reshape(32, 8, CW)
+                final[t, :, 8:16, lanes] = total[256:512].reshape(32, 8, CW)
+                mixed = total[512:640].reshape(16, 8, CW)
+                final[t, 0:16, 16:24, lanes] = mixed
+                final[t, 16:32, 16:24, lanes] = mixed
+            own_back(t).start()
+            for k in range(1, SPN):
+                home(t, k, peer(s, k)).start()
 
         c2 = t - 2
 
         @pl.when((c2 >= 0) & (c2 < CHUNKS))
         def _():
-            for side in range(2):
-                to_near_plain(c2, side).wait_recv()
-                to_near_sum(c2, side).wait_recv()
-            total = (
-                part[x, :, cols(c2)].astype(F32)
-                + near[0, c2].astype(F32)
-                + near[1, c2].astype(F32)
-            ).astype(BF)
-            final[c2, 0] = total[0:256]
-            final[c2, 1] = total[256:512]
-            final[c2, 2, 0:128, :] = total[512:640]
-            final[c2, 2, 128:256, :] = total[512:640]
-            own_back(c2).start()
-            for k in range(1, SPN):
-                home(c2, k, peer(s, k)).start()
+            own_back(c2).wait()
+            loop(1, SPN, lambda k: home(c2, k, s ^ 1).wait_recv())
+            summed = contract(combine[...], back[c2].reshape(768, 2 * CW), 1, 0)
+            held[c2] = summed[:, 0:CW]
+            give[c2] = summed[:, CW : 2 * CW].astype(BF)
+            to_other(c2).start()
 
         c3 = t - 3
 
         @pl.when((c3 >= 0) & (c3 < CHUNKS))
         def _():
-            own_back(c3).wait()
-            loop(1, SPN, lambda k: home(c3, k, s ^ 1).wait_recv())
-            summed = contract(combine[...], back[c3].reshape(768, CW), 1, 0)
-            grad[x, :, cols(c3)] = summed.astype(BF)
+            to_other(c3).wait_recv()
+            grad[x, c3] = (held[c3] + second[c3].astype(F32)).astype(BF)
             for side in range(2):
                 spread(c3, side).start()
 
@@ -512,10 +512,10 @@
     loop(0, CHUNKS + 4, stage)
 
     def finish(c):
+        for j in range(2):
+            to_pair(c, j).wait_send()
+        to_other(c).wait_send()
         for side in range(2):
-            to_far(c, side).wait_send()
-            to_near_plain(c, side).wait_send()
-            to_near_sum(c, side).wait_send()
             spread(c, side).wait_send()
             spread_on(c, side).wait_send()
             spread_on(c, side).wait_recv()
@@ -525,26 +525,28 @@
 
 
 def send_back(part, combine):
+    dma = pltpu.SemaphoreType.DMA
     return pl.pallas_call(
         back_kernel,
         in_specs=[VM, VM],
         out_specs=VM,
-        out_shape=jax.ShapeDtypeStruct((TPN, TOK, QW), BF),
+        out_shape=jax.ShapeDtypeStruct((TPN, CHUNKS, TOK, CW), BF),
         scratch_shapes=[
-            pltpu.VMEM((2, CHUNKS, HALF, CW), BF),
-            pltpu.VMEM((2, CHUNKS, 2 * HALF, CW), BF),
-            pltpu.VMEM((2, CHUNKS, HALF, CW), BF),
-            pltpu.VMEM((CHUNKS, 3, 256, CW), BF),
-            pltpu.VMEM((CHUNKS, 3, 256, CW), BF),
-            pltpu.SemaphoreType.DMA((2, CHUNKS)),
-            pltpu.SemaphoreType.DMA((2, CHUNKS)),
-            pltpu.SemaphoreType.DMA((2, 2, CHUNKS)),
-            pltpu.SemaphoreType.DMA((2, 2, CHUNKS)),
-            pltpu.SemaphoreType.DMA((CHUNKS,)),
-            pltpu.SemaphoreType.DMA((CHUNKS, SPN)),
-            pltpu.SemaphoreType.DMA((CHUNKS, SPN)),
-            pltpu.SemaphoreType.DMA((2, 2, CHUNKS)),
-            pltpu.SemaphoreType.DMA((2, 2, CHUNKS)),
+            pltpu.VMEM((CHUNKS, 2, 640, CW), BF),
+            pltpu.VMEM((CHUNKS, SPN, 24, 2 * CW), BF),
+            pltpu.VMEM((CHUNKS, SPN, 24, 2 * CW), BF),
+            pltpu.VMEM((CHUNKS, TOK, CW), F32),
+            pltpu.VMEM((CHUNKS, TOK, CW), BF),
+            pltpu.VMEM((CHUNKS, TOK, CW), BF),
+            dma((CHUNKS, 2)),
+            dma((CHUNKS, 2)),
+            dma((CHUNKS,)),
+            dma((CHUNKS, SPN)),
+            dma((CHUNKS, SPN)),
+            dma((CHUNKS,)),
+            dma((CHUNKS,)),
+            dma((2, 2, CHUNKS)),
+            dma((2, 2, CHUNKS)),
         ],
         compiler_params=pltpu.CompilerParams(
             collective_id=1, has_side_effects=True, vmem_limit_bytes=48 * 1024 * 1024
@@ -579,7 +581,7 @@
 def mixer_kernel(
     stream, out_grad, gain, grad, states, branch, out_proj, conv, decay_map, input_map, base, shift,
     branch_grad, conv_grad, proj_grad,
-    v_stream, v_out, v_grad, v_proj, v_states, v_shift, v_branch, v_conv, v_decay, v_input,
+    v_stream, v_out, v_proj, v_states, v_shift, v_branch, v_conv, v_decay, v_input,
     sgb, dot, scale, lru, pulled, linear, coeffs,
     ends, edges, pieces, pair, paired, far_y, far_z, sum_y, sum_z, last_y, last_z,
     big_sem, small_sem, end_send, end_recv, pair_send, pair_recv, one_send, one_recv,
@@ -594,7 +596,6 @@
         cols = pl.ds(pl.multiple_of(q * QW, QW), QW)
         src, dst = (
             (stream.at[:, cols], v_stream.at[q]),
-            (grad.at[q], v_grad.at[q]),
             (out_grad.at[:, cols], v_out.at[q]),
             (out_proj.at[cols, :], v_proj.at[q]),
         )[which]
@@ -617,7 +618,7 @@
         copy.start()
 
     def begin(q):
-        for which in range(4):
+        for which in range(3):
             big(which, q).start()
 
     loop(0, TPN, begin)
@@ -646,12 +647,14 @@
         )
         linear[d, 2] = width * c * i * (1.0 - i)
 
+    def grad_of(q):
+        return jnp.concatenate([grad[q, c] for c in range(CHUNKS)], axis=1).astype(F32)
+
     def squares(q, carry):
         big(0, q).wait()
-        big(1, q).wait()
         v = v_stream[q].astype(F32)
         g = gain[:, pl.ds(pl.multiple_of(q * QW, QW), QW)].astype(F32)
-        w = v * (g * v_grad[q].astype(F32))
+        w = v * (g * grad_of(q))
         return (
             carry[0] + jnp.sum(v * v, axis=1, keepdims=True),
             carry[1] + jnp.sum(w, axis=1, keepdims=True),
@@ -666,11 +669,11 @@
     pulled[...] = jnp.zeros_like(pulled)
 
     def rows_grad(q):
+        big(1, q).wait()
         big(2, q).wait()
-        big(3, q).wait()
         r = scale[:, 0:1]
         unit = v_stream[q].astype(F32) * r
-        scaled = gain[:, pl.ds(pl.multiple_of(q * QW, QW), QW)].astype(F32) * v_grad[q].astype(F32)
+        scaled = gain[:, pl.ds(pl.multiple_of(q * QW, QW), QW)].astype(F32) * grad_of(q)
         v = (v_out[q].astype(F32) + r * (scaled - unit * dot[:, 0:1])).astype(BF)
         sgb[q] = v
         pulled[...] += contract(v, v_proj[q], 1, 0)
@@ -688,6 +691,23 @@
     lru[...] = (total * gelu).astype(BF)
     branch_grad[...] = lru_grad * total * slope
     state_grad = lru_grad * gelu
+    def pair_to(q):
+        return remote(
+            pieces.at[q, :, 1 - core],
+            pair.at[q],
+            pair_send.at[q],
+            pair_recv.at[q],
+            (s + 1 - 2 * core, x),
+        )
+
+    def proj(q):
+        pieces[q] = (
+            contract(sgb[q], lru[...], 0, 0).astype(BF).reshape(TPN, 2, 128, FFQ)
+        )
+        pair_to(q).start()
+
+    met()
+    loop(0, TPN, proj)
     for d in range(2):
         reach, inner = scan_rows(coeffs[d], state_grad, d == 0)
         edge = slice(0, 1) if d == 0 else slice(TOK - 1, TOK)
@@ -700,27 +720,10 @@
     def ends_to(k, target):
         return remote(ends, edges.at[s], end_send.at[k], end_recv.at[k], (target, x))
 
-    met()
     for k in range(1, SPN):
         ends_to(k, peer(s, k)).start()
     edges[s] = ends[...]
 
-    def pair_to(q):
-        return remote(
-            pieces.at[q, :, 1 - core],
-            pair.at[q],
-            pair_send.at[q],
-            pair_recv.at[q],
-            (s + 1 - 2 * core, x),
-        )
-
-    def proj(q):
-        pieces[q] = (
-            contract(sgb[q], lru[...], 0, 0).astype(BF).reshape(TPN, 2, 128, FFQ)
-        )
-        pair_to(q).start()
-
-    loop(0, TPN, proj)
 
     def meet(q):
         pair_to(q).wait_recv()
@@ -814,7 +817,7 @@
     dma = pltpu.SemaphoreType.DMA
     return pl.pallas_call(
         mixer_kernel,
-        in_specs=[ANY, ANY, VM, ANY, ANY, ANY, ANY, ANY, ANY, ANY, VM, ANY],
+        in_specs=[ANY, ANY, VM, VM, ANY, ANY, ANY, ANY, ANY, ANY, VM, ANY],
         out_specs=[VM] * 3,
         out_shape=[
             jax.ShapeDtypeStruct(square, F32),
@@ -822,7 +825,6 @@
             jax.ShapeDtypeStruct((128, FFQ), F32),
         ],
         scratch_shapes=[
-            pltpu.VMEM(whole, BF),
             pltpu.VMEM(whole, BF),
             pltpu.VMEM(whole, BF),
             pltpu.VMEM((TPN, QW, FFQ), BF),
@@ -850,7 +852,7 @@
             pltpu.VMEM((4, 64, FFQ), BF),
             pltpu.VMEM((3, 64, FFQ), BF),
             pltpu.VMEM((3, 64, FFQ), BF),
-            dma((4, TPN)),
+            dma((3, TPN)),
             dma((6,)),
             dma((SPN,)),
             dma((SPN,)),
@@ -886,7 +888,7 @@
     decay_shift,
     states,
 ):
-    send, combine = prep(stream, out_grad, norm_gain[None, :], routes, route_weight)
+    send, combine = prep(stream, out_grad, norm_gain[None, :], routes.T, route_weight.T)
     got = dispatch(send)
     part, gate_wgrad, up_wgrad, down_wgrad = expert(
         got, gate_weight[0], up_weight[0], down_weight[0]

time: 207 us -> 210 us (1.014)
  Pallas kernels: 197 us -> 200 us
    pallas_call x2, Pallas kernels: 30.3 us -> 32.5 us  [the longest x1 25.9 us: mixer(): pl.pallas_call(mixer_kernel, in_specs=[ANY, ANY, VM, VM, ANY, ANY, ANY, A...]
    unnamed x27 -> x29, local copies, waits for them, and re-layouts: 8.23 us -> 7.98 us
where the time goes in v4:
time: 210 us; the launch traced here: 209 us
  Pallas kernels  200 us (95%)
  local copies, waits for them, and re-layouts  8.69 us (4%)
    pallas_call x1, Pallas kernels, send_back(): pl.pallas_call(back_kernel, in_specs=[VM, VM], out_specs=VM, out_shape=ja...  75.5 us
    pallas_call x1, Pallas kernels, dispatch(): pl.pallas_call(dispatch_kernel, in_specs=[ANY], out_specs=ANY, out_shape=...  73.8 us
    pallas_call x1, Pallas kernels, mixer(): pl.pallas_call(mixer_kernel, in_specs=[ANY, ANY, VM, VM, ANY, ANY, ANY, A...  25.9 us
    pallas_call x1, Pallas kernels, expert(): pl.pallas_call(expert_kernel, in_specs=[ANY] * 4, out_specs=[ANY] * 4, ou...  18.1 us
    unnamed x29, local copies, waits for them, and re-layouts  7.98 us
    pallas_call x1, Pallas kernels, prep(): pl.pallas_call(prep_kernel, grid=(2,), in_specs=[ANY, ANY, whole((1, 4 *...  6.55 us

profile of v4, /device:TPU:1, one launch (start us, length us, event | category | flops | bytes accessed | tf_op | source)
XLA Modules:
  0.0 209.4 jit_solution(12026348149670409941)
XLA Ops:
  0.6 0.7 broadcast_in_dim.13.gain
  1.3 0.0 copy-start
  1.4 1.6 copy-done
  2.9 1.6 copy-done.2
  4.5 0.7 copy-done.10
  5.2 0.7 copy-done.11
  5.9 6.6 %prep.1 = (bf16[2,5,256,1024]{3,2,1,0:T(8,128)(2,1)}, bf16[256,768]{1,0:T(8,128)(2,1)S(1)}) custom-call(bf16[256,4096]{1,0:T(8,128)(2,1)S(1)} %copy-done, bf16[256,4096]{1,0:T(8,128)(2,1)S(1)} %copy-done.2, bf16[1,4096]{1,0:T(2,128)(2,1)S(1)} %broadcast_in_dim.13.gain, s32[2,256]{1,0:T(2,128)S(1)} %bitcast.12, f32[2,256]{1,0:T(2,128)S(1)} %bitcast.13), custom_call_target="tpu_custom_call" | custom-call | tf_op jit(solution)/shard_map/prep/pallas_call | solution.py:120
  12.5 73.8 %dispatch.1.got = bf16[2,2,5,256,1024]{4,3,2,1,0:T(8,128)(2,1)} custom-call(bf16[2,5,256,1024]{3,2,1,0:T(8,128)(2,1)} %get-tuple-element.15.send), custom_call_target="tpu_custom_call" | custom-call | tf_op jit(solution)/shard_map/dispatch/pallas_call | solution.py:264
  86.3 18.1 %expert.1 = (bf16[4,8,640,128]{3,2,1,0:T(8,128)(2,1)}, bf16[4096,256]{1,0:T(8,128)(2,1)}, bf16[4096,256]{1,0:T(8,128)(2,1)}, bf16[256,4096]{1,0:T(8,128)(2,1)}) custom-call(bf16[2,2,5,256,1024]{4,3,2,1,0:T(8,128)(2,1)} %dispatch.1.got, bf16[4096,256]{1,0:T(8,128)(2,1)} %bitcast.14, bf16[4096,256]{1,0:T(8,128)(2,1)} %bitcast.15, bf16[256,4096]{1,0:T(8,128)(2,1)} %bitcast.16), custom_call_target="tpu_custom_call" | custom-call | tf_op jit(solution)/shard_map/expert/pallas_call | solution.py:375
  104.3 0.0 copy-start.12
  104.4 0.0 copy-start.1
  104.4 0.0 copy-start.4
  104.4 0.0 copy-start.5
  104.4 0.0 copy-start.6
  104.4 0.0 copy-start.7
  104.4 0.0 copy-start.8
  104.4 0.0 copy-start.9
  104.4 75.5 %send_back.1.grad = bf16[4,8,256,128]{3,2,1,0:T(8,128)(2,1)S(1)} custom-call(bf16[4,8,640,128]{3,2,1,0:T(8,128)(2,1)} %get-tuple-element.16.part, bf16[256,768]{1,0:T(8,128)(2,1)S(1)} %get-tuple-element.17.combine), custom_call_target="tpu_custom_call" | custom-call | tf_op jit(solution)/shard_map/send_back/pallas_call | solution.py:529
  180.0 1.3 copy-done.3
  181.3 0.0 copy-done.1
  181.4 25.9 %mixer.1 = (f32[256,256]{1,0:T(8,128)S(1)}, f32[256,256]{1,0:T(8,128)S(1)}, f32[128,256]{1,0:T(8,128)S(1)}) custom-call(bf16[256,4096]{1,0:T(8,128)(2,1)S(1)} %copy-done.1, bf16[256,4096]{1,0:T(8,128)(2,1)} %out_grad.3, bf16[1,4096]{1,0:T(2,128)(2,1)S(1)} %broadcast_in_dim.13.gain, bf16[4,8,256,128]{3,2,1,0:T(8,128)(2,1)} %copy-done.3, ...), custom_call_target="tpu_custom_call" | custom-call | tf_op jit(solution)/shard_map/mixer/pallas_call | solution.py:818
  207.3 0.7 copy.25
  208.0 0.7 copy.26
  208.7 0.7 copy.27
  (12 shorter events, 0.0 us)
Async XLA Ops:
  1.3 1.6 copy-start
  2.9 1.6 copy-start.2
  4.5 0.7 copy-start.10
  5.2 0.7 copy-start.11
  104.3 77.0 %copy-start.12 = (f32[2,256]{1,0:T(2,128)S(1)}, f32[2,256]{1,0:T(2,128)}, u32[]{:S(2)}) copy-start(f32[2,256]{1,0:T(2,128)} %param.29) | copy-start | bytes 6148
  104.4 77.0 %copy-start.1 = (bf16[256,4096]{1,0:T(8,128)(2,1)S(1)}, bf16[256,4096]{1,0:T(8,128)(2,1)}, u32[]{:S(2)}) copy-start(bf16[256,4096]{1,0:T(8,128)(2,1)} %stream.3) | copy-start | bytes 6291460
  104.4 77.0 %copy-start.4 = (f32[2,256,256]{2,1,0:T(8,128)S(1)}, f32[2,256,256]{2,1,0:T(8,128)}, u32[]{:S(2)}) copy-start(f32[2,256,256]{2,1,0:T(8,128)} %states.1) | copy-start | bytes 1572868
  104.4 77.0 %copy-start.5 = (f32[2,256,256]{2,1,0:T(8,128)S(1)}, f32[2,256,256]{2,1,0:T(8,128)}, u32[]{:S(2)}) copy-start(f32[2,256,256]{2,1,0:T(8,128)} %shift.1) | copy-start | bytes 1572868
  104.4 77.0 %copy-start.6 = (bf16[2,1,256,256]{3,2,1,0:T(8,128)(2,1)S(1)}, bf16[2,1,256,256]{3,2,1,0:T(8,128)(2,1)}, u32[]{:S(2)}) copy-start(bf16[2,1,256,256]{3,2,1,0:T(8,128)(2,1)} %param.27) | copy-start | bytes 786436
  104.4 77.0 %copy-start.7 = (bf16[2,1,256,256]{3,2,1,0:T(8,128)(2,1)S(1)}, bf16[2,1,256,256]{3,2,1,0:T(8,128)(2,1)}, u32[]{:S(2)}) copy-start(bf16[2,1,256,256]{3,2,1,0:T(8,128)(2,1)} %param.28) | copy-start | bytes 786436
  104.4 77.0 %copy-start.8 = (bf16[256,256]{1,0:T(8,128)(2,1)S(1)}, bf16[256,256]{1,0:T(8,128)(2,1)}, u32[]{:S(2)}) copy-start(bf16[256,256]{1,0:T(8,128)(2,1)} %branch.1) | copy-start | bytes 393220
  104.4 77.0 %copy-start.9 = (bf16[256,256]{1,0:T(8,128)(2,1)S(1)}, bf16[256,256]{1,0:T(8,128)(2,1)}, u32[]{:S(2)}) copy-start(bf16[256,256]{1,0:T(8,128)(2,1)} %conv.1) | copy-start | bytes 393220
  180.0 1.3 copy-start.3

commit v5 on v4

v5 whole, which is shorter than its diff:
```python
import functools

import jax
import jax.numpy as jnp
from jax import lax
from jax.experimental import pallas as pl
from jax.experimental.pallas import tpu as pltpu
from jax.sharding import PartitionSpec as P

BF = jnp.bfloat16
F32 = jnp.float32
I32 = jnp.int32
MESH = pl.DeviceIdType.MESH
ANY = pl.BlockSpec(memory_space=pl.ANY)
VM = pl.BlockSpec(memory_space=pltpu.VMEM)

SPN = 32
TPN = 4
TOK = 256
QW = 1024
FFQ = 256
CHUNKS = 8
SP = "sp"
CW = QW // CHUNKS
rate_scale = 8.0
norm_eps = 1e-06


def contract(left, right, left_dim, right_dim, precision=None):
    return lax.dot_general(
        left,
        right,
        (((left_dim,), (right_dim,)), ((), ())),
        preferred_element_type=F32,
        precision=precision,
    )


NEAR = (
    (0, 1), (1, 0), (0, 3), (3, 0), (1, 1), (3, 3), (1, 3), (3, 1),
    (0, 2), (2, 0), (1, 2), (2, 1), (3, 2), (2, 3), (2, 2),
)
STEPS = ((0, 0, 1),) + tuple((z, y, c) for c in (0, 1) for z, y in NEAR)


def peer(s, k, sign=1):
    z, y, c = STEPS[k - 1]
    return (
        lax.rem(s // 8 + (z if sign > 0 else 4 - z), 4) * 8
        + lax.rem((s // 2) % 4 + (y if sign > 0 else 4 - y), 4) * 2
        + lax.rem(s % 2 + c, 2)
    )


def greet(s, x):
    hello_all(s, x)
    met()


def met():
    pl.semaphore_wait(pltpu.get_barrier_semaphore(), SPN + 1)


def hello_all(s, x):
    barrier = pltpu.get_barrier_semaphore()

    def hello(d, carry):
        pl.semaphore_signal(barrier, inc=1, device_id=(s ^ d, x), device_id_type=MESH)
        return carry

    lax.fori_loop(1, SPN, hello, 0)
    for step in (1, TPN - 1):
        pl.semaphore_signal(
            barrier, inc=1, device_id=(s, lax.rem(x + step, TPN)), device_id_type=MESH
        )


def remote(src, dst, send_sem, recv_sem, target):
    return pltpu.make_async_remote_copy(
        src_ref=src,
        dst_ref=dst,
        send_sem=send_sem,
        recv_sem=recv_sem,
        device_id=target,
        device_id_type=MESH,
    )


def loop(lower, upper, step):
    def run(d, carry):
        step(d)
        return carry

    lax.fori_loop(lower, upper, run, 0)


def dispatch_kernel(
    stream, out_grad, gain, routes, weight, got, combine,
    send, v_stream, v_out, qi, qc0, qc1, scale,
    load_sem, own_sem, send_sem, recv_sem, fwd_send, fwd_recv,
):
    s = lax.axis_index("sp")
    x = lax.axis_index("tp")
    high, low = x // 2, x % 2
    right, left = lax.rem(x + 1, TPN), lax.rem(x + TPN - 1, TPN)
    hello_all(s, x)

    def columns(h):
        return pl.ds(pl.multiple_of((2 * h + low) * QW, QW), QW)

    def load(h):
        return pltpu.make_async_copy(out_grad.at[:, columns(h)], v_out.at[h], load_sem.at[1 + h])

    whole = pltpu.make_async_copy(stream, v_stream, load_sem.at[0])
    whole.start()
    load(high).start()
    load(1 - high).start()
    diagonal = lax.broadcasted_iota(I32, (TOK, TOK), 0) == lax.broadcasted_iota(
        I32, (TOK, TOK), 1
    )

    def column(row):
        return jnp.sum(jnp.where(diagonal, row.astype(F32), 0.0), axis=1, keepdims=True)

    lanes = lax.broadcasted_iota(I32, (TOK, 128), 1)
    r0 = column(routes[0:1, :]).astype(I32)
    r1 = column(routes[1:2, :]).astype(I32)
    w0, w1 = column(weight[0:1, :]), column(weight[1:2, :])
    hot0 = (r0 == lanes).astype(F32)
    hot1 = (r1 == lanes).astype(F32)
    before = (
        lax.broadcasted_iota(I32, (TOK, TOK), 1) < lax.broadcasted_iota(I32, (TOK, TOK), 0)
    ).astype(F32)
    counts = contract(before.astype(BF), (hot0 + hot1).astype(BF), 1, 0)
    upper = s // 16
    slots = lax.broadcasted_iota(I32, (TOK, 768), 1)

    def places(route, hot):
        rank = jnp.sum(counts * hot, axis=1, keepdims=True).astype(I32)
        pure = (rank // 8) * 256 + route * 8 + rank % 8
        mixed = 512 + route * 8 + (rank - 16)
        of_input = jnp.where(rank < 16, pure, mixed + 4 * upper)
        of_cotan = jnp.where(rank < 16, pure, mixed + 4 * (1 - upper))
        of_return = route * 24 + rank + jnp.where(rank < 16, 0, 4 * upper)
        return tuple((slots == place).astype(F32) for place in (of_input, of_cotan, of_return))

    in0, cot0, ret0 = places(r0, hot0)
    in1, cot1, ret1 = places(r1, hot1)
    qi[...] = (in0 + in1).astype(BF)
    combine[...] = (ret0 + ret1).astype(BF)
    qc0[...] = cot0.astype(BF)
    qc1[...] = cot1.astype(BF)
    whole.wait()
    wide = v_stream[...].astype(F32)
    mean = jnp.sum(wide * wide, axis=1, keepdims=True) * (1.0 / (TPN * QW))
    scale[...] = jnp.broadcast_to(lax.rsqrt(mean + norm_eps), (TOK, 128))

    def gather_rows(h):
        load(h).wait()
        cols = columns(h)
        normed = (
            v_stream[:, cols].astype(F32) * scale[:, 0:1] * gain[:, cols].astype(F32)
        ).astype(BF)
        grad = v_out[h].astype(F32)
        scaled0 = (w0 * grad).astype(BF)
        scaled1 = (w1 * grad).astype(BF)
        for plane in range(3):
            span = slice(plane * 256, plane * 256 + 256)
            rows_in = contract(qi[:, span], normed, 0, 0)
            rows_cot = contract(qc0[:, span], scaled0, 0, 0) + contract(
                qc1[:, span], scaled1, 0, 0
            )
            if plane < 2:
                send[h, plane] = rows_in.astype(BF)
                send[h, plane + 2] = rows_cot.astype(BF)
            else:
                send[h, 4] = (rows_in + rows_cot).astype(BF)

    def rows(i):
        return pl.ds(pl.multiple_of(i * 8, 8), 8)

    def half(turn):
        return high if turn == 0 else 1 - high

    def over(turn, k, target):
        return remote(
            send.at[half(turn), :, rows(target), :],
            got.at[half(turn), low, :, rows(s), :],
            send_sem.at[turn, k],
            recv_sem.at[turn, k],
            (target, x),
        )

    def own(turn):
        return pltpu.make_async_copy(
            send.at[half(turn), :, rows(s), :],
            got.at[half(turn), low, :, rows(s), :],
            own_sem.at[turn],
        )

    def onward(src, dst, k, side):
        return remote(
            src, dst, fwd_send.at[side, k], fwd_recv.at[side, k], (s, (right, left)[side])
        )

    def block(i):
        return got.at[high, low, :, rows(i), :]

    gather_rows(high)
    met()
    for side in range(2):
        onward(send.at[high, :, rows(s), :], block(s), 0, side).start()
    for turn in range(2):
        if turn == 1:
            gather_rows(1 - high)
        own(turn).start()
        for k in range(1, SPN):
            over(turn, k, peer(s, k)).start()
    for k in range(1, SPN):
        source = peer(s, k, -1)
        over(0, k, source).wait_recv()
        for side in range(2):
            onward(block(source), block(source), k, side).start()
    own(0).wait()
    own(1).wait()

    def finish(k):
        for turn in range(2):
            over(turn, k, s ^ 1).wait_send()
        over(1, k, s ^ 1).wait_recv()

    def finish_onward(k):
        for side in range(2):
            copy = onward(block(s), block(s), k, side)
            copy.wait_send()
            copy.wait_recv()

    loop(1, SPN, finish)
    loop(0, SPN, finish_onward)


def dispatch(stream, out_grad, gain, routes, weight):
    dma = pltpu.SemaphoreType.DMA
    return pl.pallas_call(
        dispatch_kernel,
        in_specs=[ANY, ANY, VM, VM, VM],
        out_specs=[ANY, VM],
        out_shape=[
            jax.ShapeDtypeStruct((2, 2, 5, 256, QW), BF),
            jax.ShapeDtypeStruct((TOK, 768), BF),
        ],
        scratch_shapes=[
            pltpu.VMEM((2, 5, 256, QW), BF),
            pltpu.VMEM((TOK, 4 * QW), BF),
            pltpu.VMEM((2, TOK, QW), BF),
            pltpu.VMEM((TOK, 768), BF),
            pltpu.VMEM((TOK, 768), BF),
            pltpu.VMEM((TOK, 768), BF),
            pltpu.VMEM((TOK, 128), F32),
            dma((3,)),
            dma((2,)),
            dma((2, SPN)),
            dma((2, SPN)),
            dma((2, SPN)),
            dma((2, SPN)),
        ],
        compiler_params=pltpu.CompilerParams(
            collective_id=0, has_side_effects=True, vmem_limit_bytes=62 * 1024 * 1024
        ),
        name="dispatch",
    )(stream, out_grad, gain, routes, weight)


def swap_halves(v):
    tiles = v.reshape(16, 8, v.shape[1])
    return pltpu.roll(tiles, 4, 1).reshape(v.shape)


def expert_kernel(
    got, gate, up, down, part, gate_wg, up_wg, down_wg,
    vin, vcot, vmix, vg, vu, vd, vpart, ogu, od, gp, upre, hg, gu, hid,
    in_sem, w_sem, part_sem, o_sem,
):
    def loads(q):
        hi, lo = q // 2, q % 2
        out = []
        for plane in range(5):
            if plane < 2:
                dst = vin.at[q, pl.ds(plane * 256, 256), :]
            elif plane < 4:
                dst = vcot.at[q, pl.ds((plane - 2) * 256, 256), :]
            else:
                dst = vmix.at[q]
            out.append(pltpu.make_async_copy(got.at[hi, lo, plane], dst, in_sem.at[q, plane]))
        rows = pl.ds(pl.multiple_of(q * QW, QW), QW)
        out.append(pltpu.make_async_copy(gate.at[rows, :], vg.at[q], w_sem.at[0, q]))
        out.append(pltpu.make_async_copy(up.at[rows, :], vu.at[q], w_sem.at[1, q]))
        out.append(pltpu.make_async_copy(down.at[:, rows], vd.at[q], w_sem.at[2, q]))
        return out

    loop(0, TPN, lambda q: [c.start() for c in loads(q)])
    gp[...] = jnp.zeros_like(gp)
    upre[...] = jnp.zeros_like(upre)
    hg[...] = jnp.zeros_like(hg)

    def forward(q):
        for c in loads(q):
            c.wait()
        first = lax.broadcasted_iota(I32, (128, QW), 0) % 8 < 4
        a = vmix[q, 0:128, :].astype(F32)
        b = vmix[q, 128:256, :].astype(F32)
        vin[q, 512:640, :] = jnp.where(first, a, b).astype(BF)
        vcot[q, 512:640, :] = jnp.where(first, b, a).astype(BF)
        rows = vin[q]
        gp[...] += contract(rows, vg[q], 1, 0)
        upre[...] += contract(rows, vu[q], 1, 0)
        hg[...] += contract(vcot[q], vd[q], 1, 1)

    loop(0, TPN, forward)
    hg[512:640, :] = swap_halves(hg[512:640, :])
    gate_pre, up_pre, hidden_grad = gp[...], upre[...], hg[...]
    logistic = jax.nn.sigmoid(gate_pre)
    silu = gate_pre * logistic
    hidden = silu * up_pre
    hid[0:512, :] = hidden[0:512, :].astype(BF)
    hid[512:640, :] = swap_halves(hidden[512:640, :]).astype(BF)
    gu[:, 0:FFQ] = (
        hidden_grad * up_pre * (logistic * (1.0 + gate_pre * (1.0 - logistic)))
    ).astype(BF)
    gu[:, FFQ : 2 * FFQ] = (hidden_grad * silu).astype(BF)

    def part_out(q):
        return pltpu.make_async_copy(vpart.at[q], part.at[q], part_sem.at[q])

    def back(q):
        rows = (
            contract(gu[:, 0:FFQ], vg[q], 1, 1) + contract(gu[:, FFQ : 2 * FFQ], vu[q], 1, 1)
        ).astype(BF)
        for c in range(CHUNKS):
            vpart[q, c] = rows[:, c * CW : (c + 1) * CW]
        part_out(q).start()

    loop(0, TPN, back)

    def grads_out(q):
        rows = pl.ds(pl.multiple_of(q * QW, QW), QW)
        return (
            pltpu.make_async_copy(ogu.at[0, q], gate_wg.at[rows, :], o_sem.at[0, q]),
            pltpu.make_async_copy(ogu.at[1, q], up_wg.at[rows, :], o_sem.at[1, q]),
            pltpu.make_async_copy(od.at[q], down_wg.at[:, rows], o_sem.at[2, q]),
        )

    def weights(q):
        both = contract(vin[q], gu[...], 0, 0)
        ogu[0, q] = both[:, 0:FFQ].astype(BF)
        ogu[1, q] = both[:, FFQ : 2 * FFQ].astype(BF)
        od[q] = contract(hid[...], vcot[q], 0, 0).astype(BF)
        for c in grads_out(q):
            c.start()

    loop(0, TPN, weights)
    loop(0, TPN, lambda q: part_out(q).wait())
    loop(0, TPN, lambda q: [c.wait() for c in grads_out(q)])


def expert(got, gate, up, down):
    full = TPN * QW
    return pl.pallas_call(
        expert_kernel,
        in_specs=[ANY] * 4,
        out_specs=[ANY] * 4,
        out_shape=[
            jax.ShapeDtypeStruct((TPN, CHUNKS, 640, CW), BF),
            jax.ShapeDtypeStruct((full, FFQ), BF),
            jax.ShapeDtypeStruct((full, FFQ), BF),
            jax.ShapeDtypeStruct((FFQ, full), BF),
        ],
        scratch_shapes=[
            pltpu.VMEM((TPN, 640, QW), BF),
            pltpu.VMEM((TPN, 640, QW), BF),
            pltpu.VMEM((TPN, 256, QW), BF),
            pltpu.VMEM((TPN, QW, FFQ), BF),
            pltpu.VMEM((TPN, QW, FFQ), BF),
            pltpu.VMEM((TPN, FFQ, QW), BF),
            pltpu.VMEM((TPN, CHUNKS, 640, CW), BF),
            pltpu.VMEM((2, TPN, QW, FFQ), BF),
            pltpu.VMEM((TPN, FFQ, QW), BF),
            pltpu.VMEM((640, FFQ), F32),
            pltpu.VMEM((640, FFQ), F32),
            pltpu.VMEM((640, FFQ), F32),
            pltpu.VMEM((640, 2 * FFQ), BF),
            pltpu.VMEM((640, FFQ), BF),
            pltpu.SemaphoreType.DMA((TPN, 5)),
            pltpu.SemaphoreType.DMA((3, TPN)),
            pltpu.SemaphoreType.DMA((TPN,)),
            pltpu.SemaphoreType.DMA((3, TPN)),
        ],
        compiler_params=pltpu.CompilerParams(vmem_limit_bytes=60 * 1024 * 1024),
        name="expert",
    )(got, gate, up, down)


def back_steps(
    fill, part, combine, grad, mine, near, final, back, held, give, second,
    near_send, near_recv, own_sem, ret_send, ret_recv, two_send, two_recv, all_send, all_recv, mine_sem,
):
    s = lax.axis_index("sp")
    x = lax.axis_index("tp")
    right, left = lax.rem(x + 1, TPN), lax.rem(x + 3, TPN)

    def partners(c):
        odd = lax.rem(c, 2)
        one = x + 1 - 2 * lax.rem(x, 2)
        other = TPN - 1 - x
        return one + odd * (other - one), other + odd * (one - other)

    def to_pair(c, j):
        pair, _ = partners(c)
        quarter = pair if j == 0 else lax.rem(x + 2, TPN)
        return remote(
            part.at[quarter, c],
            near.at[c, j],
            near_send.at[c, j],
            near_recv.at[c, j],
            (s, pair),
        )

    def load_mine(c, j):
        _, other = partners(c)
        return pltpu.make_async_copy(
            part.at[x if j == 0 else other, c], mine.at[c, j], mine_sem.at[c, j]
        )

    def own_back(c):
        return pltpu.make_async_copy(final.at[c, s], back.at[c, s], own_sem.at[c])

    def home(c, k, target):
        return remote(
            final.at[c, target], back.at[c, s], ret_send.at[c, k], ret_recv.at[c, k], (target, x)
        )

    def to_other(c):
        _, other = partners(c)
        return remote(give.at[c], second.at[c], two_send.at[c], two_recv.at[c], (s, other))

    def spread(c, side):
        src = grad.at[x, c]
        return remote(
            src, src, all_send.at[side, 0, c], all_recv.at[side, 0, c], (s, (right, left)[side])
        )

    def spread_on(c, side):
        src = grad.at[(left, right)[side], c, pl.ds(side * 128, 128), :]
        return remote(
            src, src, all_send.at[side, 1, c], all_recv.at[side, 1, c], (s, (right, left)[side])
        )

    def begin(c):
        for j in range(2):
            to_pair(c, j).start()

    def begin_load(c):
        for j in range(2):
            load_mine(c, j).start()

    met()
    loop(0, CHUNKS, begin)
    loop(0, CHUNKS, begin_load)

    fill()

    def open_chunk(t):
        for j in range(2):
            load_mine(t, j).wait()
            to_pair(t, j).wait_recv()
            total = (mine[t, j].astype(F32) + near[t, j].astype(F32)).astype(BF)
            lanes = slice(j * CW, (j + 1) * CW)
            final[t, :, 0:8, lanes] = total[0:256].reshape(32, 8, CW)
            final[t, :, 8:16, lanes] = total[256:512].reshape(32, 8, CW)
            mixed = total[512:640].reshape(16, 8, CW)
            final[t, 0:16, 16:24, lanes] = mixed
            final[t, 16:32, 16:24, lanes] = mixed
        own_back(t).start()
        for k in range(1, SPN):
            home(t, k, peer(s, k)).start()

    def close_chunk(c):
        own_back(c).wait()
        loop(1, SPN, lambda k: home(c, k, s ^ 1).wait_recv())
        summed = contract(combine[...], back[c].reshape(768, 2 * CW), 1, 0)
        held[c] = summed[:, 0:CW]
        give[c] = summed[:, CW : 2 * CW].astype(BF)
        to_other(c).start()

    def share(c):
        to_other(c).wait_recv()
        grad[x, c] = (held[c] + second[c].astype(F32)).astype(BF)
        for side in range(2):
            spread(c, side).start()

    def share_on(c):
        for side in range(2):
            spread(c, side).wait_recv()
            spread_on(c, side).start()

    lag = 3

    def stage(t):
        open_chunk(t)

        @pl.when(t >= lag)
        def _():
            close_chunk(t - lag)

    loop(0, CHUNKS, stage)
    loop(0, CHUNKS - lag, share)
    loop(CHUNKS - lag, CHUNKS, close_chunk)
    loop(0, CHUNKS - lag, share_on)
    loop(CHUNKS - lag, CHUNKS, share)
    loop(CHUNKS - lag, CHUNKS, share_on)

    def finish(c):
        for j in range(2):
            to_pair(c, j).wait_send()
        to_other(c).wait_send()
        for side in range(2):
            spread(c, side).wait_send()
            spread_on(c, side).wait_send()
            spread_on(c, side).wait_recv()
        loop(1, SPN, lambda k: home(c, k, s ^ 1).wait_send())

    loop(0, CHUNKS, finish)


def expm1_negative(v):
    series = 1.0 + v * (1.0 / 9.0)
    for k in (8, 7, 6, 5, 4, 3, 2):
        series = 1.0 + v * (1.0 / k) * series
    return jnp.where(v > -0.5, v * series, jnp.exp(v) - 1.0)


def scan_rows(coeff, value, reverse):
    rows = lax.broadcasted_iota(I32, coeff.shape, 0)
    for k in (1, 2, 4, 8, 16, 32, 64, 128):
        if reverse:
            inside = rows < TOK - k
            shift = TOK - k
        else:
            inside = rows >= k
            shift = k
        coeff_far = jnp.where(inside, pltpu.roll(coeff, shift, 0), 1.0)
        value_far = jnp.where(inside, pltpu.roll(value, shift, 0), 0.0)
        value = value + coeff * value_far
        coeff = coeff * coeff_far
    return coeff, value


def mixer_steps(
    stream, out_grad, gain, grad, states, branch, out_proj, conv, decay_map, input_map, base, shift,
    branch_grad, conv_grad, proj_grad,
    v_stream, v_out, v_proj, v_states, v_shift, v_branch, v_conv, v_decay, v_input,
    sgb, dot, scale, lru, pulled, linear, coeffs,
    ends, edges, pieces, pair, paired, far_y, far_z, sum_y, sum_z, last_y, last_z,
    big_sem, small_sem, end_send, end_recv, pair_send, pair_recv, one_send, one_recv,
    two_send, two_recv,
):
    s = lax.axis_index("sp")
    x = lax.axis_index("tp")
    z, y, core = s // 8, (s // 2) % 4, s % 2

    def big(which, q):
        cols = pl.ds(pl.multiple_of(q * QW, QW), QW)
        src, dst = (
            (stream.at[:, cols], v_stream.at[q]),
            (out_grad.at[:, cols], v_out.at[q]),
            (out_proj.at[cols, :], v_proj.at[q]),
        )[which]
        return pltpu.make_async_copy(src, dst, big_sem.at[which, q])

    small = [
        pltpu.make_async_copy(src, dst, small_sem.at[k])
        for k, (src, dst) in enumerate(
            (
                (conv, v_conv),
                (decay_map, v_decay),
                (input_map, v_input),
                (shift, v_shift),
                (states, v_states),
                (branch, v_branch),
            )
        )
    ]
    for copy in small:
        copy.start()

    def begin(q):
        for which in range(3):
            big(which, q).start()

    loop(0, TPN, begin)
    def gates():
        for copy in small:
            copy.wait()

        c = v_conv[...].astype(F32)
        rows = lax.broadcasted_iota(I32, (TOK, FFQ), 0)
        for d in range(2):
            r = jax.nn.sigmoid(contract(v_conv[...], v_decay[d], 1, 0))
            i = jax.nn.sigmoid(contract(v_conv[...], v_input[d], 1, 0))
            rate = (-rate_scale) * base[d : d + 1, :]
            log_decay = r * rate + v_shift[d]
            decay = jnp.exp(log_decay)
            width = jnp.sqrt(-expm1_negative(2.0 * log_decay))
            drive = width * i * c
            if d == 0:
                coeffs[d] = jnp.where(rows == TOK - 1, 1.0, pltpu.roll(decay, TOK - 1, 0))
                ends[0:1, :] = decay[0:1]
            else:
                coeffs[d] = jnp.where(rows == 0, 1.0, pltpu.roll(decay, 1, 0))
                ends[2:3, :] = decay[TOK - 1 : TOK]
            linear[d, 0] = width * i
            linear[d, 1] = (
                ((v_states[d] - drive) - i * c * decay * decay / width) * rate * r * (1.0 - r)
            )
            linear[d, 2] = width * c * i * (1.0 - i)

    def rest():
        def grad_of(q):
            return jnp.concatenate([grad[q, c] for c in range(CHUNKS)], axis=1).astype(F32)

        def squares(q, carry):
            big(0, q).wait()
            v = v_stream[q].astype(F32)
            g = gain[:, pl.ds(pl.multiple_of(q * QW, QW), QW)].astype(F32)
            w = v * (g * grad_of(q))
            return (
                carry[0] + jnp.sum(v * v, axis=1, keepdims=True),
                carry[1] + jnp.sum(w, axis=1, keepdims=True),
            )

        zero = jnp.zeros((TOK, 1), F32)
        square, along = lax.fori_loop(0, TPN, squares, (zero, zero))
        inverse = 1.0 / (TPN * QW)
        row_scale = lax.rsqrt(square * inverse + norm_eps)
        scale[...] = jnp.broadcast_to(row_scale, (TOK, 128))
        dot[...] = jnp.broadcast_to(along * row_scale * inverse, (TOK, 128))
        pulled[...] = jnp.zeros_like(pulled)

        def rows_grad(q):
            big(1, q).wait()
            big(2, q).wait()
            r = scale[:, 0:1]
            unit = v_stream[q].astype(F32) * r
            scaled = gain[:, pl.ds(pl.multiple_of(q * QW, QW), QW)].astype(F32) * grad_of(q)
            v = (v_out[q].astype(F32) + r * (scaled - unit * dot[:, 0:1])).astype(BF)
            sgb[q] = v
            pulled[...] += contract(v, v_proj[q], 1, 0)

        loop(0, TPN, rows_grad)
        lru_grad = pulled[...]
        total = v_states[0] + v_states[1]
        b = v_branch[...].astype(F32)
        root = 0.7978845608028654
        tanh = jnp.tanh(root * (b + 0.044715 * b * b * b))
        gelu = 0.5 * b * (1.0 + tanh)
        slope = 0.5 * (1.0 + tanh) + 0.5 * b * (1.0 - tanh * tanh) * root * (
            1.0 + 3.0 * 0.044715 * b * b
        )
        lru[...] = (total * gelu).astype(BF)
        branch_grad[...] = lru_grad * total * slope
        state_grad = lru_grad * gelu
        def pair_to(q):
            return remote(
                pieces.at[q, :, 1 - core],
                pair.at[q],
                pair_send.at[q],
                pair_recv.at[q],
                (s + 1 - 2 * core, x),
            )

        def proj(q):
            pieces[q] = (
                contract(sgb[q], lru[...], 0, 0).astype(BF).reshape(TPN, 2, 128, FFQ)
            )
            pair_to(q).start()

        loop(0, TPN, proj)
        for d in range(2):
            reach, inner = scan_rows(coeffs[d], state_grad, d == 0)
            edge = slice(0, 1) if d == 0 else slice(TOK - 1, TOK)
            decay = ends[2 * d : 2 * d + 1, :]
            ends[2 * d : 2 * d + 1, :] = decay * reach[edge]
            ends[2 * d + 1 : 2 * d + 2, :] = decay * inner[edge]
            linear[d, 3] = reach
            linear[d, 4] = inner

        def ends_to(k, target):
            return remote(ends, edges.at[s], end_send.at[k], end_recv.at[k], (target, x))

        for k in range(1, SPN):
            ends_to(k, peer(s, k)).start()
        edges[s] = ends[...]


        def meet(q):
            pair_to(q).wait_recv()
            paired[q] = (pieces[q, :, core].astype(F32) + pair[q].astype(F32)).astype(BF)

        loop(0, TPN, meet)
        first, second = pl.ds(0, 64), pl.ds(64, 64)

        def along_y(k):
            return lax.rem(y + k, 4), (z * 8 + lax.rem(y + k, 4) * 2 + core, x)

        def along_z(k):
            return lax.rem(z + k, 4), (lax.rem(z + k, 4) * 8 + y * 2 + core, x)

        def one(side, k):
            place, target = (along_y, along_z)[side](k)
            if side == 0:
                src, dst = paired.at[:, place, first, :], far_y.at[k - 1]
            else:
                src, dst = paired.at[place, :, second, :], far_z.at[k - 1]
            return remote(src, dst, one_send.at[side, k], one_recv.at[side, k], target)

        def two(side, k):
            place, target = (along_z, along_y)[side](k)
            if side == 0:
                src, dst = sum_y.at[place], last_y.at[k - 1]
            else:
                src, dst = sum_z.at[place], last_z.at[k - 1]
            return remote(src, dst, two_send.at[side, k], two_recv.at[side, k], target)

        for k in (1, 3, 2):
            for side in range(2):
                one(side, k).start()

        for k in range(1, SPN):
            ends_to(k, s ^ 1).wait_recv()

        def carry_in(j, carry):
            later = SPN - 1 - j
            e0, e1 = edges[later], edges[j]
            from_right = jnp.where(later > s, e0[1:2] + e0[0:1] * carry[0], carry[0])
            from_left = jnp.where(j < s, e1[3:4] + e1[2:3] * carry[1], carry[1])
            return from_right, from_left

        none = jnp.zeros((1, FFQ), F32)
        incoming = lax.fori_loop(0, SPN, carry_in, (none, none))

        def back_maps(d):
            adjoint = linear[d, 4] + linear[d, 3] * incoming[d]
            highest = lax.Precision.HIGHEST
            return (
                adjoint * linear[d, 0]
                + contract(adjoint * linear[d, 1], v_decay[d].astype(F32), 1, 1, highest)
                + contract(adjoint * linear[d, 2], v_input[d].astype(F32), 1, 1, highest)
            )

        conv_grad[...] = back_maps(0) + back_maps(1)

        for side in range(2):
            for k in (1, 3, 2):
                one(side, k).wait_recv()
            if side == 0:
                acc = paired[:, y, first, :].astype(F32)
            else:
                acc = paired[z, :, second, :].astype(F32)
            came = (far_y, far_z)[side]
            acc = acc + came[0].astype(F32) + came[1].astype(F32) + came[2].astype(F32)
            (sum_y, sum_z)[side][...] = acc.astype(BF)
            for k in (1, 3, 2):
                two(side, k).start()

        for side in range(2):
            for k in (1, 3, 2):
                two(side, k).wait_recv()
            came = (last_y, last_z)[side]
            acc = (sum_y[z] if side == 0 else sum_z[y]).astype(F32)
            acc = acc + came[0].astype(F32) + came[1].astype(F32) + came[2].astype(F32)
            proj_grad[pl.ds(side * 64, 64), :] = acc

        for side in range(2):
            for k in (1, 3, 2):
                one(side, k).wait_send()
                two(side, k).wait_send()
        loop(1, SPN, lambda k: ends_to(k, s ^ 1).wait_send())
        loop(0, TPN, lambda q: pair_to(q).wait_send())

    return gates, rest


def tail_kernel(
    part, combine, stream, out_grad, gain, states, branch, out_proj, conv, decay_map, input_map,
    base, shift, branch_grad, conv_grad, proj_grad, grad, *scratch,
):
    hello_all(lax.axis_index("sp"), lax.axis_index("tp"))
    gates, rest = mixer_steps(
        stream, out_grad, gain, grad, states, branch, out_proj, conv, decay_map, input_map, base,
        shift, branch_grad, conv_grad, proj_grad, *scratch[17:],
    )
    back_steps(gates, part, combine, grad, *scratch[:17])
    rest()


def tail(*operands):
    whole = (TPN, TOK, QW)
    square = (TOK, FFQ)
    dma = pltpu.SemaphoreType.DMA
    return pl.pallas_call(
        tail_kernel,
        in_specs=[ANY, VM, ANY, ANY, VM, ANY, ANY, ANY, ANY, ANY, ANY, VM, ANY],
        out_specs=[VM] * 3,
        out_shape=[
            jax.ShapeDtypeStruct(square, F32),
            jax.ShapeDtypeStruct(square, F32),
            jax.ShapeDtypeStruct((128, FFQ), F32),
        ],
        scratch_shapes=[
            pltpu.VMEM((TPN, CHUNKS, TOK, CW), BF),
            pltpu.VMEM((CHUNKS, 2, 640, CW), BF),
            pltpu.VMEM((CHUNKS, 2, 640, CW), BF),
            pltpu.VMEM((CHUNKS, SPN, 24, 2 * CW), BF),
            pltpu.VMEM((CHUNKS, SPN, 24, 2 * CW), BF),
            pltpu.VMEM((CHUNKS, TOK, CW), F32),
            pltpu.VMEM((CHUNKS, TOK, CW), BF),
            pltpu.VMEM((CHUNKS, TOK, CW), BF),
            dma((CHUNKS, 2)),
            dma((CHUNKS, 2)),
            dma((CHUNKS,)),
            dma((CHUNKS, SPN)),
            dma((CHUNKS, SPN)),
            dma((CHUNKS,)),
            dma((CHUNKS,)),
            dma((2, 2, CHUNKS)),
            dma((2, 2, CHUNKS)),
            dma((CHUNKS, 2)),
            pltpu.VMEM(whole, BF),
            pltpu.VMEM(whole, BF),
            pltpu.VMEM((TPN, QW, FFQ), BF),
            pltpu.VMEM((2,) + square, F32),
            pltpu.VMEM((2,) + square, F32),
            pltpu.VMEM(square, BF),
            pltpu.VMEM(square, BF),
            pltpu.VMEM((2, FFQ, FFQ), BF),
            pltpu.VMEM((2, FFQ, FFQ), BF),
            pltpu.VMEM(whole, BF),
            pltpu.VMEM((TOK, 128), F32),
            pltpu.VMEM((TOK, 128), F32),
            pltpu.VMEM(square, BF),
            pltpu.VMEM(square, F32),
            pltpu.VMEM((2, 5) + square, F32),
            pltpu.VMEM((2,) + square, F32),
            pltpu.VMEM((4, FFQ), F32),
            pltpu.VMEM((SPN, 4, FFQ), F32),
            pltpu.VMEM((4, 4, 2, 128, FFQ), BF),
            pltpu.VMEM((4, 4, 128, FFQ), BF),
            pltpu.VMEM((4, 4, 128, FFQ), BF),
            pltpu.VMEM((3, 4, 64, FFQ), BF),
            pltpu.VMEM((3, 4, 64, FFQ), BF),
            pltpu.VMEM((4, 64, FFQ), BF),
            pltpu.VMEM((4, 64, FFQ), BF),
            pltpu.VMEM((3, 64, FFQ), BF),
            pltpu.VMEM((3, 64, FFQ), BF),
            dma((3, TPN)),
            dma((6,)),
            dma((SPN,)),
            dma((SPN,)),
            dma((TPN,)),
            dma((TPN,)),
            dma((2, 4)),
            dma((2, 4)),
            dma((2, 4)),
            dma((2, 4)),
        ],
        compiler_params=pltpu.CompilerParams(
            collective_id=1, has_side_effects=True, vmem_limit_bytes=60 * 1024 * 1024
        ),
        name="tail",
    )(*operands)


def body(
    out_grad,
    stream,
    norm_gain,
    routes,
    route_weight,
    gate_weight,
    up_weight,
    down_weight,
    out_proj,
    conv_out,
    gate_branch,
    decay_map,
    input_map,
    decay_param,
    decay_shift,
    states,
):
    gain = norm_gain[None, :]
    got, combine = dispatch(stream, out_grad, gain, routes.T, route_weight.T)
    part, gate_wgrad, up_wgrad, down_wgrad = expert(
        got, gate_weight[0], up_weight[0], down_weight[0]
    )
    base = jax.nn.softplus(-decay_param)
    branch_grad, conv_grad, proj_grad = tail(
        part, combine, stream, out_grad, gain, states, gate_branch, out_proj, conv_out,
        decay_map[:, 0], input_map[:, 0], base, decay_shift,
    )
    return (
        conv_grad, branch_grad, proj_grad, gate_wgrad[None], up_wgrad[None], down_wgrad[None]
    )


def solution(mesh):
    in_specs = (
        P(SP, None),
        P(SP, None),
        P(),
        P(SP, None),
        P(SP, None),
        P(SP, None, "tp"),
        P(SP, None, "tp"),
        P(SP, "tp", None),
        P(None, "tp"),
        P(SP, "tp"),
        P(SP, "tp"),
        P(None, "tp", None, None),
        P(None, "tp", None, None),
        P(None, "tp"),
        P(None, SP, "tp"),
        P(None, SP, "tp"),
    )
    out_specs = (
        P(SP, "tp"),
        P(SP, "tp"),
        P(SP, "tp"),
        P(SP, None, "tp"),
        P(SP, None, "tp"),
        P(SP, "tp", None),
    )
    return jax.shard_map(body, mesh=mesh, in_specs=in_specs, out_specs=out_specs, check_vma=False)
```

time: 210 us -> 195 us (0.929)
  Pallas kernels: 200 us -> 187 us
  local copies, waits for them, and re-layouts: 8.69 us -> 6.22 us
    pallas_call x4 -> x2, Pallas kernels: 182 us -> 169 us  [the longest x1 94.3 us: tail(): pl.pallas_call(tail_kernel, in_specs=[ANY, VM, ANY, ANY, VM, ANY, ANY, AN...]
    unnamed x29 -> x5, local copies, waits for them, and re-layouts: 7.98 us -> 4.91 us
where the time goes in v5:
time: 195 us
  Pallas kernels  187 us (96%)
  local copies, waits for them, and re-layouts  6.22 us (3%)
    pallas_call x1, Pallas kernels, tail(): pl.pallas_call(tail_kernel, in_specs=[ANY, VM, ANY, ANY, VM, ANY, ANY, AN...  94.3 us
    pallas_call x1, Pallas kernels, dispatch(): pl.pallas_call(dispatch_kernel, in_specs=[ANY, ANY, VM, VM, VM], out_spec...  74.7 us
    pallas_call x1, Pallas kernels, expert(): pl.pallas_call(expert_kernel, in_specs=[ANY] * 4, out_specs=[ANY] * 4, ou...  18.1 us
    unnamed x5, local copies, waits for them, and re-layouts  4.91 us

profile of v5, /device:TPU:1, one launch (start us, length us, event | category | flops | bytes accessed | tf_op | source)
XLA Modules:
  0.0 194.6 jit_solution(1553783374432592890)
XLA Ops:
  0.6 1.3 broadcast_in_dim.12.gain
  1.9 74.7 %dispatch.1 = (bf16[2,2,5,256,1024]{4,3,2,1,0:T(8,128)(2,1)}, bf16[256,768]{1,0:T(8,128)(2,1)}) custom-call(bf16[256,4096]{1,0:T(8,128)(2,1)} %stream.3, bf16[256,4096]{1,0:T(8,128)(2,1)} %out_grad.3, bf16[1,4096]{1,0:T(2,128)(2,1)} %broadcast_in_dim.12.gain, s32[2,256]{1,0:T(2,128)} %bitcast.15, f32[2,256]{1,0:T(2,128)} %bitcast.16), custom_call_target="tpu_custom_call" | custom-call | tf_op jit(solution)/shard_map/dispatch/pallas_call | solution.py:244
  76.6 0.0 copy-start
  76.6 18.1 %expert.1 = (bf16[4,8,640,128]{3,2,1,0:T(8,128)(2,1)}, bf16[4096,256]{1,0:T(8,128)(2,1)}, bf16[4096,256]{1,0:T(8,128)(2,1)}, bf16[256,4096]{1,0:T(8,128)(2,1)}) custom-call(bf16[2,2,5,256,1024]{4,3,2,1,0:T(8,128)(2,1)} %get-tuple-element.15.got, bf16[4096,256]{1,0:T(8,128)(2,1)} %bitcast.10, bf16[4096,256]{1,0:T(8,128)(2,1)} %bitcast.11, ...), custom_call_target="tpu_custom_call" | custom-call | tf_op jit(solution)/shard_map/expert/pallas_call | solution.py:368
  94.7 0.0 copy-done
  94.7 0.6 compare_select_fusion.base
  95.3 94.3 %tail.1 = (f32[256,256]{1,0:T(8,128)}, f32[256,256]{1,0:T(8,128)}, f32[128,256]{1,0:T(8,128)}) custom-call(bf16[4,8,640,128]{3,2,1,0:T(8,128)(2,1)} %get-tuple-element.16.part, bf16[256,768]{1,0:T(8,128)(2,1)} %get-tuple-element.17.combine, bf16[256,4096]{1,0:T(8,128)(2,1)} %stream.3, bf16[256,4096]{1,0:T(8,128)(2,1)} %out_grad.3, ...), custom_call_target="tpu_custom_call" | custom-call | tf_op jit(solution)/shard_map/tail/pallas_call | solution.py:810
  189.7 1.7 copy.25
  191.3 1.7 copy.26
  193.0 1.6 copy.27
Async XLA Ops:
  76.6 18.1 %copy-start = (f32[2,256]{1,0:T(2,128)S(1)}, f32[2,256]{1,0:T(2,128)}, u32[]{:S(2)}) copy-start(f32[2,256]{1,0:T(2,128)} %param.29) | copy-start | bytes 6148

commit v6 on v5

--- a/solution.py
+++ b/solution.py
@@ -24,6 +24,7 @@
 CW = QW // CHUNKS
 rate_scale = 8.0
 norm_eps = 1e-06
+NBACK = 22
 
 
 def contract(left, right, left_dim, right_dim, precision=None):
@@ -52,27 +53,41 @@
     )
 
 
-def greet(s, x):
-    hello_all(s, x)
-    met()
-
-
-def met():
-    pl.semaphore_wait(pltpu.get_barrier_semaphore(), SPN + 1)
-
-
-def hello_all(s, x):
+def tell(sem, target):
+    pl.semaphore_signal(sem, inc=1, device_id=target, device_id_type=MESH)
+
+
+def line_y(s, k):
+    return s // 8 * 8 + lax.rem((s // 2) % 4 + k, 4) * 2 + s % 2
+
+
+def line_z(s, k):
+    return lax.rem(s // 8 + k, 4) * 8 + s % 8
+
+
+def hello(s, x):
     barrier = pltpu.get_barrier_semaphore()
-
-    def hello(d, carry):
-        pl.semaphore_signal(barrier, inc=1, device_id=(s ^ d, x), device_id_type=MESH)
-        return carry
-
-    lax.fori_loop(1, SPN, hello, 0)
+    for k in (1, 3, 2):
+        tell(barrier, (line_y(s, k), x))
+        tell(barrier, (line_z(s, k), x))
+    tell(barrier, (s + 1 - 2 * (s % 2), x))
     for step in (1, TPN - 1):
-        pl.semaphore_signal(
-            barrier, inc=1, device_id=(s, lax.rem(x + step, TPN)), device_id_type=MESH
-        )
+        tell(barrier, (s, lax.rem(x + step, TPN)))
+
+
+def hello_lines(s, x, sem):
+    pl.semaphore_wait(pltpu.get_barrier_semaphore(), 9)
+    for k in (1, 3, 2):
+        tell(sem.at[0], (line_y(s, k), x))
+
+
+def hello_cores(s, x, sem):
+    pl.semaphore_wait(sem.at[0], 3)
+    tell(sem.at[1], (s + 1 - 2 * (s % 2), x))
+
+
+def met(sem):
+    pl.semaphore_wait(sem.at[1], 1)
 
 
 def remote(src, dst, send_sem, recv_sem, target):
@@ -97,13 +112,13 @@
 def dispatch_kernel(
     stream, out_grad, gain, routes, weight, got, combine,
     send, v_stream, v_out, qi, qc0, qc1, scale,
-    load_sem, own_sem, send_sem, recv_sem, fwd_send, fwd_recv,
+    load_sem, own_sem, send_sem, recv_sem, fwd_send, fwd_recv, met_sem,
 ):
     s = lax.axis_index("sp")
     x = lax.axis_index("tp")
     high, low = x // 2, x % 2
     right, left = lax.rem(x + 1, TPN), lax.rem(x + TPN - 1, TPN)
-    hello_all(s, x)
+    hello(s, x)
 
     def columns(h):
         return pl.ds(pl.multiple_of((2 * h + low) * QW, QW), QW)
@@ -150,6 +165,7 @@
     combine[...] = (ret0 + ret1).astype(BF)
     qc0[...] = cot0.astype(BF)
     qc1[...] = cot1.astype(BF)
+    hello_lines(s, x, met_sem)
     whole.wait()
     wide = v_stream[...].astype(F32)
     mean = jnp.sum(wide * wide, axis=1, keepdims=True) * (1.0 / (TPN * QW))
@@ -206,8 +222,9 @@
     def block(i):
         return got.at[high, low, :, rows(i), :]
 
+    hello_cores(s, x, met_sem)
     gather_rows(high)
-    met()
+    met(met_sem)
     for side in range(2):
         onward(send.at[high, :, rows(s), :], block(s), 0, side).start()
     for turn in range(2):
@@ -263,6 +280,7 @@
             dma((2, SPN)),
             dma((2, SPN)),
             dma((2, SPN)),
+            pltpu.SemaphoreType.REGULAR((2,)),
         ],
         compiler_params=pltpu.CompilerParams(
             collective_id=0, has_side_effects=True, vmem_limit_bytes=62 * 1024 * 1024
@@ -277,9 +295,9 @@
 
 
 def expert_kernel(
-    got, gate, up, down, part, gate_wg, up_wg, down_wg,
-    vin, vcot, vmix, vg, vu, vd, vpart, ogu, od, gp, upre, hg, gu, hid,
-    in_sem, w_sem, part_sem, o_sem,
+    got, gate, up, down, slopes, gate_wg, up_wg, down_wg,
+    vin, vcot, vmix, vg, vu, vd, ogu, od, gp, upre, hg, gu, hid,
+    in_sem, w_sem, slope_sem, o_sem,
 ):
     def loads(q):
         hi, lo = q // 2, q % 2
@@ -329,18 +347,8 @@
     ).astype(BF)
     gu[:, FFQ : 2 * FFQ] = (hidden_grad * silu).astype(BF)
 
-    def part_out(q):
-        return pltpu.make_async_copy(vpart.at[q], part.at[q], part_sem.at[q])
-
-    def back(q):
-        rows = (
-            contract(gu[:, 0:FFQ], vg[q], 1, 1) + contract(gu[:, FFQ : 2 * FFQ], vu[q], 1, 1)
-        ).astype(BF)
-        for c in range(CHUNKS):
-            vpart[q, c] = rows[:, c * CW : (c + 1) * CW]
-        part_out(q).start()
-
-    loop(0, TPN, back)
+    out = pltpu.make_async_copy(gu, slopes, slope_sem)
+    out.start()
 
     def grads_out(q):
         rows = pl.ds(pl.multiple_of(q * QW, QW), QW)
@@ -359,7 +367,7 @@
             c.start()
 
     loop(0, TPN, weights)
-    loop(0, TPN, lambda q: part_out(q).wait())
+    out.wait()
     loop(0, TPN, lambda q: [c.wait() for c in grads_out(q)])
 
 
@@ -370,7 +378,7 @@
         in_specs=[ANY] * 4,
         out_specs=[ANY] * 4,
         out_shape=[
-            jax.ShapeDtypeStruct((TPN, CHUNKS, 640, CW), BF),
+            jax.ShapeDtypeStruct((640, 2 * FFQ), BF),
             jax.ShapeDtypeStruct((full, FFQ), BF),
             jax.ShapeDtypeStruct((full, FFQ), BF),
             jax.ShapeDtypeStruct((FFQ, full), BF),
@@ -382,7 +390,6 @@
             pltpu.VMEM((TPN, QW, FFQ), BF),
             pltpu.VMEM((TPN, QW, FFQ), BF),
             pltpu.VMEM((TPN, FFQ, QW), BF),
-            pltpu.VMEM((TPN, CHUNKS, 640, CW), BF),
             pltpu.VMEM((2, TPN, QW, FFQ), BF),
             pltpu.VMEM((TPN, FFQ, QW), BF),
             pltpu.VMEM((640, FFQ), F32),
@@ -392,7 +399,7 @@
             pltpu.VMEM((640, FFQ), BF),
             pltpu.SemaphoreType.DMA((TPN, 5)),
             pltpu.SemaphoreType.DMA((3, TPN)),
-            pltpu.SemaphoreType.DMA((TPN,)),
+            pltpu.SemaphoreType.DMA,
             pltpu.SemaphoreType.DMA((3, TPN)),
         ],
         compiler_params=pltpu.CompilerParams(vmem_limit_bytes=60 * 1024 * 1024),
@@ -401,8 +408,10 @@
 
 
 def back_steps(
-    fill, part, combine, grad, mine, near, final, back, held, give, second,
-    near_send, near_recv, own_sem, ret_send, ret_recv, two_send, two_recv, all_send, all_recv, mine_sem,
+    start, fill, slopes, gate, up, combine, grad,
+    part, v_gate, v_up, v_slopes, near, final, back, held, give, second,
+    near_send, near_recv, own_sem, ret_send, ret_recv, two_send, two_recv, all_send, all_recv,
+    w_sem, slope_sem, met_sem,
 ):
     s = lax.axis_index("sp")
     x = lax.axis_index("tp")
@@ -425,12 +434,6 @@
             (s, pair),
         )
 
-    def load_mine(c, j):
-        _, other = partners(c)
-        return pltpu.make_async_copy(
-            part.at[x if j == 0 else other, c], mine.at[c, j], mine_sem.at[c, j]
-        )
-
     def own_back(c):
         return pltpu.make_async_copy(final.at[c, s], back.at[c, s], own_sem.at[c])
 
@@ -459,21 +462,46 @@
         for j in range(2):
             to_pair(c, j).start()
 
-    def begin_load(c):
+    def load(q):
+        rows = pl.ds(pl.multiple_of(q * QW, QW), QW)
+        return (
+            pltpu.make_async_copy(gate.at[rows, :], v_gate.at[q], w_sem.at[0, q]),
+            pltpu.make_async_copy(up.at[rows, :], v_up.at[q], w_sem.at[1, q]),
+        )
+
+    def begin_load(q):
+        for copy in load(q):
+            copy.start()
+
+    def rows_of(q):
+        for copy in load(q):
+            copy.wait()
+        rows = (
+            contract(v_slopes[:, 0:FFQ], v_gate[q], 1, 1)
+            + contract(v_slopes[:, FFQ : 2 * FFQ], v_up[q], 1, 1)
+        ).astype(BF)
+        for c in range(CHUNKS):
+            part[q, c] = rows[:, c * CW : (c + 1) * CW]
+
+    take = pltpu.make_async_copy(slopes, v_slopes, slope_sem)
+    take.start()
+    loop(0, TPN, begin_load)
+    start()
+    take.wait()
+    loop(0, TPN // 2, rows_of)
+    hello_lines(s, x, met_sem)
+    loop(TPN // 2, TPN, rows_of)
+    hello_cores(s, x, met_sem)
+    met(met_sem)
+    loop(0, CHUNKS, begin)
+    fill()
+
+    def open_chunk(t):
+        _, other = partners(t)
         for j in range(2):
-            load_mine(c, j).start()
-
-    met()
-    loop(0, CHUNKS, begin)
-    loop(0, CHUNKS, begin_load)
-
-    fill()
-
-    def open_chunk(t):
-        for j in range(2):
-            load_mine(t, j).wait()
             to_pair(t, j).wait_recv()
-            total = (mine[t, j].astype(F32) + near[t, j].astype(F32)).astype(BF)
+            mine = part[x if j == 0 else other, t]
+            total = (mine.astype(F32) + near[t, j].astype(F32)).astype(BF)
             lanes = slice(j * CW, (j + 1) * CW)
             final[t, :, 0:8, lanes] = total[0:256].reshape(32, 8, CW)
             final[t, :, 8:16, lanes] = total[256:512].reshape(32, 8, CW)
@@ -559,7 +587,7 @@
     stream, out_grad, gain, grad, states, branch, out_proj, conv, decay_map, input_map, base, shift,
     branch_grad, conv_grad, proj_grad,
     v_stream, v_out, v_proj, v_states, v_shift, v_branch, v_conv, v_decay, v_input,
-    sgb, dot, scale, lru, pulled, linear, coeffs,
+    sgb, dot, scale, lru, pulled, linear, coeffs, factors,
     ends, edges, pieces, pair, paired, far_y, far_z, sum_y, sum_z, last_y, last_z,
     big_sem, small_sem, end_send, end_recv, pair_send, pair_recv, one_send, one_recv,
     two_send, two_recv,
@@ -590,14 +618,15 @@
             )
         )
     ]
-    for copy in small:
-        copy.start()
-
     def begin(q):
         for which in range(3):
             big(which, q).start()
 
-    loop(0, TPN, begin)
+    def start():
+        for copy in small:
+            copy.start()
+        loop(0, TPN, begin)
+
     def gates():
         for copy in small:
             copy.wait()
@@ -623,27 +652,39 @@
                 ((v_states[d] - drive) - i * c * decay * decay / width) * rate * r * (1.0 - r)
             )
             linear[d, 2] = width * c * i * (1.0 - i)
+        total = v_states[0] + v_states[1]
+        b = v_branch[...].astype(F32)
+        root = 0.7978845608028654
+        tanh = jnp.tanh(root * (b + 0.044715 * b * b * b))
+        gelu = 0.5 * b * (1.0 + tanh)
+        slope = 0.5 * (1.0 + tanh) + 0.5 * b * (1.0 - tanh * tanh) * root * (
+            1.0 + 3.0 * 0.044715 * b * b
+        )
+        lru[...] = (total * gelu).astype(BF)
+        factors[0] = total * slope
+        factors[1] = gelu
+
+        def squares(q, carry):
+            big(0, q).wait()
+            v = v_stream[q].astype(F32)
+            return carry + jnp.sum(v * v, axis=1, keepdims=True)
+
+        square = lax.fori_loop(0, TPN, squares, jnp.zeros((TOK, 1), F32))
+        scale[...] = jnp.broadcast_to(
+            lax.rsqrt(square * (1.0 / (TPN * QW)) + norm_eps), (TOK, 128)
+        )
 
     def rest():
         def grad_of(q):
             return jnp.concatenate([grad[q, c] for c in range(CHUNKS)], axis=1).astype(F32)
 
-        def squares(q, carry):
-            big(0, q).wait()
-            v = v_stream[q].astype(F32)
+        def projected(q, carry):
             g = gain[:, pl.ds(pl.multiple_of(q * QW, QW), QW)].astype(F32)
-            w = v * (g * grad_of(q))
-            return (
-                carry[0] + jnp.sum(v * v, axis=1, keepdims=True),
-                carry[1] + jnp.sum(w, axis=1, keepdims=True),
-            )
-
-        zero = jnp.zeros((TOK, 1), F32)
-        square, along = lax.fori_loop(0, TPN, squares, (zero, zero))
-        inverse = 1.0 / (TPN * QW)
-        row_scale = lax.rsqrt(square * inverse + norm_eps)
-        scale[...] = jnp.broadcast_to(row_scale, (TOK, 128))
-        dot[...] = jnp.broadcast_to(along * row_scale * inverse, (TOK, 128))
+            w = v_stream[q].astype(F32) * (g * grad_of(q))
+            return carry + jnp.sum(w, axis=1, keepdims=True)
+
+        along = lax.fori_loop(0, TPN, projected, jnp.zeros((TOK, 1), F32))
+        dot[...] = jnp.broadcast_to(along * scale[:, 0:1] * (1.0 / (TPN * QW)), (TOK, 128))
         pulled[...] = jnp.zeros_like(pulled)
 
         def rows_grad(q):
@@ -658,17 +699,8 @@
 
         loop(0, TPN, rows_grad)
         lru_grad = pulled[...]
-        total = v_states[0] + v_states[1]
-        b = v_branch[...].astype(F32)
-        root = 0.7978845608028654
-        tanh = jnp.tanh(root * (b + 0.044715 * b * b * b))
-        gelu = 0.5 * b * (1.0 + tanh)
-        slope = 0.5 * (1.0 + tanh) + 0.5 * b * (1.0 - tanh * tanh) * root * (
-            1.0 + 3.0 * 0.044715 * b * b
-        )
-        lru[...] = (total * gelu).astype(BF)
-        branch_grad[...] = lru_grad * total * slope
-        state_grad = lru_grad * gelu
+        branch_grad[...] = lru_grad * factors[0]
+        state_grad = lru_grad * factors[1]
         def pair_to(q):
             return remote(
                 pieces.at[q, :, 1 - core],
@@ -787,19 +819,19 @@
         loop(1, SPN, lambda k: ends_to(k, s ^ 1).wait_send())
         loop(0, TPN, lambda q: pair_to(q).wait_send())
 
-    return gates, rest
+    return start, gates, rest
 
 
 def tail_kernel(
-    part, combine, stream, out_grad, gain, states, branch, out_proj, conv, decay_map, input_map,
-    base, shift, branch_grad, conv_grad, proj_grad, grad, *scratch,
+    slopes, gate, up, combine, stream, out_grad, gain, states, branch, out_proj, conv, decay_map,
+    input_map, base, shift, branch_grad, conv_grad, proj_grad, grad, *scratch,
 ):
-    hello_all(lax.axis_index("sp"), lax.axis_index("tp"))
-    gates, rest = mixer_steps(
+    hello(lax.axis_index("sp"), lax.axis_index("tp"))
+    start, gates, rest = mixer_steps(
         stream, out_grad, gain, grad, states, branch, out_proj, conv, decay_map, input_map, base,
-        shift, branch_grad, conv_grad, proj_grad, *scratch[17:],
+        shift, branch_grad, conv_grad, proj_grad, *scratch[NBACK:],
     )
-    back_steps(gates, part, combine, grad, *scratch[:17])
+    back_steps(start, gates, slopes, gate, up, combine, grad, *scratch[:NBACK])
     rest()
 
 
@@ -809,7 +841,7 @@
     dma = pltpu.SemaphoreType.DMA
     return pl.pallas_call(
         tail_kernel,
-        in_specs=[ANY, VM, ANY, ANY, VM, ANY, ANY, ANY, ANY, ANY, ANY, VM, ANY],
+        in_specs=[ANY, ANY, ANY, VM, ANY, ANY, VM, ANY, ANY, ANY, ANY, ANY, ANY, VM, ANY],
         out_specs=[VM] * 3,
         out_shape=[
             jax.ShapeDtypeStruct(square, F32),
@@ -818,7 +850,10 @@
         ],
         scratch_shapes=[
             pltpu.VMEM((TPN, CHUNKS, TOK, CW), BF),
-            pltpu.VMEM((CHUNKS, 2, 640, CW), BF),
+            pltpu.VMEM((TPN, CHUNKS, 640, CW), BF),
+            pltpu.VMEM((TPN, QW, FFQ), BF),
+            pltpu.VMEM((TPN, QW, FFQ), BF),
+            pltpu.VMEM((640, 2 * FFQ), BF),
             pltpu.VMEM((CHUNKS, 2, 640, CW), BF),
             pltpu.VMEM((CHUNKS, SPN, 24, 2 * CW), BF),
             pltpu.VMEM((CHUNKS, SPN, 24, 2 * CW), BF),
@@ -834,7 +869,9 @@
             dma((CHUNKS,)),
             dma((2, 2, CHUNKS)),
             dma((2, 2, CHUNKS)),
-            dma((CHUNKS, 2)),
+            dma((2, TPN)),
+            dma,
+            pltpu.SemaphoreType.REGULAR((2,)),
             pltpu.VMEM(whole, BF),
             pltpu.VMEM(whole, BF),
             pltpu.VMEM((TPN, QW, FFQ), BF),
@@ -850,6 +887,7 @@
             pltpu.VMEM(square, BF),
             pltpu.VMEM(square, F32),
             pltpu.VMEM((2, 5) + square, F32),
+            pltpu.VMEM((2,) + square, F32),
             pltpu.VMEM((2,) + square, F32),
             pltpu.VMEM((4, FFQ), F32),
             pltpu.VMEM((SPN, 4, FFQ), F32),
@@ -874,7 +912,7 @@
             dma((2, 4)),
         ],
         compiler_params=pltpu.CompilerParams(
-            collective_id=1, has_side_effects=True, vmem_limit_bytes=60 * 1024 * 1024
+            collective_id=1, has_side_effects=True, vmem_limit_bytes=52 * 1024 * 1024
         ),
         name="tail",
     )(*operands)
@@ -900,12 +938,12 @@
 ):
     gain = norm_gain[None, :]
     got, combine = dispatch(stream, out_grad, gain, routes.T, route_weight.T)
-    part, gate_wgrad, up_wgrad, down_wgrad = expert(
+    slopes, gate_wgrad, up_wgrad, down_wgrad = expert(
         got, gate_weight[0], up_weight[0], down_weight[0]
     )
     base = jax.nn.softplus(-decay_param)
     branch_grad, conv_grad, proj_grad = tail(
-        part, combine, stream, out_grad, gain, states, gate_branch, out_proj, conv_out,
+        slopes, gate_weight[0], up_weight[0], combine, stream, out_grad, gain, states, gate_branch, out_proj, conv_out,
         decay_map[:, 0], input_map[:, 0], base, decay_shift,
     )
     return (

time: 195 us -> 186 us (0.954)
  Pallas kernels: 187 us -> 181 us
  local copies, waits for them, and re-layouts: 6.22 us -> 3.42 us
    pallas_call x1, Pallas kernels: 18.1 us -> 14.6 us  [expert(): pl.pallas_call(expert_kernel, in_specs=[ANY] * 4, out_specs=[ANY] * 4, ou...]
    unnamed x5 -> x17, local copies, waits for them, and re-layouts: 4.91 us -> 2.1 us
where the time goes in v6:
time: 186 us
  Pallas kernels  181 us (97%)
  local copies, waits for them, and re-layouts  3.42 us (2%)
    pallas_call x1, Pallas kernels, tail(): pl.pallas_call(tail_kernel, in_specs=[ANY, ANY, ANY, VM, ANY, ANY, VM, AN...  93.3 us
    pallas_call x1, Pallas kernels, dispatch(): pl.pallas_call(dispatch_kernel, in_specs=[ANY, ANY, VM, VM, VM], out_spec...  73.4 us
    pallas_call x1, Pallas kernels, expert(): pl.pallas_call(expert_kernel, in_specs=[ANY] * 4, out_specs=[ANY] * 4, ou...  14.6 us

profile of v6, /device:TPU:1, one launch (start us, length us, event | category | flops | bytes accessed | tf_op | source)
XLA Modules:
  0.0 185.6 jit_solution(12927766797502350296)
XLA Ops:
  0.6 1.3 broadcast_in_dim.12.gain
  1.9 73.4 %dispatch.1 = (bf16[2,2,5,256,1024]{4,3,2,1,0:T(8,128)(2,1)}, bf16[256,768]{1,0:T(8,128)(2,1)}) custom-call(bf16[256,4096]{1,0:T(8,128)(2,1)} %stream.3, bf16[256,4096]{1,0:T(8,128)(2,1)} %out_grad.3, bf16[1,4096]{1,0:T(2,128)(2,1)} %broadcast_in_dim.12.gain, s32[2,256]{1,0:T(2,128)} %bitcast.17, f32[2,256]{1,0:T(2,128)} %bitcast.18), custom_call_target="tpu_custom_call" | custom-call | tf_op jit(solution)/shard_map/dispatch/pallas_call | solution.py:261
  75.4 0.0 copy-start.6
  75.4 0.0 copy-start
  75.4 0.0 copy-start.1
  75.4 0.0 copy-start.2
  75.4 0.0 copy-start.3
  75.5 0.0 copy-start.4
  75.5 0.0 copy-start.5
  75.5 14.6 %expert.1 = (bf16[640,512]{1,0:T(8,128)(2,1)}, bf16[4096,256]{1,0:T(8,128)(2,1)}, bf16[4096,256]{1,0:T(8,128)(2,1)}, bf16[256,4096]{1,0:T(8,128)(2,1)}) custom-call(bf16[2,2,5,256,1024]{4,3,2,1,0:T(8,128)(2,1)} %get-tuple-element.15.got, bf16[4096,256]{1,0:T(8,128)(2,1)} %bitcast.12, bf16[4096,256]{1,0:T(8,128)(2,1)} %bitcast.14, bf16[256,4096]{1,0:T(8,128)(2,1)} %bitcast.16), custom_call_target="tpu_custom_call" | custom-call | tf_op jit(solution)/shard_map/expert/pallas_call | solution.py:376
  90.1 0.0 copy-done.6
  90.1 0.0 copy-done
  90.2 0.0 copy-done.1
  90.2 0.0 copy-done.2
  90.2 0.0 copy-done.3
  90.2 0.0 copy-done.4
  90.2 0.0 copy-done.5
  90.2 93.3 %tail.1 = (f32[256,256]{1,0:T(8,128)S(1)}, f32[256,256]{1,0:T(8,128)S(1)}, f32[128,256]{1,0:T(8,128)S(1)}) custom-call(bf16[640,512]{1,0:T(8,128)(2,1)} %get-tuple-element.16.slopes, bf16[4096,256]{1,0:T(8,128)(2,1)} %bitcast.13, bf16[4096,256]{1,0:T(8,128)(2,1)} %bitcast.15, bf16[256,768]{1,0:T(8,128)(2,1)S(1)} %copy-done, bf16[256,4096]{1,0:T(8,128)(2,1)} %stream.3, ...), custom_call_target="tpu_custom_call" | custom-call | tf_op jit(solution)/shard_map/tail/pallas_call | solution.py:842
  183.5 0.7 copy.25
  184.2 0.7 copy.26
  184.9 0.7 copy.27
  (1 shorter events, 0.0 us)
Async XLA Ops:
  75.4 14.7 %copy-start.6 = (f32[2,256]{1,0:T(2,128)S(1)}, f32[2,256]{1,0:T(2,128)}, u32[]{:S(2)}) copy-start(f32[2,256]{1,0:T(2,128)} %param.29) | copy-start | bytes 6148
  75.4 14.7 %copy-start = (bf16[256,768]{1,0:T(8,128)(2,1)S(1)}, bf16[256,768]{1,0:T(8,128)(2,1)}, u32[]{:S(2)}) copy-start(bf16[256,768]{1,0:T(8,128)(2,1)} %get-tuple-element.17.combine) | copy-start | bytes 1179652
  75.4 14.7 %copy-start.1 = (bf16[2,1,256,256]{3,2,1,0:T(8,128)(2,1)S(1)}, bf16[2,1,256,256]{3,2,1,0:T(8,128)(2,1)}, u32[]{:S(2)}) copy-start(bf16[2,1,256,256]{3,2,1,0:T(8,128)(2,1)} %param.27) | copy-start | bytes 786436
  75.4 14.7 %copy-start.2 = (bf16[2,1,256,256]{3,2,1,0:T(8,128)(2,1)S(1)}, bf16[2,1,256,256]{3,2,1,0:T(8,128)(2,1)}, u32[]{:S(2)}) copy-start(bf16[2,1,256,256]{3,2,1,0:T(8,128)(2,1)} %param.28) | copy-start | bytes 786436
  75.4 14.7 %copy-start.3 = (bf16[1,4096]{1,0:T(2,128)(2,1)S(1)}, bf16[1,4096]{1,0:T(2,128)(2,1)}, u32[]{:S(2)}) copy-start(bf16[1,4096]{1,0:T(2,128)(2,1)} %broadcast_in_dim.12.gain) | copy-start | bytes 24580
  75.5 14.7 %copy-start.4 = (bf16[256,256]{1,0:T(8,128)(2,1)S(1)}, bf16[256,256]{1,0:T(8,128)(2,1)}, u32[]{:S(2)}) copy-start(bf16[256,256]{1,0:T(8,128)(2,1)} %branch.1) | copy-start | bytes 393220
  75.5 14.7 %copy-start.5 = (bf16[256,256]{1,0:T(8,128)(2,1)S(1)}, bf16[256,256]{1,0:T(8,128)(2,1)}, u32[]{:S(2)}) copy-start(bf16[256,256]{1,0:T(8,128)(2,1)} %conv.1) | copy-start | bytes 393220

commit v7 on v6

--- a/solution.py
+++ b/solution.py
@@ -175,7 +175,7 @@
         load(h).wait()
         cols = columns(h)
         normed = (
-            v_stream[:, cols].astype(F32) * scale[:, 0:1] * gain[:, cols].astype(F32)
+            v_stream[:, cols].astype(F32) * scale[:, 0:1] * gain[cols].astype(F32).reshape(1, QW)
         ).astype(BF)
         grad = v_out[h].astype(F32)
         scaled0 = (w0 * grad).astype(BF)
@@ -531,7 +531,7 @@
             spread(c, side).wait_recv()
             spread_on(c, side).start()
 
-    lag = 3
+    lag = 2
 
     def stage(t):
         open_chunk(t)
@@ -541,11 +541,17 @@
             close_chunk(t - lag)
 
     loop(0, CHUNKS, stage)
-    loop(0, CHUNKS - lag, share)
-    loop(CHUNKS - lag, CHUNKS, close_chunk)
-    loop(0, CHUNKS - lag, share_on)
-    loop(CHUNKS - lag, CHUNKS, share)
-    loop(CHUNKS - lag, CHUNKS, share_on)
+    early = CHUNKS - 3
+    loop(0, early, share)
+    close_chunk(CHUNKS - 2)
+    loop(0, early, share_on)
+    share(CHUNKS - 3)
+    close_chunk(CHUNKS - 1)
+    share(CHUNKS - 2)
+    share_on(CHUNKS - 3)
+    share(CHUNKS - 1)
+    share_on(CHUNKS - 2)
+    share_on(CHUNKS - 1)
 
     def finish(c):
         for j in range(2):
@@ -679,7 +685,7 @@
             return jnp.concatenate([grad[q, c] for c in range(CHUNKS)], axis=1).astype(F32)
 
         def projected(q, carry):
-            g = gain[:, pl.ds(pl.multiple_of(q * QW, QW), QW)].astype(F32)
+            g = gain[pl.ds(pl.multiple_of(q * QW, QW), QW)].astype(F32).reshape(1, QW)
             w = v_stream[q].astype(F32) * (g * grad_of(q))
             return carry + jnp.sum(w, axis=1, keepdims=True)
 
@@ -692,7 +698,7 @@
             big(2, q).wait()
             r = scale[:, 0:1]
             unit = v_stream[q].astype(F32) * r
-            scaled = gain[:, pl.ds(pl.multiple_of(q * QW, QW), QW)].astype(F32) * grad_of(q)
+            scaled = gain[pl.ds(pl.multiple_of(q * QW, QW), QW)].astype(F32).reshape(1, QW) * grad_of(q)
             v = (v_out[q].astype(F32) + r * (scaled - unit * dot[:, 0:1])).astype(BF)
             sgb[q] = v
             pulled[...] += contract(v, v_proj[q], 1, 0)
@@ -936,7 +942,7 @@
     decay_shift,
     states,
 ):
-    gain = norm_gain[None, :]
+    gain = norm_gain
     got, combine = dispatch(stream, out_grad, gain, routes.T, route_weight.T)
     slopes, gate_wgrad, up_wgrad, down_wgrad = expert(
         got, gate_weight[0], up_weight[0], down_weight[0]

time: 186 us -> 185 us (level)
  no operation moved by 1% of the time
where the time goes in v7:
time: 185 us; the launch traced here: 184 us
  Pallas kernels  181 us (98%)
  local copies, waits for them, and re-layouts  2.1 us (1%)
    pallas_call x1, Pallas kernels, tail(): pl.pallas_call(tail_kernel, in_specs=[ANY, ANY, ANY, VM, ANY, ANY, VM, AN...  93.3 us
    pallas_call x1, Pallas kernels, dispatch(): pl.pallas_call(dispatch_kernel, in_specs=[ANY, ANY, VM, VM, VM], out_spec...  73.5 us
    pallas_call x1, Pallas kernels, expert(): pl.pallas_call(expert_kernel, in_specs=[ANY] * 4, out_specs=[ANY] * 4, ou...  14.6 us

profile of v7, /device:TPU:1, one launch (start us, length us, event | category | flops | bytes accessed | tf_op | source)
XLA Modules:
  0.0 184.4 jit_solution(6092142318273535308)
XLA Ops:
  0.6 73.5 %dispatch.1 = (bf16[2,2,5,256,1024]{4,3,2,1,0:T(8,128)(2,1)}, bf16[256,768]{1,0:T(8,128)(2,1)}) custom-call(bf16[256,4096]{1,0:T(8,128)(2,1)} %stream.3, bf16[256,4096]{1,0:T(8,128)(2,1)} %out_grad.3, bf16[4096]{0:T(1024)(128)(2,1)} %gain.3, s32[2,256]{1,0:T(2,128)} %bitcast.17, f32[2,256]{1,0:T(2,128)} %bitcast.18), custom_call_target="tpu_custom_call" | custom-call | tf_op jit(solution)/shard_map/dispatch/pallas_call | solution.py:261
  74.2 0.0 copy-start.6
  74.2 0.0 copy-start
  74.2 0.0 copy-start.1
  74.2 0.0 copy-start.2
  74.2 0.0 copy-start.3
  74.2 0.0 copy-start.4
  74.2 0.0 copy-start.5
  74.2 14.6 %expert.1 = (bf16[640,512]{1,0:T(8,128)(2,1)}, bf16[4096,256]{1,0:T(8,128)(2,1)}, bf16[4096,256]{1,0:T(8,128)(2,1)}, bf16[256,4096]{1,0:T(8,128)(2,1)}) custom-call(bf16[2,2,5,256,1024]{4,3,2,1,0:T(8,128)(2,1)} %get-tuple-element.15.got, bf16[4096,256]{1,0:T(8,128)(2,1)} %bitcast.12, bf16[4096,256]{1,0:T(8,128)(2,1)} %bitcast.14, bf16[256,4096]{1,0:T(8,128)(2,1)} %bitcast.16), custom_call_target="tpu_custom_call" | custom-call | tf_op jit(solution)/shard_map/expert/pallas_call | solution.py:376
  88.9 0.0 copy-done.6
  88.9 0.0 copy-done
  88.9 0.0 copy-done.1
  88.9 0.0 copy-done.2
  88.9 0.0 copy-done.3
  88.9 0.0 copy-done.4
  88.9 0.0 copy-done.5
  88.9 93.3 %tail.1 = (f32[256,256]{1,0:T(8,128)S(1)}, f32[256,256]{1,0:T(8,128)S(1)}, f32[128,256]{1,0:T(8,128)S(1)}) custom-call(bf16[640,512]{1,0:T(8,128)(2,1)} %get-tuple-element.16.slopes, bf16[4096,256]{1,0:T(8,128)(2,1)} %bitcast.13, bf16[4096,256]{1,0:T(8,128)(2,1)} %bitcast.15, bf16[256,768]{1,0:T(8,128)(2,1)S(1)} %copy-done, bf16[256,4096]{1,0:T(8,128)(2,1)} %stream.3, ...), custom_call_target="tpu_custom_call" | custom-call | tf_op jit(solution)/shard_map/tail/pallas_call | solution.py:848
  182.3 0.7 copy.25
  183.0 0.7 copy.26
  183.7 0.7 copy.27
  (1 shorter events, 0.0 us)
Async XLA Ops:
  74.2 14.7 %copy-start.6 = (f32[2,256]{1,0:T(2,128)S(1)}, f32[2,256]{1,0:T(2,128)}, u32[]{:S(2)}) copy-start(f32[2,256]{1,0:T(2,128)} %param.29) | copy-start | bytes 6148
  74.2 14.7 %copy-start = (bf16[256,768]{1,0:T(8,128)(2,1)S(1)}, bf16[256,768]{1,0:T(8,128)(2,1)}, u32[]{:S(2)}) copy-start(bf16[256,768]{1,0:T(8,128)(2,1)} %get-tuple-element.17.combine) | copy-start | bytes 1179652
  74.2 14.7 %copy-start.1 = (bf16[2,1,256,256]{3,2,1,0:T(8,128)(2,1)S(1)}, bf16[2,1,256,256]{3,2,1,0:T(8,128)(2,1)}, u32[]{:S(2)}) copy-start(bf16[2,1,256,256]{3,2,1,0:T(8,128)(2,1)} %param.27) | copy-start | bytes 786436
  74.2 14.7 %copy-start.2 = (bf16[2,1,256,256]{3,2,1,0:T(8,128)(2,1)S(1)}, bf16[2,1,256,256]{3,2,1,0:T(8,128)(2,1)}, u32[]{:S(2)}) copy-start(bf16[2,1,256,256]{3,2,1,0:T(8,128)(2,1)} %param.28) | copy-start | bytes 786436
  74.2 14.7 %copy-start.3 = (bf16[256,256]{1,0:T(8,128)(2,1)S(1)}, bf16[256,256]{1,0:T(8,128)(2,1)}, u32[]{:S(2)}) copy-start(bf16[256,256]{1,0:T(8,128)(2,1)} %branch.1) | copy-start | bytes 393220
  74.2 14.7 %copy-start.4 = (bf16[256,256]{1,0:T(8,128)(2,1)S(1)}, bf16[256,256]{1,0:T(8,128)(2,1)}, u32[]{:S(2)}) copy-start(bf16[256,256]{1,0:T(8,128)(2,1)} %conv.1) | copy-start | bytes 393220
  74.2 14.7 %copy-start.5 = (bf16[4096]{0:T(1024)(128)(2,1)S(1)}, bf16[4096]{0:T(1024)(128)(2,1)}, u32[]{:S(2)}) copy-start(bf16[4096]{0:T(1024)(128)(2,1)} %gain.3) | copy-start | bytes 24580

commit v8 on v7

--- a/solution.py
+++ b/solution.py
@@ -488,12 +488,13 @@
     loop(0, TPN, begin_load)
     start()
     take.wait()
-    loop(0, TPN // 2, rows_of)
+    loop(1, TPN // 2, lambda k: rows_of(lax.rem(x + k, TPN)))
     hello_lines(s, x, met_sem)
-    loop(TPN // 2, TPN, rows_of)
+    loop(TPN // 2, TPN, lambda k: rows_of(lax.rem(x + k, TPN)))
     hello_cores(s, x, met_sem)
     met(met_sem)
     loop(0, CHUNKS, begin)
+    rows_of(x)
     fill()
 
     def open_chunk(t):

time: 185 us -> 185 us (level)
  no operation moved by 1% of the time
where the time goes in v8:
time: 185 us
  Pallas kernels  182 us (98%)
  local copies, waits for them, and re-layouts  2.1 us (1%)
    pallas_call x1, Pallas kernels, tail(): pl.pallas_call(tail_kernel, in_specs=[ANY, ANY, ANY, VM, ANY, ANY, VM, AN...  93.7 us
    pallas_call x1, Pallas kernels, dispatch(): pl.pallas_call(dispatch_kernel, in_specs=[ANY, ANY, VM, VM, VM], out_spec...  73.5 us
    pallas_call x1, Pallas kernels, expert(): pl.pallas_call(expert_kernel, in_specs=[ANY] * 4, out_specs=[ANY] * 4, ou...  14.6 us

profile of v8, /device:TPU:1, one launch (start us, length us, event | category | flops | bytes accessed | tf_op | source)
XLA Modules:
  0.0 184.7 jit_solution(9753363522466593172)
XLA Ops:
  0.6 73.5 %dispatch.1 = (bf16[2,2,5,256,1024]{4,3,2,1,0:T(8,128)(2,1)}, bf16[256,768]{1,0:T(8,128)(2,1)}) custom-call(bf16[256,4096]{1,0:T(8,128)(2,1)} %stream.3, bf16[256,4096]{1,0:T(8,128)(2,1)} %out_grad.3, bf16[4096]{0:T(1024)(128)(2,1)} %gain.3, s32[2,256]{1,0:T(2,128)} %bitcast.17, f32[2,256]{1,0:T(2,128)} %bitcast.18), custom_call_target="tpu_custom_call" | custom-call | tf_op jit(solution)/shard_map/dispatch/pallas_call | solution.py:261
  74.2 0.0 copy-start.6
  74.2 0.0 copy-start
  74.2 0.0 copy-start.1
  74.2 0.0 copy-start.2
  74.2 0.0 copy-start.3
  74.2 0.0 copy-start.4
  74.2 0.0 copy-start.5
  74.2 14.6 %expert.1 = (bf16[640,512]{1,0:T(8,128)(2,1)}, bf16[4096,256]{1,0:T(8,128)(2,1)}, bf16[4096,256]{1,0:T(8,128)(2,1)}, bf16[256,4096]{1,0:T(8,128)(2,1)}) custom-call(bf16[2,2,5,256,1024]{4,3,2,1,0:T(8,128)(2,1)} %get-tuple-element.15.got, bf16[4096,256]{1,0:T(8,128)(2,1)} %bitcast.12, bf16[4096,256]{1,0:T(8,128)(2,1)} %bitcast.14, bf16[256,4096]{1,0:T(8,128)(2,1)} %bitcast.16), custom_call_target="tpu_custom_call" | custom-call | tf_op jit(solution)/shard_map/expert/pallas_call | solution.py:376
  88.9 0.0 copy-done.6
  88.9 0.0 copy-done
  88.9 0.0 copy-done.1
  88.9 0.0 copy-done.2
  88.9 0.0 copy-done.3
  88.9 0.0 copy-done.4
  88.9 0.0 copy-done.5
  88.9 93.7 %tail.1 = (f32[256,256]{1,0:T(8,128)S(1)}, f32[256,256]{1,0:T(8,128)S(1)}, f32[128,256]{1,0:T(8,128)S(1)}) custom-call(bf16[640,512]{1,0:T(8,128)(2,1)} %get-tuple-element.16.slopes, bf16[4096,256]{1,0:T(8,128)(2,1)} %bitcast.13, bf16[4096,256]{1,0:T(8,128)(2,1)} %bitcast.15, bf16[256,768]{1,0:T(8,128)(2,1)S(1)} %copy-done, bf16[256,4096]{1,0:T(8,128)(2,1)} %stream.3, ...), custom_call_target="tpu_custom_call" | custom-call | tf_op jit(solution)/shard_map/tail/pallas_call | solution.py:849
  182.7 0.7 copy.25
  183.4 0.7 copy.26
  184.1 0.7 copy.27
  (1 shorter events, 0.0 us)
Async XLA Ops:
  74.2 14.7 %copy-start.6 = (f32[2,256]{1,0:T(2,128)S(1)}, f32[2,256]{1,0:T(2,128)}, u32[]{:S(2)}) copy-start(f32[2,256]{1,0:T(2,128)} %param.29) | copy-start | bytes 6148
  74.2 14.7 %copy-start = (bf16[256,768]{1,0:T(8,128)(2,1)S(1)}, bf16[256,768]{1,0:T(8,128)(2,1)}, u32[]{:S(2)}) copy-start(bf16[256,768]{1,0:T(8,128)(2,1)} %get-tuple-element.17.combine) | copy-start | bytes 1179652
  74.2 14.7 %copy-start.1 = (bf16[2,1,256,256]{3,2,1,0:T(8,128)(2,1)S(1)}, bf16[2,1,256,256]{3,2,1,0:T(8,128)(2,1)}, u32[]{:S(2)}) copy-start(bf16[2,1,256,256]{3,2,1,0:T(8,128)(2,1)} %param.27) | copy-start | bytes 786436
  74.2 14.7 %copy-start.2 = (bf16[2,1,256,256]{3,2,1,0:T(8,128)(2,1)S(1)}, bf16[2,1,256,256]{3,2,1,0:T(8,128)(2,1)}, u32[]{:S(2)}) copy-start(bf16[2,1,256,256]{3,2,1,0:T(8,128)(2,1)} %param.28) | copy-start | bytes 786436
  74.2 14.7 %copy-start.3 = (bf16[256,256]{1,0:T(8,128)(2,1)S(1)}, bf16[256,256]{1,0:T(8,128)(2,1)}, u32[]{:S(2)}) copy-start(bf16[256,256]{1,0:T(8,128)(2,1)} %branch.1) | copy-start | bytes 393220
  74.2 14.7 %copy-start.4 = (bf16[256,256]{1,0:T(8,128)(2,1)S(1)}, bf16[256,256]{1,0:T(8,128)(2,1)}, u32[]{:S(2)}) copy-start(bf16[256,256]{1,0:T(8,128)(2,1)} %conv.1) | copy-start | bytes 393220
  74.2 14.7 %copy-start.5 = (bf16[4096]{0:T(1024)(128)(2,1)S(1)}, bf16[4096]{0:T(1024)(128)(2,1)}, u32[]{:S(2)}) copy-start(bf16[4096]{0:T(1024)(128)(2,1)} %gain.3) | copy-start | bytes 24580
